TPU v7x, 512 devices: a whole 4x4x16 slice. The times are simulated.
512 devices in a mesh: sp: 32 (over z, core), tp: 16 (over y, x).
Axes of the slice: x: 4, y: 4, z: 16, core: 2. Of those that a mesh axis runs over, the one named last changes fastest.
Arguments:
- moe_input: bfloat16 [10240, 2048], P('sp', 'tp'), may hold values from -6 to 6
- out_cotangent: bfloat16 [10240, 2048], P('sp', 'tp'), may hold values from -0.59765625 to 0.59765625
- routes: int32 [10240, 2], P('sp'), may hold values from 0 to 31, all different within a row; in each aligned block of 320 rows (0 to 319, 320 to 639, ...) at most 30 rows name the same one
- route_weight: float32 [10240, 2], P('sp'), may hold values from 0.1 to 0.9
- gate_weight: bfloat16 [32, 1024, 2048], P('sp', 'tp'), may hold values from -0.125 to 0.125
- up_weight: bfloat16 [32, 1024, 2048], P('sp', 'tp'), may hold values from -0.125 to 0.125
- down_weight: bfloat16 [32, 1024, 2048], P('sp', 'tp'), may hold values from -0.1875 to 0.1875
- glu_value: bfloat16 [10240, 1024], P('sp', 'tp'), may hold values from -6 to 6
- glu_gate: bfloat16 [10240, 1024], P('sp', 'tp'), may hold values from -8 to 8
- conv_result: bfloat16 [10240, 1024], P('sp', 'tp'), may hold values from -12 to 12
- conv_taps: float32 [31, 1024], P(None, 'tp'), may hold values from -1 to 1
- norm_gain: float32 [1024], P('tp'), may hold values from 0.1 to 1.9
- proj_weight: bfloat16 [1024, 2048], P('tp'), may hold values from -0.1875 to 0.1875
Outputs:
- grad_gate: float32 [32, 1024, 2048], P('sp', 'tp')
- grad_up: float32 [32, 1024, 2048], P('sp', 'tp')
- grad_down: float32 [32, 1024, 2048], P('sp', 'tp')
- grad_proj: float32 [2048, 1024], P('sp', 'tp')
- grad_value: bfloat16 [10240, 1024], P('sp', 'tp')
- grad_glu_gate: bfloat16 [10240, 1024], P('sp', 'tp')
Inputs may be any that keep to these rules, and one draw needn't show every extreme that they name: `routes`: each row names two different experts. In the aligned blocks of 320 rows (the rows of one index of sp) no expert is named by more than 30 rows, and that bound is reached.
All inputs are finite; a program needn't handle non-finite values.
Results may differ from a plain program's by a relative error of at most 0.025.
Values may be sent and summed in bfloat16 or wider, within the bound.
No kernel may reach another device: no remote copies, remote signals or barrier semaphores. Data moves between devices by JAX's collectives and lax.ppermute only.
A program may use at most 64 MiB of HBM per device.

v0:
```python
import jax
import jax.numpy as jnp
from jax import lax
from jax.sharding import Mesh
from jax.sharding import PartitionSpec as P

C = 1024
TP = ("tp_0", "tp_1")


NORM_EPS = 0.25


def sent_together(arrays, axis, split_dim, concat_dim, along):
    both = jnp.concatenate(arrays, axis=along)
    whole, at, outs = (
        lax.all_to_all(both, axis, split_axis=split_dim, concat_axis=concat_dim, tiled=True),
        0,
        [],
    )
    for a in arrays:
        outs.append(lax.slice_in_dim(whole, at, at + a.shape[along], axis=along))
        at += a.shape[along]
    return tuple(outs)


def sent_together_2(arrays, axis, dim, along):
    ends, at = ([], 0)
    for a in arrays[:-1]:
        at += a.shape[along]
        ends.append(at)
    both = jnp.concatenate(arrays, axis=along)
    return tuple(jnp.split(lax.all_gather(both, axis, axis=dim, tiled=True), ends, axis=along))


def cut_along(value, dim, length):
    lengths = value.shape
    tiles = value.reshape(*lengths[:dim], length, lengths[dim] // length, *lengths[dim + 1 :])
    return jnp.moveaxis(tiles, dim, 0)


def summed_on_arrival(value, axis, dim):
    tiles = cut_along(value, dim, lax.axis_size(axis))
    arrived = lax.all_to_all(tiles, axis, split_axis=0, concat_axis=0, tiled=True)
    return arrived.astype(jnp.float32).sum(axis=0)


def one_axis_at_a_time(value, axes):
    for axis in axes:
        value = lax.psum(value, axis)
    return value


def joined_along(tiles, dim):
    lengths = list(tiles.shape[1:])
    lengths[dim] *= tiles.shape[0]
    return jnp.moveaxis(tiles, 0, dim).reshape(lengths)


def sent_to_all(value, axis):
    length = lax.axis_size(axis)
    return lax.all_to_all(
        jnp.broadcast_to(value[None], (length, *value.shape)), axis, 0, 0, tiled=True
    )


def gather_directly(value, axis, dim):
    return joined_along(sent_to_all(value, axis), dim)


def from_behind(value, axis, steps):
    count = lax.axis_size(axis)
    leading, last = (max(0, -steps), min(count, count - steps))
    return lax.ppermute(value, axis, [(source, source + steps) for source in range(leading, last)])


def pair_places(route_ids, experts, capacity):
    flat_ids = route_ids.reshape(-1)
    onehot = (flat_ids[:, None] == jnp.arange(experts, dtype=jnp.int32)[None, :]).astype(jnp.int32)
    earlier = jnp.cumsum(onehot, axis=0) - onehot
    slot_rank = jnp.sum(earlier * onehot, axis=1)
    return flat_ids * capacity + slot_rank


def place_rows(values, target, experts, capacity):
    empty_rows = jnp.zeros((experts * capacity, values.shape[1]), values.dtype)
    return empty_rows.at[target].set(values).reshape(experts, capacity, values.shape[1])


def contract_rows(left, right):
    return lax.dot_general(
        left, right, (((0,), (0,)), ((), ())), preferred_element_type=jnp.float32
    )


def contract_cols(left, right):
    return lax.dot_general(
        left, right, (((1,), (1,)), ((), ())), preferred_element_type=jnp.float32
    )


def expert_backward(token_rows, cot_rows, gate_matrix, up_matrix, down_matrix):
    gate_pre = contract_cols(token_rows, gate_matrix)
    up_pre = contract_cols(token_rows, up_matrix)
    gate_sigmoid = jax.nn.sigmoid(gate_pre)
    activation = gate_pre * gate_sigmoid
    hidden = (activation * up_pre).astype(jnp.bfloat16)
    grad_down = contract_rows(hidden, cot_rows)
    hidden_cot = contract_cols(cot_rows, down_matrix)
    up_cot = (hidden_cot * activation).astype(jnp.bfloat16)
    gate_cot = (
        hidden_cot * up_pre * gate_sigmoid * (1.0 + gate_pre * (1.0 - gate_sigmoid))
    ).astype(jnp.bfloat16)
    grad_gate = contract_rows(gate_cot, token_rows)
    grad_up = contract_rows(up_cot, token_rows)
    partial_value = jnp.dot(gate_cot, gate_matrix, preferred_element_type=jnp.float32) + jnp.dot(
        up_cot, up_matrix, preferred_element_type=jnp.float32
    )
    return (
        grad_gate[None],
        grad_up[None],
        grad_down[None],
        partial_value.astype(jnp.bfloat16)[None],
    )


def body(
    moe_input,
    out_cotangent,
    routes,
    route_weight,
    gate_weight,
    up_weight,
    down_weight,
    glu_value,
    glu_gate,
    conv_result,
    conv_taps,
    norm_gain,
    proj_weight,
):
    sp_count = lax.axis_size("sp")
    token_count = moe_input.shape[0]
    experts = sp_count * gate_weight.shape[0]
    capacity = 3 * token_count // experts
    target = pair_places(routes, experts, capacity)
    weights = route_weight.reshape(-1, 1)
    pair_rows = jnp.repeat(moe_input, 2, axis=0)
    scaled = (weights * jnp.repeat(out_cotangent, 2, axis=0).astype(jnp.float32)).astype(
        jnp.bfloat16
    )
    sent_rows = place_rows(pair_rows, target, experts, capacity)
    sent_cot = place_rows(scaled, target, experts, capacity)
    got_rows, got_cot = sent_together((sent_rows, sent_cot), "sp", 0, 1, 2)
    full_rows, full_cot = sent_together_2((got_rows, got_cot), TP, 2, 0)
    grad_gate, grad_up, grad_down, partial_value = expert_backward(
        full_rows[0], full_cot[0], gate_weight[0], up_weight[0], down_weight[0]
    )
    summed = summed_on_arrival(partial_value, TP, 2).astype(jnp.bfloat16)
    returned_slices = lax.all_to_all(summed, "sp", split_axis=1, concat_axis=0, tiled=True)
    returned = returned_slices.reshape(experts * capacity, -1)[target]
    moe_grad = jnp.sum(returned.astype(jnp.float32).reshape(token_count, 2, -1), axis=1)
    total_cot = (out_cotangent.astype(jnp.float32) + moe_grad).astype(jnp.bfloat16)
    conv_values = conv_result.astype(jnp.float32)
    moments = (
        one_axis_at_a_time(jnp.sum(conv_values, axis=1), TP),
        one_axis_at_a_time(jnp.sum(conv_values * conv_values, axis=1), TP),
    )
    row_mean = moments[0][:, None] / C
    row_var = moments[1][:, None] / C - row_mean * row_mean
    inv_scale = lax.rsqrt(row_var + NORM_EPS)
    normed = (conv_values - row_mean) * inv_scale
    linear = normed * norm_gain[None, :]
    lin_sigmoid = jax.nn.sigmoid(linear)
    act_out = (linear * lin_sigmoid).astype(jnp.bfloat16)
    cot_full = gather_directly(total_cot, TP, 1)
    act_cot = contract_cols(cot_full, proj_weight)
    grad_proj = summed_on_arrival(contract_rows(cot_full, act_out).astype(jnp.bfloat16), "sp", 0)
    norm_cot = act_cot * lin_sigmoid * (1.0 + linear * (1.0 - lin_sigmoid)) * norm_gain[None, :]
    cot_sums = (
        one_axis_at_a_time(jnp.sum(norm_cot, axis=1), TP),
        one_axis_at_a_time(jnp.sum(norm_cot * normed, axis=1), TP),
    )
    conv_cot = inv_scale * (
        norm_cot - cot_sums[0][:, None] / C - normed * (cot_sums[1][:, None] / C)
    )
    reach_rows = conv_taps.shape[0] - 1
    next_block = from_behind(conv_cot[:reach_rows], "sp", -1)
    extended = jnp.concatenate([conv_cot, next_block], axis=0)
    glu_cot = lax.conv_general_dilated(
        extended[None],
        jnp.flip(conv_taps, 0)[:, None, :],
        (1,),
        "VALID",
        dimension_numbers=("NWC", "WIO", "NWC"),
        feature_group_count=conv_taps.shape[1],
        precision=lax.Precision.HIGHEST,
    )[0]
    gate_sigmoid = jax.nn.sigmoid(glu_gate.astype(jnp.float32))
    grad_value = (glu_cot * gate_sigmoid).astype(jnp.bfloat16)
    grad_glu_gate = (
        glu_cot * glu_value.astype(jnp.float32) * gate_sigmoid * (1.0 - gate_sigmoid)
    ).astype(jnp.bfloat16)
    return (grad_gate, grad_up, grad_down, grad_proj, grad_value, grad_glu_gate)


def solution(mesh):
    split = Mesh(mesh.devices.reshape(mesh.shape["sp"], 4, 4), ("sp", "tp_0", "tp_1"))
    placed = (
        P("sp", TP),
        P("sp", TP),
        P("sp", None),
        P("sp", None),
        P("sp", TP, None),
        P("sp", TP, None),
        P("sp", TP, None),
        P("sp", TP),
        P("sp", TP),
        P("sp", TP),
        P(None, TP),
        P(TP),
        P(TP, None),
    )
    return jax.shard_map(
        body,
        mesh=split,
        in_specs=placed,
        out_specs=(
            P("sp", TP, None),
            P("sp", TP, None),
            P("sp", TP, None),
            P("sp", TP),
            P("sp", TP),
            P("sp", TP),
        ),
        check_vma=False,
    )
```

profile of v0, /device:TPU:1, one launch (start us, length us, event | category | flops | bytes accessed | tf_op | source)
XLA Modules:
  0.0 346.5 jit_solution(8437389909996260354)
XLA Ops:
  9.4 1.5 reduce-window.6
  13.2 4.9 %scatter_custom_fusion.1 = bf16[960,128]{1,0:T(8,128)(2,1)S(1)} fusion(s32[640]{0:T(1024)S(1)} %fusion.69, f32[640,128]{1,0:T(8,128)S(1)} %bitcast.133, f32[640]{0:T(1024)S(1)} %mul.124, bf16[]{:T(256)} %constant.10.clone.1), kind=kCustom, calls=%fused_computation.49 | custom fusion | flops 163840 | bytes 577538 | tf_op jit(solution)/shard_map/scatter | solution.py:87
  19.1 4.3 %scatter_custom_fusion = bf16[960,128]{1,0:T(8,128)(2,1)S(1)} fusion(s32[640]{0:T(1024)S(1)} %fusion.69, bf16[640,128]{1,0:T(8,128)(2,1)S(1)} %bitcast.136, bf16[]{:T(256)} %constant.10.clone.1), kind=kCustom, calls=%fused_computation.58 | custom fusion | bytes 245762 | tf_op jit(solution)/shard_map/scatter | solution.py:87
  23.6 50.1 %all_to_all.36 = bf16[32,30,256]{2,1,0:T(8,128)(2,1)S(1)} all-to-all(bf16[32,30,256]{2,1,0:T(8,128)(2,1)S(1)} %pad_maximum_fusion), channel_id=1, replica_groups=mesh['sp'=32,'tp_0'=4,'tp_1'=4] {'sp'}, dimensions={0} | all-to-all | bytes 983040 | tf_op jit(solution)/shard_map/all_to_all | solution.py:17
  74.7 80.0 %all-gather.2.cloned.1.call-done = bf16[2,960,2048]{2,1,0:T(8,128)(2,1)} async-done(((bf16[2,960,128]{2,1,0:T(8,128)(2,1)}), bf16[2,960,2048]{2,1,0:T(8,128)(2,1)}) %all-gather.2.cloned.1.call-update) | async-done | bytes 7864336 | tf_op jit(solution)/shard_map/all_gather | solution.py:33
  154.7 3.5 %fusion.4 = f32[960,64]{0,1:T(8,128)S(1)} fusion(bf16[2,960,2048]{2,1,0:T(8,128)(2,1)} %all-gather.2.cloned.1.call-done, bf16[1,64,2048]{2,1,0:T(8,128)(2,1)S(1)} %copy-done), kind=kOutput, calls=%fused_computation.11 | convolution fusion | flops 251658240 | bytes 4440064 | tf_op jit(solution)/shard_map/dot_general | solution.py:97
  160.4 1.3 multiply_convert_fusion.2
  166.5 51.6 %all_to_all.37 = bf16[16,1,960,128]{3,2,1,0:T(8,128)(2,1)} all-to-all(bf16[16,1,960,128]{3,2,1,0:T(8,128)(2,1)S(1)} %bitcast.128), channel_id=1, replica_groups=mesh['sp'=32,'tp_0'=4,'tp_1'=4] {'tp_0','tp_1'}, dimensions={0} | all-to-all | bytes 7864320 | tf_op jit(solution)/shard_map/all_to_all | solution.py:44
  218.0 2.8 reduce_sum.81
  221.7 2.1 reduce.6
  224.6 15.7 %all-to-all-start.2 = ((bf16[32,2,1920]{2,1,0:T(2,128)(2,1)}), bf16[32,2,1920]{2,1,0:T(2,128)(2,1)S(1)}, u32[]{:S(2)}, u32[]{:S(2)}) async-start(bf16[32,2,1920]{2,1,0:T(2,128)(2,1)} %reshape.154), calls=%async_computation.2 | async-start | bytes 491520 | tf_op jit(solution)/shard_map/all_to_all | solution.py:160
  240.3 20.9 %all-to-all-done.2 = bf16[32,2,1920]{2,1,0:T(2,128)(2,1)S(1)} async-done(((bf16[32,2,1920]{2,1,0:T(2,128)(2,1)}), bf16[32,2,1920]{2,1,0:T(2,128)(2,1)S(1)}, u32[]{:S(2)}, u32[]{:S(2)}) %all-to-all-start.2) | async-done | bytes 245792 | tf_op jit(solution)/shard_map/all_to_all | solution.py:160
  261.5 2.0 gather_fusion
  264.0 1.4 broadcast_in_dim.42
  265.4 3.7 %all-to-all-start.3 = ((bf16[16,320,128]{2,1,0:T(8,128)(2,1)}), bf16[16,320,128]{2,1,0:T(8,128)(2,1)S(1)}, u32[]{:S(2)}, u32[]{:S(2)}) async-start(bf16[16,320,128]{2,1,0:T(8,128)(2,1)} %broadcast_in_dim.42), calls=%async_computation.3 | async-start | bytes 2621440 | tf_op jit(solution)/shard_map/all_to_all | solution.py:62
  269.2 14.1 %all-reduce.3 = (f32[320]{0:T(512)S(1)}, f32[320]{0:T(512)S(1)}) all-reduce(f32[320]{0:T(512)S(1)} %get-tuple-element.21, f32[320]{0:T(512)S(1)} %get-tuple-element.20), channel_id=1, replica_groups=mesh['sp'=32,'tp_0'=4,'tp_1'=4] {'tp_0'}, use_global_device_ids=true, to_apply=%region_11.12 | all-reduce | flops 640 | bytes 5120 | tf_op jit(solution)/shard_map/psum | solution.py:50
  283.4 13.1 %all-reduce.1 = (f32[320]{0:T(512)S(1)}, f32[320]{0:T(512)S(1)}) all-reduce(f32[320]{0:T(512)S(1)} %get-tuple-element.28, f32[320]{0:T(512)S(1)} %get-tuple-element.29), channel_id=1, replica_groups=mesh['sp'=32,'tp_0'=4,'tp_1'=4] {'tp_1'}, use_global_device_ids=true, to_apply=%region_12.13 | all-reduce | flops 640 | bytes 5120 | tf_op jit(solution)/shard_map/psum | solution.py:50
  296.5 3.7 %fusion.6 = f32[1,64,2048]{2,1,0:T(8,128)} fusion(bf16[960,64]{0,1:T(8,128)(2,1)S(1)} %get-tuple-element.31, bf16[2,960,2048]{2,1,0:T(8,128)(2,1)} %all-gather.2.cloned.1.call-done), kind=kOutput, calls=%fused_computation.13 | convolution fusion | flops 251658240 | bytes 4579328 | tf_op jit(solution)/shard_map/dot_general | solution.py:91
  300.2 3.7 %fusion.8 = f32[1,64,2048]{2,1,0:T(8,128)} fusion(bf16[2,960,2048]{2,1,0:T(8,128)(2,1)} %all-gather.2.cloned.1.call-done, f32[960,64]{0,1:T(8,128)S(1)} %fusion.5, f32[960,64]{0,1:T(8,128)S(1)} %fusion.4), kind=kOutput, calls=%fused_computation.15 | convolution fusion | flops 252026880 | bytes 4947968 | tf_op jit(solution)/shard_map/dot_general | solution.py:91
  306.2 7.8 %all-to-all-start.4 = ((bf16[32,2,2048]{2,1,0:T(2,128)(2,1)}), bf16[32,2,2048]{2,1,0:T(2,128)(2,1)S(1)}, u32[]{:S(2)}, u32[]{:S(2)}) async-start(bf16[32,2,2048]{2,1,0:T(2,128)(2,1)} %reshape.156), calls=%async_computation.4 | async-start | bytes 524288 | tf_op jit(solution)/shard_map/all_to_all | solution.py:44
  314.6 6.6 %all-reduce.2 = (f32[320]{0:T(512)S(1)}, f32[320]{0:T(512)S(1)}) all-reduce(f32[320]{0:T(512)S(1)} %get-tuple-element.19, f32[320]{0:T(512)S(1)} %get-tuple-element.18), channel_id=1, replica_groups=mesh['sp'=32,'tp_0'=4,'tp_1'=4] {'tp_0'}, use_global_device_ids=true, to_apply=%region_18.19 | all-reduce | flops 640 | bytes 5120 | tf_op jit(solution)/shard_map/psum | solution.py:50
  321.1 6.6 %all-reduce = (f32[320]{0:T(512)S(1)}, f32[320]{0:T(512)S(1)}) all-reduce(f32[320]{0:T(512)S(1)} %get-tuple-element.26, f32[320]{0:T(512)S(1)} %get-tuple-element.27), channel_id=1, replica_groups=mesh['sp'=32,'tp_0'=4,'tp_1'=4] {'tp_1'}, use_global_device_ids=true, to_apply=%region_19.20 | all-reduce | flops 640 | bytes 5120 | tf_op jit(solution)/shard_map/psum | solution.py:50
  327.8 5.1 %collective-permute-start = (f32[30,64]{0,1:T(8,128)S(1)}, f32[30,64]{0,1:T(8,128)S(1)}, u32[]{:S(2)}, u32[]{:S(2)}) collective-permute-start(f32[30,64]{0,1:T(8,128)S(1)} %slice.27), channel_id=1, source_target_pairs={{16,0},{32,16},{48,32},{64,48},{80,64},{96,80},{112,96},{128,112},... | collective-permute-start | bytes 23048 | tf_op jit(solution)/shard_map/ppermute | solution.py:74
  332.9 3.7 %fusion.7 = f32[1,64,2048]{2,1,0:T(8,128)} fusion(bf16[960,64]{0,1:T(8,128)(2,1)S(1)} %get-tuple-element.30, bf16[2,960,2048]{2,1,0:T(8,128)(2,1)} %all-gather.2.cloned.1.call-done), kind=kOutput, calls=%fused_computation.14 | convolution fusion | flops 251658240 | bytes 4579328 | tf_op jit(solution)/shard_map/dot_general | solution.py:91
  (86 shorter events, 21.9 us)
Async XLA Ops:
  7.2 147.5 %copy-start = (bf16[1,64,2048]{2,1,0:T(8,128)(2,1)S(1)}, bf16[1,64,2048]{2,1,0:T(8,128)(2,1)}, u32[]{:S(2)}) copy-start(bf16[1,64,2048]{2,1,0:T(8,128)(2,1)} %param.17) | copy-start | bytes 786436
  7.2 147.5 %all-gather.2.cloned.1.call-start = ((), (), s32[]{:S(2)}) async-start(), calls=%async_computation.5 | async-start | bytes 8355840 | tf_op jit(solution)/shard_map/all_gather | solution.py:33
  74.6 83.6 %copy-start.2 = (bf16[1,64,2048]{2,1,0:T(8,128)(2,1)S(1)}, bf16[1,64,2048]{2,1,0:T(8,128)(2,1)}, u32[]{:S(2)}) copy-start(bf16[1,64,2048]{2,1,0:T(8,128)(2,1)} %param.18) | copy-start | bytes 786436
  154.7 4.4 %copy-start.7 = (bf16[2,960,2048]{2,1,0:T(8,128)(2,1)S(1)}, bf16[2,960,2048]{2,1,0:T(8,128)(2,1)}, u32[]{:S(2)}) copy-start(bf16[2,960,2048]{2,1,0:T(8,128)(2,1)} %all-gather.2.cloned.1.call-done) | copy-start | bytes 23592964
  159.1 1.3 copy-start.8
  218.0 45.9 %copy-start.1 = (bf16[320,128]{1,0:T(8,128)(2,1)S(1)}, bf16[320,128]{1,0:T(8,128)(2,1)}, u32[]{:S(2)}) copy-start(bf16[320,128]{1,0:T(8,128)(2,1)} %param.14) | copy-start | bytes 245764
  224.6 36.7 %all-to-all-start.2 = ((bf16[32,2,1920]{2,1,0:T(2,128)(2,1)}), bf16[32,2,1920]{2,1,0:T(2,128)(2,1)S(1)}, u32[]{:S(2)}, u32[]{:S(2)}) async-start(bf16[32,2,1920]{2,1,0:T(2,128)(2,1)} %reshape.154), calls=%async_computation.2 | async-start | bytes 491520 | tf_op jit(solution)/shard_map/all_to_all | solution.py:160
  240.3 28.9 %copy-start.6 = (f32[31,64]{1,0:T(8,128)S(1)}, f32[31,64]{1,0:T(8,128)}, u32[]{:S(2)}) copy-start(f32[31,64]{1,0:T(8,128)} %param.23) | copy-start | bytes 23812
  240.3 28.9 %copy-start.3 = (bf16[320,64]{0,1:T(8,128)(2,1)S(1)}, bf16[320,64]{0,1:T(8,128)(2,1)}, u32[]{:S(2)}) copy-start(bf16[320,64]{0,1:T(8,128)(2,1)} %param.22) | copy-start | bytes 122884
  265.4 38.5 %all-to-all-start.3 = ((bf16[16,320,128]{2,1,0:T(8,128)(2,1)}), bf16[16,320,128]{2,1,0:T(8,128)(2,1)S(1)}, u32[]{:S(2)}, u32[]{:S(2)}) async-start(bf16[16,320,128]{2,1,0:T(8,128)(2,1)} %broadcast_in_dim.42), calls=%async_computation.3 | async-start | bytes 2621440 | tf_op jit(solution)/shard_map/all_to_all | solution.py:62
  300.2 3.7 %copy-start.10 = (f32[64]{0:T(128)S(1)}, f32[64]{0:T(128)}, u32[]{:S(2)}) copy-start(f32[64]{0:T(128)} %param.24) | copy-start | bytes 772
  303.9 10.1 %copy-start.9 = (bf16[64,2048]{1,0:T(8,128)(2,1)S(1)}, bf16[64,2048]{1,0:T(8,128)(2,1)}, u32[]{:S(2)}) copy-start(bf16[64,2048]{1,0:T(8,128)(2,1)} %param.25) | copy-start | bytes 786436
  306.2 32.3 %all-to-all-start.4 = ((bf16[32,2,2048]{2,1,0:T(2,128)(2,1)}), bf16[32,2,2048]{2,1,0:T(2,128)(2,1)S(1)}, u32[]{:S(2)}, u32[]{:S(2)}) async-start(bf16[32,2,2048]{2,1,0:T(2,128)(2,1)} %reshape.156), calls=%async_computation.4 | async-start | bytes 524288 | tf_op jit(solution)/shard_map/all_to_all | solution.py:44
  314.6 22.5 %copy-start.11 = (pred[8,44]{0,1:T(8,128)(4,1)S(1)}, pred[8,44]{0,1:T(8,128)(4,1)}, u32[]{:S(2)}) copy-start(pred[8,44]{0,1:T(8,128)(4,1)} %constant.36) | copy-start | bytes 1060
  327.8 8.9 %collective-permute-start = (f32[30,64]{0,1:T(8,128)S(1)}, f32[30,64]{0,1:T(8,128)S(1)}, u32[]{:S(2)}, u32[]{:S(2)}) collective-permute-start(f32[30,64]{0,1:T(8,128)S(1)} %slice.27), channel_id=1, source_target_pairs={{16,0},{32,16},{48,32},{64,48},{80,64},{96,80},{112,96},{128,112},... | collective-permute-start | bytes 23048 | tf_op jit(solution)/shard_map/ppermute | solution.py:74
  336.6 1.2 copy-start.4
  336.6 1.2 copy-start.5
Sparse Core Ops, SparseCore 0:
  74.8 79.8 all-gather.1
where the time goes:
time: 347 us
  blocking collectives  142 us (41%)
  waiting for transfers between devices  101 us (29%)
  starting transfers between devices  32.4 us (9%)
  local copies, waits for them, and re-layouts  21.2 us (6%)
  matrix products  21.1 us (6%)
  between operations  14.5 us (4%)
  other arithmetic  14.4 us (4%)
    all_gather x1, waiting for transfers between devices, sent_together_2(): lax.all_gather(both, axis, axis=dim, tiled=True)  80 us
    all_to_all x1, blocking collectives, summed_on_arrival(): lax.all_to_all(tiles, axis, split_axis=0, concat_axis=0, tiled=True)  51.6 us
    all_to_all x1, blocking collectives, sent_together(): lax.all_to_all(both, axis, split_axis=split_dim, concat_axis=concat_dim,...  50.1 us
    psum x4, blocking collectives, one_axis_at_a_time(): value = lax.psum(value, axis)  40.4 us
    all_to_all x1, waiting for transfers between devices, body(): lax.all_to_all(summed, 'sp', split_axis=1, concat_axis=0, tiled=True)  20.9 us
    all_to_all x1, starting transfers between devices, body(): lax.all_to_all(summed, 'sp', split_axis=1, concat_axis=0, tiled=True)  15.7 us
    dot_general x4, matrix products, contract_rows(): lax.dot_general(left, right, (((0,), (0,)), ((), ())), preferred_element_...  11.6 us
    all_to_all x1, starting transfers between devices, summed_on_arrival(): lax.all_to_all(tiles, axis, split_axis=0, concat_axis=0, tiled=True)  7.81 us
  transfers between devices with their start and end apart: 5, of which 2 were waited for; matrix products, arithmetic and copies ran while one was open for 4% of the time, Pallas kernels for 0%

commit v1 on v0

v1 whole, which is shorter than its diff:
```python
import jax
import jax.numpy as jnp
from jax import lax
from jax.experimental import pallas as pl
from jax.experimental.pallas import tpu as pltpu
from jax.sharding import Mesh
from jax.sharding import PartitionSpec as P

NORM_EPS = 0.25
SP = ("z", "c")
TP = ("y", "x")
PLANE = ("c", "y", "x")
SIDE = 4
SLOT = 32
BF = jnp.bfloat16
F32 = jnp.float32
VM = pltpu.VMEM

NT = (((1,), (1,)), ((), ()))
TN = (((0,), (0,)), ((), ()))
NN = (((1,), (0,)), ((), ()))


def place(core, row, col):
    return core * SIDE * SIDE + row * SIDE + col


def plane_groups():
    r = range(SIDE)
    down = [[[place(k, y, x) for y in r] for x in r] for k in (0, 1)]
    across = [[[place(k, y, x) for x in r] for y in r] for k in (0, 1)]
    return down[0] + across[1], across[0] + down[1]


def mm(a, b, dims):
    return lax.dot_general(a, b, dims, preferred_element_type=F32)


def exchange(v, groups):
    return lax.all_to_all(v, PLANE, 0, 0, axis_index_groups=groups, tiled=True)


def cost(flops, nbytes):
    return pl.CostEstimate(flops=flops, bytes_accessed=nbytes, transcendentals=0)


def route_kernel(rt_ref, w_ref, x_ref, c_ref, s_ref, p_ref):
    tokens = rt_ref.shape[1]
    experts = s_ref.shape[0] // SLOT
    first, second = rt_ref[0:1, :], rt_ref[1:2, :]
    ids = lax.broadcasted_iota(jnp.int32, (experts, tokens), 0)
    o0, o1 = ids == first, ids == second
    both = jnp.where(o0 | o1, 1.0, 0.0).astype(BF)
    before = lax.broadcasted_iota(jnp.int32, (tokens, tokens), 0) < lax.broadcasted_iota(
        jnp.int32, (tokens, tokens), 1
    )
    earlier = mm(both, jnp.where(before, 1.0, 0.0).astype(BF), NN)
    rank0 = jnp.sum(jnp.where(o0, earlier, 0.0), axis=0, keepdims=True)
    rank1 = jnp.sum(jnp.where(o1, earlier, 0.0), axis=0, keepdims=True)
    t0 = first * SLOT + rank0.astype(jnp.int32)
    t1 = second * SLOT + rank1.astype(jnp.int32)
    w0, w1 = w_ref[0:1, :], w_ref[1:2, :]
    x, c = x_ref[...], c_ref[...]
    size = 128
    for k in range(s_ref.shape[0] // size):
        slots = lax.broadcasted_iota(jnp.int32, (size, tokens), 0) + k * size
        m0, m1 = slots == t0, slots == t1
        pick = jnp.where(m0 | m1, 1.0, 0.0).astype(BF)
        weight = jnp.sum(
            jnp.where(m0, w0, 0.0) + jnp.where(m1, w1, 0.0), axis=1, keepdims=True
        )
        rows = pl.ds(k * size, size)
        p_ref[rows, :] = pick
        s_ref[rows, 0:128] = mm(pick, x, NN).astype(BF)
        s_ref[rows, 128:256] = (weight * mm(pick, c, NN)).astype(BF)


def split_kernel(core_ref, g_ref, u_ref, d_ref, o_ref):
    core = core_ref[0]
    for b in range(SIDE):
        for a in range(SIDE):
            at = jnp.where(core == 0, a * SIDE + b, b * SIDE + a)
            cols = pl.ds(pl.multiple_of(at * 128, 128), 128)
            for q, ref in enumerate((g_ref, u_ref, d_ref)):
                o_ref[b, q * 64 : q * 64 + 64, a * 128 : a * 128 + 128] = ref[:, cols]


def merge_kernel(core_ref, s_ref, g_ref, u_ref, d_ref):
    core = core_ref[0]
    for b in range(SIDE):
        for a in range(SIDE):
            at = jnp.where(core == 0, a * SIDE + b, b * SIDE + a)
            cols = pl.ds(pl.multiple_of(at * 128, 128), 128)
            for q, ref in enumerate((g_ref, u_ref, d_ref)):
                ref[:, cols] = s_ref[
                    b, q * 64 : q * 64 + 64, a * 128 : a * 128 + 128
                ].astype(F32)


def pre_kernel(a_ref, w_ref, o_ref):
    x = jnp.concatenate([a_ref[i, :, 0:128] for i in range(SIDE)], axis=1)
    c = jnp.concatenate([a_ref[i, :, 128:256] for i in range(SIDE)], axis=1)
    for b in range(SIDE):
        o_ref[b, 0:128, :] = mm(w_ref[b, 0:128, :], x, NT).astype(BF)
        o_ref[b, 128:192, :] = mm(w_ref[b, 128:192, :], c, NT).astype(BF)


def gate_kernel(p_ref, o_ref):
    total = p_ref[0].astype(F32)
    for b in range(1, SIDE):
        total = total + p_ref[b].astype(F32)
    gate, up, cot = total[0:64], total[64:128], total[128:192]
    s = jax.nn.sigmoid(gate)
    act = gate * s
    hidden = (act * up).astype(BF)
    up_cot = (cot * act).astype(BF)
    gate_cot = (cot * up * s * (1.0 + gate * (1.0 - s))).astype(BF)
    for b in range(SIDE):
        o_ref[b, 0:64, :] = gate_cot
        o_ref[b, 64:128, :] = up_cot
        o_ref[b, 128:192, :] = hidden


def partial_kernel(h_ref, w_ref, o_ref):
    h = jnp.concatenate([h_ref[b, 0:128, :] for b in range(SIDE)], axis=0)
    w = jnp.concatenate([w_ref[b, 0:128, :] for b in range(SIDE)], axis=0)
    total = mm(h, w, TN)
    for a in range(SIDE):
        o_ref[a] = total[:, a * 128 : a * 128 + 128].astype(BF)


def grads_kernel(h_ref, a_ref, o_ref):
    x, c = a_ref[0, :, 0:128], a_ref[0, :, 128:256]
    for b in range(SIDE):
        o_ref[b, 0:128, :] = mm(h_ref[b, 0:128, :], x, NN).astype(BF)
        o_ref[b, 128:192, :] = mm(h_ref[b, 128:192, :], c, NN).astype(BF)


def combine_kernel(p_ref, r_ref, c_ref, o_ref):
    moe = mm(p_ref[...], r_ref[...], TN)
    total = (c_ref[...].astype(F32) + moe).astype(BF)
    for b in range(o_ref.shape[0]):
        o_ref[b] = total


def normed_of(conv, sums, channels):
    mean = sums[0:1, :] / channels
    var = sums[1:2, :] / channels - mean * mean
    inv = lax.rsqrt(var + NORM_EPS)
    return (conv.astype(F32) - mean) * inv, inv


def proj_kernel(f_ref, conv_ref, sums_ref, gain_ref, o_ref):
    channels = 16 * conv_ref.shape[0]
    normed, _ = normed_of(conv_ref[...], sums_ref[...], channels)
    linear = normed * gain_ref[...]
    act = (linear * jax.nn.sigmoid(linear)).astype(BF)
    low = lax.broadcasted_iota(jnp.int32, (32, 128), 1) < 64
    for b in range(f_ref.shape[0]):
        g = mm(act, f_ref[b], NN)
        turned = pltpu.roll(g, 64, 1)
        o_ref[2 * b] = jnp.where(low, g[0:32], turned[32:64]).astype(BF)
        o_ref[2 * b + 1] = jnp.where(low, turned[0:32], g[32:64]).astype(BF)


def norm_kernel(f_ref, proj_ref, conv_ref, sums_ref, gain_ref, n_ref, t_ref):
    channels = 16 * conv_ref.shape[0]
    total = mm(proj_ref[:, 0:128], f_ref[0], NT)
    for b in range(1, f_ref.shape[0]):
        total = total + mm(proj_ref[:, b * 128 : b * 128 + 128], f_ref[b], NT)
    normed, _ = normed_of(conv_ref[...], sums_ref[...], channels)
    gain = gain_ref[...]
    linear = normed * gain
    s = jax.nn.sigmoid(linear)
    cot = total * s * (1.0 + linear * (1.0 - s)) * gain
    n_ref[...] = cot
    t_ref[0:1, :] = jnp.sum(cot, axis=0, keepdims=True)
    t_ref[1:2, :] = jnp.sum(cot * normed, axis=0, keepdims=True)


def head_kernel(n_ref, t_ref, conv_ref, sums_ref, o_ref, h_ref):
    channels = 16 * conv_ref.shape[0]
    normed, inv = normed_of(conv_ref[...], sums_ref[...], channels)
    t = t_ref[...]
    cot = inv * (n_ref[...] - t[0:1, :] / channels - normed * (t[1:2, :] / channels))
    o_ref[...] = cot
    h_ref[...] = cot[:, 0:128]


def conv_kernel(cot_ref, next_ref, taps_ref, gate_ref, value_ref, v_ref, g_ref, buf):
    rows, tokens = cot_ref.shape
    wide = buf.shape[1]
    reach = taps_ref.shape[1] - 1
    buf[:, 0:128] = next_ref[...]
    buf[:, 128:wide] = jnp.zeros((rows, wide - 128), F32)
    after = pltpu.roll(buf[...], tokens, 1)
    buf[:, 0:tokens] = cot_ref[...]
    lane = lax.broadcasted_iota(jnp.int32, (rows, wide), 1)
    whole = jnp.where(lane < tokens, buf[...], after)
    taps = taps_ref[...]
    total = whole * taps[:, reach : reach + 1]
    for s in range(1, reach + 1):
        total = total + pltpu.roll(whole, wide - s, 1) * taps[:, reach - s : reach - s + 1]
    cot = total[:, 0:tokens]
    s = jax.nn.sigmoid(gate_ref[...].astype(F32))
    v_ref[...] = (cot * s).astype(BF)
    g_ref[...] = (cot * value_ref[...].astype(F32) * s * (1.0 - s)).astype(BF)


def whole(shape, dtype):
    return jax.ShapeDtypeStruct(shape, dtype)


def body(
    moe_input,
    out_cotangent,
    routes,
    route_weight,
    gate_weight,
    up_weight,
    down_weight,
    glu_value,
    glu_gate,
    conv_result,
    conv_taps,
    norm_gain,
    proj_weight,
):
    sp_count = lax.axis_size(SP)
    tp_count = lax.axis_size(TP)
    tokens = moe_input.shape[0]
    slots = sp_count * SLOT
    feature_groups, unit_groups = plane_groups()
    core = lax.axis_index("c").reshape(1).astype(jnp.int32)
    smem = pl.BlockSpec(memory_space=pltpu.SMEM)
    vmem = pl.BlockSpec(memory_space=VM)

    split = pl.pallas_call(
        split_kernel,
        out_shape=whole((SIDE, 192, 512), BF),
        in_specs=[smem, vmem, vmem, vmem],
        out_specs=vmem,
        cost_estimate=cost(1000000, 1600000),
        name="split_weights",
    )(core, gate_weight[0], up_weight[0], down_weight[0])
    weights = exchange(split, unit_groups)

    sent, pick = pl.pallas_call(
        route_kernel,
        out_shape=(whole((slots, 256), BF), whole((slots, tokens), BF)),
        in_specs=[vmem] * 4,
        out_specs=(vmem, vmem),
        cost_estimate=cost(400000000, 2000000),
        name="route",
    )(routes.T, route_weight.T, moe_input, out_cotangent)
    weights, sent = lax.optimization_barrier((weights, sent))
    got = lax.all_to_all(sent.reshape(sp_count, SLOT, 256), SP, 0, 0, tiled=True)
    got = got.reshape(slots, 256)

    conv_t = conv_result.T
    conv_f = conv_t.astype(F32)
    sums = jnp.stack([jnp.sum(conv_f, axis=0), jnp.sum(conv_f * conv_f, axis=0)])
    sums = lax.psum(lax.psum(sums, "y"), "x")
    got, sums = lax.optimization_barrier((got, sums))
    gain = norm_gain.reshape(-1, 1)
    taps_t = conv_taps.T

    rows = exchange(jnp.broadcast_to(got[None], (SIDE, slots, 256)), feature_groups)
    step = 256
    pre = pl.pallas_call(
        pre_kernel,
        grid=(slots // step,),
        out_shape=whole((SIDE, 192, slots), BF),
        in_specs=[
            pl.BlockSpec((SIDE, step, 256), lambda i: (0, i, 0)),
            pl.BlockSpec((SIDE, 192, 512), lambda i: (0, 0, 0)),
        ],
        out_specs=pl.BlockSpec((SIDE, 192, step), lambda i: (0, 0, i)),
        cost_estimate=cost(800000000, 4400000),
        name="pre",
    )(rows, weights)
    pre = exchange(pre, unit_groups)
    hidden = pl.pallas_call(
        gate_kernel,
        grid=(slots // step,),
        out_shape=whole((SIDE, 192, slots), BF),
        in_specs=[pl.BlockSpec((SIDE, 192, step), lambda i: (0, 0, i))],
        out_specs=pl.BlockSpec((SIDE, 192, step), lambda i: (0, 0, i)),
        cost_estimate=cost(3000000, 3200000),
        name="gates",
    )(pre)
    hidden = exchange(hidden, unit_groups)
    part = pl.pallas_call(
        partial_kernel,
        grid=(slots // step,),
        out_shape=whole((SIDE, slots, 128), BF),
        in_specs=[
            pl.BlockSpec((SIDE, 192, step), lambda i: (0, 0, i)),
            pl.BlockSpec((SIDE, 192, 512), lambda i: (0, 0, 0)),
        ],
        out_specs=pl.BlockSpec((SIDE, step, 128), lambda i: (0, i, 0)),
        cost_estimate=cost(540000000, 3400000),
        name="partial",
    )(hidden, weights)
    part = exchange(part, feature_groups)
    back = jnp.sum(part.astype(F32), axis=0).astype(BF).reshape(sp_count, SLOT, 128)
    returned = lax.all_to_all(back, SP, 0, 0, tiled=True).reshape(slots, 128)

    grads = pl.pallas_call(
        grads_kernel,
        grid=(SIDE,),
        out_shape=whole((SIDE, 192, 512), BF),
        in_specs=[
            pl.BlockSpec((SIDE, 192, slots), lambda i: (0, 0, 0)),
            pl.BlockSpec((1, slots, 256), lambda i: (i, 0, 0)),
        ],
        out_specs=pl.BlockSpec((SIDE, 192, 128), lambda i: (0, 0, i)),
        cost_estimate=cost(800000000, 4400000),
        name="grads",
    )(hidden, rows)

    spread = pl.pallas_call(
        combine_kernel,
        out_shape=whole((tp_count, tokens, 128), BF),
        in_specs=[vmem] * 3,
        out_specs=vmem,
        cost_estimate=cost(80000000, 2500000),
        name="combine",
    )(pick, returned, out_cotangent)
    full = lax.all_to_all(spread, TP, 0, 0, tiled=True)

    proj_part = pl.pallas_call(
        proj_kernel,
        out_shape=whole((sp_count, 32, 128), BF),
        in_specs=[vmem] * 4,
        out_specs=vmem,
        cost_estimate=cost(84000000, 1600000),
        name="proj_grad",
    )(full, conv_t, sums, gain)
    norm_cot, cot_sums = pl.pallas_call(
        norm_kernel,
        out_shape=(whole((64, tokens), F32), whole((2, tokens), F32)),
        in_specs=[vmem] * 5,
        out_specs=(vmem, vmem),
        cost_estimate=cost(84000000, 1600000),
        name="norm_cot",
    )(full, proj_weight, conv_t, sums, gain)
    proj_part = lax.all_to_all(proj_part, SP, 0, 0, tiled=True)
    grads = exchange(grads, unit_groups)

    cot_sums = lax.psum(lax.psum(cot_sums, "y"), "x")
    conv_cot, head = pl.pallas_call(
        head_kernel,
        out_shape=(whole((64, tokens), F32), whole((64, 128), F32)),
        in_specs=[vmem] * 4,
        out_specs=(vmem, vmem),
        cost_estimate=cost(1000000, 200000),
        name="conv_cot",
    )(norm_cot, cot_sums, conv_t, sums)
    behind = [(i + 1, i) for i in range(sp_count - 1)]
    after = lax.ppermute(head, SP, behind)
    value, gate = pl.pallas_call(
        conv_kernel,
        out_shape=(whole((64, tokens), BF), whole((64, tokens), BF)),
        in_specs=[vmem] * 5,
        out_specs=(vmem, vmem),
        scratch_shapes=[VM((64, 384), F32)],
        cost_estimate=cost(4000000, 400000),
        name="conv",
    )(conv_cot, after, taps_t, glu_gate.T, glu_value.T)

    total = jnp.sum(proj_part.astype(F32), axis=0)
    grad_proj = jnp.concatenate([total[:, 0:64], total[:, 64:128]], axis=0).T

    grad_gate, grad_up, grad_down = pl.pallas_call(
        merge_kernel,
        out_shape=(whole((64, 2048), F32),) * 3,
        in_specs=[smem, vmem],
        out_specs=(vmem,) * 3,
        cost_estimate=cost(1000000, 2400000),
        name="merge_grads",
    )(core, grads)
    return (
        grad_gate[None],
        grad_up[None],
        grad_down[None],
        grad_proj,
        value.T,
        gate.T,
    )


def solution(mesh):
    split = Mesh(mesh.devices.reshape(16, 2, SIDE, SIDE), ("z", "c", "y", "x"))
    placed = (
        P(SP, TP),
        P(SP, TP),
        P(SP, None),
        P(SP, None),
        P(SP, TP, None),
        P(SP, TP, None),
        P(SP, TP, None),
        P(SP, TP),
        P(SP, TP),
        P(SP, TP),
        P(None, TP),
        P(TP),
        P(TP, None),
    )
    return jax.shard_map(
        body,
        mesh=split,
        in_specs=placed,
        out_specs=(
            P(SP, TP, None),
            P(SP, TP, None),
            P(SP, TP, None),
            P(SP, TP),
            P(SP, TP),
            P(SP, TP),
        ),
        check_vma=False,
    )
```

time: 347 us -> 258 us (0.74)
  waiting for transfers between devices: 101 us -> 39.9 us
  Pallas kernels: 0 us -> 38.9 us
  matrix products: 21.1 us -> 0 us
  local copies, waits for them, and re-layouts: 21.2 us -> 2.95 us
  other arithmetic: 14.4 us -> 0.37 us
  between operations: 14.5 us -> 0.76 us
  blocking collectives: 142 us -> 130 us
  starting transfers between devices: 32.4 us -> 43.9 us
    all_gather x1 -> x0, waiting for transfers between devices: 80 us -> none  [sent_together_2(): lax.all_gather(both, axis, axis=dim, tiled=True)]
    pallas_call x0 -> x12, Pallas kernels: none -> 38.9 us  [the longest x1 5.65 us: body(): pl.pallas_call(pre_kernel, grid=(slots // step,), out_shape=whole((SIDE,...]
    dot_general x10 -> x0, matrix products: 20.6 us -> none  [the longest x4 11.6 us: contract_rows(): lax.dot_general(left, right, (((0,), (0,)), ((), ())), preferred_element_...]
    all_to_all x3 -> x5, waiting for transfers between devices: 21 us -> 39.7 us  [the longest x1 16.4 us: body(): lax.all_to_all(sent.reshape(sp_count, SLOT, 256), SP, 0, 0, tiled=True)]
    all_to_all x3 -> x5, starting transfers between devices: 27.2 us -> 38.9 us  [the longest x1 17.2 us: body(): lax.all_to_all(sent.reshape(sp_count, SLOT, 256), SP, 0, 0, tiled=True)]
    psum x4, blocking collectives: 40.4 us -> 32.9 us  [the longest x2 17 us: body(): sums = lax.psum(lax.psum(sums, 'y'), 'x')]
    unnamed x34 -> x16, local copies, waits for them, and re-layouts: 7.55 us -> 2.03 us
    scatter x1 -> x0, other arithmetic: 4.86 us -> none  [place_rows(): empty_rows.at[target].set(values)]
  transfers between devices with their start and end apart: 5 -> 6, of which waited for: 2 -> 5; matrix products, arithmetic and copies ran while one was open for 4% -> 1% of each run, Pallas kernels for 0% -> 8%
where the time goes in v1:
time: 258 us; the launch traced here: 257 us
  blocking collectives  130 us (50%)
  starting transfers between devices  43.9 us (17%)
  waiting for transfers between devices  39.9 us (15%)
  Pallas kernels  38.9 us (15%)
  local copies, waits for them, and re-layouts  2.95 us (1%)
    all_to_all x4, blocking collectives, exchange(): return lax.all_to_all(v, PLANE, 0, 0, axis_index_groups=groups, tiled=True)  66.7 us
    all_to_all x1, blocking collectives, body(): returned = lax.all_to_all(back, SP, 0, 0, tiled=True).reshape(slots, 128)  30.3 us
    all_to_all x1, starting transfers between devices, body(): lax.all_to_all(sent.reshape(sp_count, SLOT, 256), SP, 0, 0, tiled=True)  17.2 us
    psum x2, blocking collectives, body(): sums = lax.psum(lax.psum(sums, 'y'), 'x')  17 us
    all_to_all x1, waiting for transfers between devices, body(): lax.all_to_all(sent.reshape(sp_count, SLOT, 256), SP, 0, 0, tiled=True)  16.4 us
    psum x2, blocking collectives, body(): cot_sums = lax.psum(lax.psum(cot_sums, 'y'), 'x')  15.8 us
    all_to_all x1, waiting for transfers between devices, body(): full = lax.all_to_all(spread, TP, 0, 0, tiled=True)  13 us
    all_to_all x2, waiting for transfers between devices, exchange(): return lax.all_to_all(v, PLANE, 0, 0, axis_index_groups=groups, tiled=True)  10.3 us
  transfers between devices with their start and end apart: 6, of which 5 were waited for; matrix products, arithmetic and copies ran while one was open for 1% of the time, Pallas kernels for 8%

profile of v1, /device:TPU:1, one launch (start us, length us, event | category | flops | bytes accessed | tf_op | source)
XLA Modules:
  0.0 256.6 jit_solution(7532683217096725042)
XLA Ops:
  2.8 5.0 %all-to-all-start = ((bf16[4,192,512]{2,1,0:T(8,128)(2,1)}), bf16[4,192,512]{2,1,0:T(8,128)(2,1)S(1)}, u32[]{:S(2)}, u32[]{:S(2)}) async-start(bf16[4,192,512]{2,1,0:T(8,128)(2,1)} %split_weights.1), calls=%async_computation | async-start | bytes 1572864 | tf_op jit(solution)/shard_map/all_to_all | solution.py:40
  7.8 3.0 %route.1 = (bf16[1024,256]{1,0:T(8,128)(2,1)}, bf16[1024,320]{1,0:T(8,128)(2,1)}) custom-call(s32[2,320]{1,0:T(2,128)} %bitcast.43, f32[2,320]{1,0:T(2,128)} %bitcast.44, bf16[320,128]{1,0:T(8,128)(2,1)} %x_ref.1, bf16[320,128]{1,0:T(8,128)(2,1)} %c_ref.3), custom_call_target="tpu_custom_call" | custom-call | flops 400000000 | bytes 2000000 | tf_op jit(solution)/shard_map/route/pallas_call | solution.py:248
  10.8 5.4 %all-to-all-done.w_ref = bf16[4,192,512]{2,1,0:T(8,128)(2,1)S(1)} async-done(((bf16[4,192,512]{2,1,0:T(8,128)(2,1)}), bf16[4,192,512]{2,1,0:T(8,128)(2,1)S(1)}, u32[]{:S(2)}, u32[]{:S(2)}) %all-to-all-start) | async-done | bytes 786464 | tf_op jit(solution)/shard_map/all_to_all | solution.py:40
  16.1 17.2 %all-to-all-start.1 = ((bf16[32,32,256]{2,1,0:T(8,128)(2,1)}), bf16[32,32,256]{2,1,0:T(8,128)(2,1)S(1)}, u32[]{:S(2)}, u32[]{:S(2)}) async-start(bf16[32,32,256]{2,1,0:T(8,128)(2,1)} %bitcast.30), calls=%async_computation.1 | async-start | bytes 1048576 | tf_op jit(solution)/shard_map/all_to_all | solution.py:257
  33.4 9.0 %psum.28 = f32[2,320]{1,0:T(2,128)S(1)} all-reduce(f32[2,320]{1,0:T(2,128)S(1)} %pad_maximum_fusion), channel_id=1, replica_groups=mesh['z'=16,'c'=2,'y'=4,'x'=4] {'y'}, use_global_device_ids=true, to_apply=%region_2.0 | all-reduce | flops 640 | bytes 5120 | tf_op jit(solution)/shard_map/psum | solution.py:263
  42.4 8.0 %psum.29.sums_ref = f32[2,320]{1,0:T(2,128)} all-reduce(f32[2,320]{1,0:T(2,128)S(1)} %psum.28), channel_id=1, replica_groups=mesh['z'=16,'c'=2,'y'=4,'x'=4] {'x'}, use_global_device_ids=true, to_apply=%region_3.0 | all-reduce | flops 640 | bytes 5120 | tf_op jit(solution)/shard_map/psum | solution.py:263
  50.5 16.4 %all-to-all-done.1 = bf16[32,32,256]{2,1,0:T(8,128)(2,1)S(1)} async-done(((bf16[32,32,256]{2,1,0:T(8,128)(2,1)}), bf16[32,32,256]{2,1,0:T(8,128)(2,1)S(1)}, u32[]{:S(2)}, u32[]{:S(2)}) %all-to-all-start.1) | async-done | bytes 524320 | tf_op jit(solution)/shard_map/all_to_all | solution.py:257
  67.0 18.9 %all_to_all.50.a_ref = bf16[4,1024,256]{2,1,0:T(8,128)(2,1)} all-to-all(bf16[4,1024,256]{2,1,0:T(8,128)(2,1)S(1)} %broadcast_in_dim.15), channel_id=1, replica_groups={{0,4,8,12},{1,5,9,13},{2,6,10,14},{3,7,11,15},{16,17,18,19},{20,21,22,2..., dimensions={0} | all-to-all | bytes 4194304 | tf_op jit(solution)/shard_map/all_to_all | solution.py:40
  85.9 5.6 %pre.1 = bf16[4,192,1024]{2,1,0:T(8,128)(2,1)} custom-call(bf16[4,1024,256]{2,1,0:T(8,128)(2,1)} %all_to_all.50.a_ref, bf16[4,192,512]{2,1,0:T(8,128)(2,1)} %copy-done.1), custom_call_target="tpu_custom_call" | custom-call | flops 800000000 | bytes 4400000 | tf_op jit(solution)/shard_map/pre/pallas_call | solution.py:270
  91.5 17.2 %all_to_all.51.p_ref = bf16[4,192,1024]{2,1,0:T(8,128)(2,1)} all-to-all(bf16[4,192,1024]{2,1,0:T(8,128)(2,1)} %pre.1), channel_id=1, replica_groups={{0,1,2,3},{4,5,6,7},{8,9,10,11},{12,13,14,15},{16,20,24,28},{17,21,25,2..., dimensions={0} | all-to-all | bytes 3145728 | tf_op jit(solution)/shard_map/all_to_all | solution.py:40
  108.8 3.8 %gates.1 = bf16[4,192,1024]{2,1,0:T(8,128)(2,1)} custom-call(bf16[4,192,1024]{2,1,0:T(8,128)(2,1)} %all_to_all.51.p_ref), custom_call_target="tpu_custom_call" | custom-call | flops 3000000 | bytes 3200000 | tf_op jit(solution)/shard_map/gates/pallas_call | solution.py:283
  112.5 17.2 %all_to_all.52.h_ref = bf16[4,192,1024]{2,1,0:T(8,128)(2,1)} all-to-all(bf16[4,192,1024]{2,1,0:T(8,128)(2,1)} %gates.1), channel_id=1, replica_groups={{0,1,2,3},{4,5,6,7},{8,9,10,11},{12,13,14,15},{16,20,24,28},{17,21,25,2..., dimensions={0} | all-to-all | bytes 3145728 | tf_op jit(solution)/shard_map/all_to_all | solution.py:40
  129.8 4.4 %partial.1 = bf16[4,1024,128]{2,1,0:T(8,128)(2,1)} custom-call(bf16[4,192,1024]{2,1,0:T(8,128)(2,1)} %all_to_all.52.h_ref, bf16[4,192,512]{2,1,0:T(8,128)(2,1)} %copy-done.1), custom_call_target="tpu_custom_call" | custom-call | flops 540000000 | bytes 3400000 | tf_op jit(solution)/shard_map/partial/pallas_call | solution.py:293
  134.1 13.3 %all_to_all.53 = bf16[4,1024,128]{2,1,0:T(8,128)(2,1)S(1)} all-to-all(bf16[4,1024,128]{2,1,0:T(8,128)(2,1)} %partial.1), channel_id=1, replica_groups={{0,4,8,12},{1,5,9,13},{2,6,10,14},{3,7,11,15},{16,17,18,19},{20,21,22,2..., dimensions={0} | all-to-all | bytes 2097152 | tf_op jit(solution)/shard_map/all_to_all | solution.py:40
  147.7 30.3 %all_to_all.54 = bf16[32,32,128]{2,1,0:T(8,128)(2,1)} all-to-all(bf16[32,32,128]{2,1,0:T(8,128)(2,1)S(1)} %bitcast.26), channel_id=1, replica_groups=mesh['z'=16,'c'=2,'y'=4,'x'=4] {'z','c'}, dimensions={0} | all-to-all | bytes 524288 | tf_op jit(solution)/shard_map/all_to_all | solution.py:307
  180.7 3.7 %all-to-all-start.8 = ((bf16[16,320,128]{2,1,0:T(8,128)(2,1)}), bf16[16,320,128]{2,1,0:T(8,128)(2,1)S(1)}, u32[]{:S(2)}, u32[]{:S(2)}) async-start(bf16[16,320,128]{2,1,0:T(8,128)(2,1)} %combine.1), calls=%async_computation.8 | async-start | bytes 2621440 | tf_op jit(solution)/shard_map/all_to_all | solution.py:330
  184.4 5.2 %grads.1 = bf16[4,192,512]{2,1,0:T(8,128)(2,1)} custom-call(bf16[4,192,1024]{2,1,0:T(8,128)(2,1)} %all_to_all.52.h_ref, bf16[4,1024,256]{2,1,0:T(8,128)(2,1)} %all_to_all.50.a_ref), custom_call_target="tpu_custom_call" | custom-call | flops 800000000 | bytes 4400000 | tf_op jit(solution)/shard_map/grads/pallas_call | solution.py:309
  189.6 13.0 %all-to-all-done.8.f_ref = bf16[16,320,128]{2,1,0:T(8,128)(2,1)S(1)} async-done(((bf16[16,320,128]{2,1,0:T(8,128)(2,1)}), bf16[16,320,128]{2,1,0:T(8,128)(2,1)S(1)}, u32[]{:S(2)}, u32[]{:S(2)}) %all-to-all-start.8) | async-done | bytes 1310752 | tf_op jit(solution)/shard_map/all_to_all | solution.py:330
  202.7 3.5 %all-to-all-start.5 = ((bf16[4,192,512]{2,1,0:T(8,128)(2,1)}), bf16[4,192,512]{2,1,0:T(8,128)(2,1)S(1)}, u32[]{:S(2)}, u32[]{:S(2)}) async-start(bf16[4,192,512]{2,1,0:T(8,128)(2,1)} %grads.1), calls=%async_computation.5 | async-start | bytes 1572864 | tf_op jit(solution)/shard_map/all_to_all | solution.py:40
  209.5 5.0 %all-to-all-done.5.s_ref = bf16[4,192,512]{2,1,0:T(8,128)(2,1)S(1)} async-done(((bf16[4,192,512]{2,1,0:T(8,128)(2,1)}), bf16[4,192,512]{2,1,0:T(8,128)(2,1)S(1)}, u32[]{:S(2)}, u32[]{:S(2)}) %all-to-all-start.5) | async-done | bytes 786464 | tf_op jit(solution)/shard_map/all_to_all | solution.py:40
  214.5 9.5 %all-to-all-start.9 = ((bf16[32,32,128]{2,1,0:T(8,128)(2,1)}), bf16[32,32,128]{2,1,0:T(8,128)(2,1)S(1)}, u32[]{:S(2)}, u32[]{:S(2)}) async-start(bf16[32,32,128]{2,1,0:T(8,128)(2,1)} %proj_grad.1), calls=%async_computation.9 | async-start | bytes 524288 | tf_op jit(solution)/shard_map/all_to_all | solution.py:348
  226.7 7.9 %psum.30 = f32[2,320]{1,0:T(2,128)S(1)} all-reduce(f32[2,320]{1,0:T(2,128)} %get-tuple-element.31), channel_id=1, replica_groups=mesh['z'=16,'c'=2,'y'=4,'x'=4] {'y'}, use_global_device_ids=true, to_apply=%region_6.0 | all-reduce | flops 640 | bytes 5120 | tf_op jit(solution)/shard_map/psum | solution.py:351
  234.6 8.0 %psum.31.t_ref = f32[2,320]{1,0:T(2,128)} all-reduce(f32[2,320]{1,0:T(2,128)S(1)} %psum.30), channel_id=1, replica_groups=mesh['z'=16,'c'=2,'y'=4,'x'=4] {'x'}, use_global_device_ids=true, to_apply=%region_7.0 | all-reduce | flops 640 | bytes 5120 | tf_op jit(solution)/shard_map/psum | solution.py:351
  244.1 5.0 %collective-permute-start = (f32[64,128]{1,0:T(8,128)}, f32[64,128]{1,0:T(8,128)S(1)}, u32[]{:S(2)}, u32[]{:S(2)}) collective-permute-start(f32[64,128]{1,0:T(8,128)} %get-tuple-element.33), channel_id=1, source_target_pairs={{16,0},{32,16},{48,32},{64,48},{80,64},{96,80},{112,96},{128,112},... | collective-permute-start | bytes 98312 | tf_op jit(solution)/shard_map/ppermute | solution.py:361
  (35 shorter events, 20.4 us)
Async XLA Ops:
  2.8 13.3 %all-to-all-start = ((bf16[4,192,512]{2,1,0:T(8,128)(2,1)}), bf16[4,192,512]{2,1,0:T(8,128)(2,1)S(1)}, u32[]{:S(2)}, u32[]{:S(2)}) async-start(bf16[4,192,512]{2,1,0:T(8,128)(2,1)} %split_weights.1), calls=%async_computation | async-start | bytes 1572864 | tf_op jit(solution)/shard_map/all_to_all | solution.py:40
  7.8 25.5 %copy-start.3 = (bf16[320,64]{0,1:T(8,128)(2,1)S(1)}, bf16[320,64]{0,1:T(8,128)(2,1)}, u32[]{:S(2)}) copy-start(bf16[320,64]{0,1:T(8,128)(2,1)} %param.22) | copy-start | bytes 122884
  16.1 50.8 %copy-start.1 = (bf16[4,192,512]{2,1,0:T(8,128)(2,1)}, bf16[4,192,512]{2,1,0:T(8,128)(2,1)S(1)}, u32[]{:S(2)}) copy-start(bf16[4,192,512]{2,1,0:T(8,128)(2,1)S(1)} %all-to-all-done.w_ref) | copy-start | bytes 2359300
  16.1 50.7 %all-to-all-start.1 = ((bf16[32,32,256]{2,1,0:T(8,128)(2,1)}), bf16[32,32,256]{2,1,0:T(8,128)(2,1)S(1)}, u32[]{:S(2)}, u32[]{:S(2)}) async-start(bf16[32,32,256]{2,1,0:T(8,128)(2,1)} %bitcast.30), calls=%async_computation.1 | async-start | bytes 1048576 | tf_op jit(solution)/shard_map/all_to_all | solution.py:257
  180.7 22.0 %all-to-all-start.8 = ((bf16[16,320,128]{2,1,0:T(8,128)(2,1)}), bf16[16,320,128]{2,1,0:T(8,128)(2,1)S(1)}, u32[]{:S(2)}, u32[]{:S(2)}) async-start(bf16[16,320,128]{2,1,0:T(8,128)(2,1)} %combine.1), calls=%async_computation.8 | async-start | bytes 2621440 | tf_op jit(solution)/shard_map/all_to_all | solution.py:330
  189.6 16.6 %copy-start.6 = (f32[64]{0:T(128)S(1)}, f32[64]{0:T(128)}, u32[]{:S(2)}) copy-start(f32[64]{0:T(128)} %param.24) | copy-start | bytes 772
  202.7 4.2 %copy-start = (bf16[16,320,128]{2,1,0:T(8,128)(2,1)}, bf16[16,320,128]{2,1,0:T(8,128)(2,1)S(1)}, u32[]{:S(2)}) copy-start(bf16[16,320,128]{2,1,0:T(8,128)(2,1)S(1)} %all-to-all-done.8.f_ref) | copy-start | bytes 3932164
  202.7 11.8 %all-to-all-start.5 = ((bf16[4,192,512]{2,1,0:T(8,128)(2,1)}), bf16[4,192,512]{2,1,0:T(8,128)(2,1)S(1)}, u32[]{:S(2)}, u32[]{:S(2)}) async-start(bf16[4,192,512]{2,1,0:T(8,128)(2,1)} %grads.1), calls=%async_computation.5 | async-start | bytes 1572864 | tf_op jit(solution)/shard_map/all_to_all | solution.py:40
  209.5 39.6 %copy-start.5 = (f32[31,64]{1,0:T(8,128)S(1)}, f32[31,64]{1,0:T(8,128)}, u32[]{:S(2)}) copy-start(f32[31,64]{1,0:T(8,128)} %param.23) | copy-start | bytes 23812
  214.5 35.4 %copy-start.2 = (bf16[4,192,512]{2,1,0:T(8,128)(2,1)}, bf16[4,192,512]{2,1,0:T(8,128)(2,1)S(1)}, u32[]{:S(2)}) copy-start(bf16[4,192,512]{2,1,0:T(8,128)(2,1)S(1)} %all-to-all-done.5.s_ref) | copy-start | bytes 2359300
  214.5 41.3 %all-to-all-start.9 = ((bf16[32,32,128]{2,1,0:T(8,128)(2,1)}), bf16[32,32,128]{2,1,0:T(8,128)(2,1)S(1)}, u32[]{:S(2)}, u32[]{:S(2)}) async-start(bf16[32,32,128]{2,1,0:T(8,128)(2,1)} %proj_grad.1), calls=%async_computation.9 | async-start | bytes 524288 | tf_op jit(solution)/shard_map/all_to_all | solution.py:348
  244.1 8.2 %collective-permute-start = (f32[64,128]{1,0:T(8,128)}, f32[64,128]{1,0:T(8,128)S(1)}, u32[]{:S(2)}, u32[]{:S(2)}) collective-permute-start(f32[64,128]{1,0:T(8,128)} %get-tuple-element.33), channel_id=1, source_target_pairs={{16,0},{32,16},{48,32},{64,48},{80,64},{96,80},{112,96},{128,112},... | collective-permute-start | bytes 98312 | tf_op jit(solution)/shard_map/ppermute | solution.py:361
  252.3 0.6 copy-start.4

commit v2 on v1

--- a/solution.py
+++ b/solution.py
@@ -1,5 +1,6 @@
 import jax
 import jax.numpy as jnp
+import numpy as np
 from jax import lax
 from jax.experimental import pallas as pl
 from jax.experimental.pallas import tpu as pltpu
@@ -12,6 +13,7 @@
 PLANE = ("c", "y", "x")
 SIDE = 4
 SLOT = 32
+ROOM = 24 << 20
 BF = jnp.bfloat16
 F32 = jnp.float32
 VM = pltpu.VMEM
@@ -32,6 +34,32 @@
     return down[0] + across[1], across[0] + down[1]
 
 
+def step_tables():
+    features, units = plane_groups()
+    of_features = {p: g for g in features for p in g}
+    table = np.zeros((2 * SIDE * SIDE, 64), np.int32)
+    for group in units:
+        for me, p in enumerate(group):
+            table[p, 0] = me
+            for k in range(SIDE):
+                ahead = of_features[group[(me + k) % SIDE]]
+                back = of_features[group[(me - k) % SIDE]]
+                for a in range(SIDE):
+                    table[p, 16 + k * SIDE + a] = ahead[a] % (SIDE * SIDE)
+                    table[p, 32 + k * SIDE + a] = back[a] % (SIDE * SIDE)
+    return table
+
+
+def steps_ahead(groups, k):
+    return [(g[i], g[(i + k) % SIDE]) for g in groups for i in range(SIDE)]
+
+
+def pass_on(parts, groups):
+    return (parts[0],) + tuple(
+        lax.ppermute(parts[k], PLANE, steps_ahead(groups, k)) for k in range(1, SIDE)
+    )
+
+
 def mm(a, b, dims):
     return lax.dot_general(a, b, dims, preferred_element_type=F32)
 
@@ -44,7 +72,7 @@
     return pl.CostEstimate(flops=flops, bytes_accessed=nbytes, transcendentals=0)
 
 
-def route_kernel(rt_ref, w_ref, x_ref, c_ref, s_ref, p_ref):
+def route_kernel(rt_ref, w_ref, x_ref, c_ref, s_ref, t_ref):
     tokens = rt_ref.shape[1]
     experts = s_ref.shape[0] // SLOT
     first, second = rt_ref[0:1, :], rt_ref[1:2, :]
@@ -59,6 +87,8 @@
     rank1 = jnp.sum(jnp.where(o1, earlier, 0.0), axis=0, keepdims=True)
     t0 = first * SLOT + rank0.astype(jnp.int32)
     t1 = second * SLOT + rank1.astype(jnp.int32)
+    t_ref[0:1, :] = t0
+    t_ref[1:2, :] = t1
     w0, w1 = w_ref[0:1, :], w_ref[1:2, :]
     x, c = x_ref[...], c_ref[...]
     size = 128
@@ -70,39 +100,51 @@
             jnp.where(m0, w0, 0.0) + jnp.where(m1, w1, 0.0), axis=1, keepdims=True
         )
         rows = pl.ds(k * size, size)
-        p_ref[rows, :] = pick
         s_ref[rows, 0:128] = mm(pick, x, NN).astype(BF)
         s_ref[rows, 128:256] = (weight * mm(pick, c, NN)).astype(BF)
 
 
-def split_kernel(core_ref, g_ref, u_ref, d_ref, o_ref):
-    core = core_ref[0]
-    for b in range(SIDE):
+def pick_kernel(t_ref, p_ref):
+    slots = lax.broadcasted_iota(jnp.int32, p_ref.shape, 0)
+    held = (slots == t_ref[0:1, :]) | (slots == t_ref[1:2, :])
+    p_ref[...] = jnp.where(held, 1.0, 0.0).astype(BF)
+
+
+def split_kernel(at_ref, g_ref, u_ref, d_ref, *outs):
+    for k, out in enumerate(outs):
         for a in range(SIDE):
-            at = jnp.where(core == 0, a * SIDE + b, b * SIDE + a)
+            at = at_ref[16 + k * SIDE + a]
             cols = pl.ds(pl.multiple_of(at * 128, 128), 128)
             for q, ref in enumerate((g_ref, u_ref, d_ref)):
-                o_ref[b, q * 64 : q * 64 + 64, a * 128 : a * 128 + 128] = ref[:, cols]
-
-
-def merge_kernel(core_ref, s_ref, g_ref, u_ref, d_ref):
-    core = core_ref[0]
-    for b in range(SIDE):
+                out[q * 64 : q * 64 + 64, a * 128 : a * 128 + 128] = ref[:, cols]
+
+
+def merge_kernel(at_ref, s0, s1, s2, s3, g_ref, u_ref, d_ref):
+    for k, s_ref in enumerate((s0, s1, s2, s3)):
         for a in range(SIDE):
-            at = jnp.where(core == 0, a * SIDE + b, b * SIDE + a)
+            at = at_ref[32 + k * SIDE + a]
             cols = pl.ds(pl.multiple_of(at * 128, 128), 128)
             for q, ref in enumerate((g_ref, u_ref, d_ref)):
                 ref[:, cols] = s_ref[
-                    b, q * 64 : q * 64 + 64, a * 128 : a * 128 + 128
+                    q * 64 : q * 64 + 64, a * 128 : a * 128 + 128
                 ].astype(F32)
 
 
-def pre_kernel(a_ref, w_ref, o_ref):
+def behind_of(at_ref, k):
+    return lax.rem(at_ref[0] + (SIDE - k), SIDE)
+
+
+def ahead_of(at_ref, k):
+    return lax.rem(at_ref[0] + k, SIDE)
+
+
+def pre_kernel(at_ref, a_ref, w0, w1, w2, w3, o_ref):
     x = jnp.concatenate([a_ref[i, :, 0:128] for i in range(SIDE)], axis=1)
     c = jnp.concatenate([a_ref[i, :, 128:256] for i in range(SIDE)], axis=1)
-    for b in range(SIDE):
-        o_ref[b, 0:128, :] = mm(w_ref[b, 0:128, :], x, NT).astype(BF)
-        o_ref[b, 128:192, :] = mm(w_ref[b, 128:192, :], c, NT).astype(BF)
+    for k, w_ref in enumerate((w0, w1, w2, w3)):
+        b = behind_of(at_ref, k)
+        o_ref[b, 0:128, :] = mm(w_ref[0:128, :], x, NT).astype(BF)
+        o_ref[b, 128:192, :] = mm(w_ref[128:192, :], c, NT).astype(BF)
 
 
 def gate_kernel(p_ref, o_ref):
@@ -121,19 +163,21 @@
         o_ref[b, 128:192, :] = hidden
 
 
-def partial_kernel(h_ref, w_ref, o_ref):
-    h = jnp.concatenate([h_ref[b, 0:128, :] for b in range(SIDE)], axis=0)
-    w = jnp.concatenate([w_ref[b, 0:128, :] for b in range(SIDE)], axis=0)
+def partial_kernel(at_ref, h_ref, w0, w1, w2, w3, o_ref):
+    ws = (w0, w1, w2, w3)
+    h = jnp.concatenate([h_ref[behind_of(at_ref, k), 0:128, :] for k in range(SIDE)], axis=0)
+    w = jnp.concatenate([w_ref[0:128, :] for w_ref in ws], axis=0)
     total = mm(h, w, TN)
     for a in range(SIDE):
         o_ref[a] = total[:, a * 128 : a * 128 + 128].astype(BF)
 
 
-def grads_kernel(h_ref, a_ref, o_ref):
+def grads_kernel(at_ref, h_ref, a_ref, *outs):
     x, c = a_ref[0, :, 0:128], a_ref[0, :, 128:256]
-    for b in range(SIDE):
-        o_ref[b, 0:128, :] = mm(h_ref[b, 0:128, :], x, NN).astype(BF)
-        o_ref[b, 128:192, :] = mm(h_ref[b, 128:192, :], c, NN).astype(BF)
+    for k, out in enumerate(outs):
+        b = ahead_of(at_ref, k)
+        out[0:128, :] = mm(h_ref[b, 0:128, :], x, NN).astype(BF)
+        out[128:192, :] = mm(h_ref[b, 128:192, :], c, NN).astype(BF)
 
 
 def combine_kernel(p_ref, r_ref, c_ref, o_ref):
@@ -231,29 +275,42 @@
     tokens = moe_input.shape[0]
     slots = sp_count * SLOT
     feature_groups, unit_groups = plane_groups()
-    core = lax.axis_index("c").reshape(1).astype(jnp.int32)
     smem = pl.BlockSpec(memory_space=pltpu.SMEM)
     vmem = pl.BlockSpec(memory_space=VM)
-
-    split = pl.pallas_call(
-        split_kernel,
-        out_shape=whole((SIDE, 192, 512), BF),
-        in_specs=[smem, vmem, vmem, vmem],
-        out_specs=vmem,
-        cost_estimate=cost(1000000, 1600000),
-        name="split_weights",
-    )(core, gate_weight[0], up_weight[0], down_weight[0])
-    weights = exchange(split, unit_groups)
-
-    sent, pick = pl.pallas_call(
+    room = pltpu.CompilerParams(vmem_limit_bytes=ROOM)
+
+    sent, target = pl.pallas_call(
         route_kernel,
-        out_shape=(whole((slots, 256), BF), whole((slots, tokens), BF)),
+        out_shape=(whole((slots, 256), BF), whole((2, tokens), jnp.int32)),
         in_specs=[vmem] * 4,
         out_specs=(vmem, vmem),
         cost_estimate=cost(400000000, 2000000),
         name="route",
     )(routes.T, route_weight.T, moe_input, out_cotangent)
-    weights, sent = lax.optimization_barrier((weights, sent))
+    sent, target, table, gate_weight, conv_result = lax.optimization_barrier(
+        (sent, target, jnp.asarray(step_tables()), gate_weight, conv_result)
+    )
+    at = table[lax.axis_index(PLANE)]
+    pick = pl.pallas_call(
+        pick_kernel,
+        out_shape=whole((slots, tokens), BF),
+        in_specs=[vmem],
+        out_specs=vmem,
+        compiler_params=room,
+        cost_estimate=cost(1000000, 700000),
+        name="pick",
+    )(target)
+    split = pl.pallas_call(
+        split_kernel,
+        out_shape=(whole((192, 512), BF),) * SIDE,
+        in_specs=[smem, vmem, vmem, vmem],
+        out_specs=(vmem,) * SIDE,
+        compiler_params=room,
+        cost_estimate=cost(1000000, 1600000),
+        name="split_weights",
+    )(at, gate_weight[0], up_weight[0], down_weight[0])
+    weights = pass_on(split, unit_groups)
+
     got = lax.all_to_all(sent.reshape(sp_count, SLOT, 256), SP, 0, 0, tiled=True)
     got = got.reshape(slots, 256)
 
@@ -261,7 +318,7 @@
     conv_f = conv_t.astype(F32)
     sums = jnp.stack([jnp.sum(conv_f, axis=0), jnp.sum(conv_f * conv_f, axis=0)])
     sums = lax.psum(lax.psum(sums, "y"), "x")
-    got, sums = lax.optimization_barrier((got, sums))
+    got, sums, weights = lax.optimization_barrier((got, sums, weights))
     gain = norm_gain.reshape(-1, 1)
     taps_t = conv_taps.T
 
@@ -271,14 +328,13 @@
         pre_kernel,
         grid=(slots // step,),
         out_shape=whole((SIDE, 192, slots), BF),
-        in_specs=[
-            pl.BlockSpec((SIDE, step, 256), lambda i: (0, i, 0)),
-            pl.BlockSpec((SIDE, 192, 512), lambda i: (0, 0, 0)),
-        ],
+        in_specs=[smem, pl.BlockSpec((SIDE, step, 256), lambda i: (0, i, 0))]
+        + [pl.BlockSpec((192, 512), lambda i: (0, 0))] * SIDE,
         out_specs=pl.BlockSpec((SIDE, 192, step), lambda i: (0, 0, i)),
+        compiler_params=room,
         cost_estimate=cost(800000000, 4400000),
         name="pre",
-    )(rows, weights)
+    )(at, rows, *weights)
     pre = exchange(pre, unit_groups)
     hidden = pl.pallas_call(
         gate_kernel,
@@ -286,6 +342,7 @@
         out_shape=whole((SIDE, 192, slots), BF),
         in_specs=[pl.BlockSpec((SIDE, 192, step), lambda i: (0, 0, i))],
         out_specs=pl.BlockSpec((SIDE, 192, step), lambda i: (0, 0, i)),
+        compiler_params=room,
         cost_estimate=cost(3000000, 3200000),
         name="gates",
     )(pre)
@@ -294,14 +351,13 @@
         partial_kernel,
         grid=(slots // step,),
         out_shape=whole((SIDE, slots, 128), BF),
-        in_specs=[
-            pl.BlockSpec((SIDE, 192, step), lambda i: (0, 0, i)),
-            pl.BlockSpec((SIDE, 192, 512), lambda i: (0, 0, 0)),
-        ],
+        in_specs=[smem, pl.BlockSpec((SIDE, 192, step), lambda i: (0, 0, i))]
+        + [pl.BlockSpec((192, 512), lambda i: (0, 0))] * SIDE,
         out_specs=pl.BlockSpec((SIDE, step, 128), lambda i: (0, i, 0)),
+        compiler_params=room,
         cost_estimate=cost(540000000, 3400000),
         name="partial",
-    )(hidden, weights)
+    )(at, hidden, *weights)
     part = exchange(part, feature_groups)
     back = jnp.sum(part.astype(F32), axis=0).astype(BF).reshape(sp_count, SLOT, 128)
     returned = lax.all_to_all(back, SP, 0, 0, tiled=True).reshape(slots, 128)
@@ -309,21 +365,26 @@
     grads = pl.pallas_call(
         grads_kernel,
         grid=(SIDE,),
-        out_shape=whole((SIDE, 192, 512), BF),
+        out_shape=(whole((192, 512), BF),) * SIDE,
         in_specs=[
+            smem,
             pl.BlockSpec((SIDE, 192, slots), lambda i: (0, 0, 0)),
             pl.BlockSpec((1, slots, 256), lambda i: (i, 0, 0)),
         ],
-        out_specs=pl.BlockSpec((SIDE, 192, 128), lambda i: (0, 0, i)),
+        out_specs=(pl.BlockSpec((192, 128), lambda i: (0, i)),) * SIDE,
+        compiler_params=room,
         cost_estimate=cost(800000000, 4400000),
         name="grads",
-    )(hidden, rows)
+    )(at, hidden, rows)
+    grads = pass_on(grads, unit_groups)
+    returned, grads = lax.optimization_barrier((returned, grads))
 
     spread = pl.pallas_call(
         combine_kernel,
         out_shape=whole((tp_count, tokens, 128), BF),
         in_specs=[vmem] * 3,
         out_specs=vmem,
+        compiler_params=room,
         cost_estimate=cost(80000000, 2500000),
         name="combine",
     )(pick, returned, out_cotangent)
@@ -334,6 +395,7 @@
         out_shape=whole((sp_count, 32, 128), BF),
         in_specs=[vmem] * 4,
         out_specs=vmem,
+        compiler_params=room,
         cost_estimate=cost(84000000, 1600000),
         name="proj_grad",
     )(full, conv_t, sums, gain)
@@ -342,18 +404,18 @@
         out_shape=(whole((64, tokens), F32), whole((2, tokens), F32)),
         in_specs=[vmem] * 5,
         out_specs=(vmem, vmem),
+        compiler_params=room,
         cost_estimate=cost(84000000, 1600000),
         name="norm_cot",
     )(full, proj_weight, conv_t, sums, gain)
     proj_part = lax.all_to_all(proj_part, SP, 0, 0, tiled=True)
-    grads = exchange(grads, unit_groups)
-
     cot_sums = lax.psum(lax.psum(cot_sums, "y"), "x")
     conv_cot, head = pl.pallas_call(
         head_kernel,
         out_shape=(whole((64, tokens), F32), whole((64, 128), F32)),
         in_specs=[vmem] * 4,
         out_specs=(vmem, vmem),
+        compiler_params=room,
         cost_estimate=cost(1000000, 200000),
         name="conv_cot",
     )(norm_cot, cot_sums, conv_t, sums)
@@ -365,6 +427,7 @@
         in_specs=[vmem] * 5,
         out_specs=(vmem, vmem),
         scratch_shapes=[VM((64, 384), F32)],
+        compiler_params=room,
         cost_estimate=cost(4000000, 400000),
         name="conv",
     )(conv_cot, after, taps_t, glu_gate.T, glu_value.T)
@@ -375,11 +438,12 @@
     grad_gate, grad_up, grad_down = pl.pallas_call(
         merge_kernel,
         out_shape=(whole((64, 2048), F32),) * 3,
-        in_specs=[smem, vmem],
+        in_specs=[smem] + [vmem] * SIDE,
         out_specs=(vmem,) * 3,
+        compiler_params=room,
         cost_estimate=cost(1000000, 2400000),
         name="merge_grads",
-    )(core, grads)
+    )(at, *grads)
     return (
         grad_gate[None],
         grad_up[None],

time: 258 us -> 221 us (0.86)
  blocking collectives: 130 us -> 93.6 us
  starting transfers between devices: 43.9 us -> 65 us
  Pallas kernels: 38.9 us -> 21 us
  waiting for transfers between devices: 39.9 us -> 35.5 us
    all_to_all x1 -> x0, blocking collectives: 30.3 us -> none  [body(): returned = lax.all_to_all(back, SP, 0, 0, tiled=True).reshape(slots, 128)]
    ppermute x0 -> x6, starting transfers between devices: none -> 19.1 us  [pass_on(): lax.ppermute(parts[k], PLANE, steps_ahead(groups, k))]
    all_to_all x1, waiting for transfers between devices: 16.4 us -> 5.19 us  [body(): lax.all_to_all(sent.reshape(sp_count, SLOT, 256), SP, 0, 0, tiled=True)]
    all_to_all x1, waiting for transfers between devices: 13 us -> 20 us  [body(): full = lax.all_to_all(spread, TP, 0, 0, tiled=True)]
    all_to_all x2 -> x1, waiting for transfers between devices: 10.3 us -> 5.25 us  [body(): returned = lax.all_to_all(back, SP, 0, 0, tiled=True).reshape(slots, 128)]
    ppermute x0 -> x6, waiting for transfers between devices: none -> 3.94 us  [pass_on(): lax.ppermute(parts[k], PLANE, steps_ahead(groups, k))]
    pallas_call x3 -> x4, Pallas kernels: 10.4 us -> 6.83 us  [the longest x1 2.97 us: body(): pl.pallas_call(grads_kernel, grid=(SIDE,), out_shape=(whole((192, 512), B...]
    all_to_all x2 -> x1, starting transfers between devices: 8.49 us -> 11.7 us  [body(): returned = lax.all_to_all(back, SP, 0, 0, tiled=True).reshape(slots, 128)]
  transfers between devices with their start and end apart: 6 -> 11, of which waited for: 5 -> 6; matrix products, arithmetic and copies ran while one was open for 1% -> 0% of each run, Pallas kernels for 8% -> 4%
where the time goes in v2:
time: 221 us; the launch traced here: 220 us
  blocking collectives  93.6 us (42%)
  starting transfers between devices  65 us (29%)
  waiting for transfers between devices  35.5 us (16%)
  Pallas kernels  21 us (10%)
  local copies, waits for them, and re-layouts  3.25 us (1%)
    all_to_all x4, blocking collectives, exchange(): return lax.all_to_all(v, PLANE, 0, 0, axis_index_groups=groups, tiled=True)  63.6 us
    all_to_all x1, waiting for transfers between devices, body(): full = lax.all_to_all(spread, TP, 0, 0, tiled=True)  20 us
    ppermute x6, starting transfers between devices, pass_on(): lax.ppermute(parts[k], PLANE, steps_ahead(groups, k))  19.1 us
    all_to_all x1, starting transfers between devices, body(): lax.all_to_all(sent.reshape(sp_count, SLOT, 256), SP, 0, 0, tiled=True)  16.7 us
    psum x2, blocking collectives, body(): sums = lax.psum(lax.psum(sums, 'y'), 'x')  16 us
    psum x2, blocking collectives, body(): cot_sums = lax.psum(lax.psum(cot_sums, 'y'), 'x')  14 us
    all_to_all x1, starting transfers between devices, body(): returned = lax.all_to_all(back, SP, 0, 0, tiled=True).reshape(slots, 128)  11.7 us
    all_to_all x1, starting transfers between devices, body(): proj_part = lax.all_to_all(proj_part, SP, 0, 0, tiled=True)  8.61 us
  transfers between devices with their start and end apart: 11, of which 6 were waited for; matrix products, arithmetic and copies ran while one was open for 0% of the time, Pallas kernels for 4%

profile of v2, /device:TPU:1, one launch (start us, length us, event | category | flops | bytes accessed | tf_op | source)
XLA Modules:
  0.0 220.3 jit_solution(4967264914344302546)
XLA Ops:
  0.7 2.9 %route.1 = (bf16[1024,256]{1,0:T(8,128)(2,1)}, s32[2,320]{1,0:T(2,128)}) custom-call(s32[2,320]{1,0:T(2,128)} %bitcast.43, f32[2,320]{1,0:T(2,128)} %bitcast.44, bf16[320,128]{1,0:T(8,128)(2,1)} %x_ref.1, bf16[320,128]{1,0:T(8,128)(2,1)} %c_ref.3), custom_call_target="tpu_custom_call" | custom-call | flops 400000000 | bytes 2000000 | tf_op jit(solution)/shard_map/route/pallas_call | solution.py:282
  3.6 16.7 %all-to-all-start = ((bf16[32,32,256]{2,1,0:T(8,128)(2,1)}), bf16[32,32,256]{2,1,0:T(8,128)(2,1)S(1)}, u32[]{:S(2)}, u32[]{:S(2)}) async-start(bf16[32,32,256]{2,1,0:T(8,128)(2,1)} %bitcast.36), calls=%async_computation | async-start | bytes 1048576 | tf_op jit(solution)/shard_map/all_to_all | solution.py:314
  21.8 3.2 %collective-permute-start = (bf16[192,512]{1,0:T(8,128)(2,1)S(1)}, bf16[192,512]{1,0:T(8,128)(2,1)S(1)}, u32[]{:S(2)}, u32[]{:S(2)}) collective-permute-start(bf16[192,512]{1,0:T(8,128)(2,1)S(1)} %get-tuple-element.48), channel_id=1, source_target_pairs={{0,1},{1,2},{2,3},{3,0},{4,5},{5,6},{6,7},{7,4},{8,9},{9,10},{10,1... | collective-permute-start | bytes 589832 | tf_op jit(solution)/shard_map/ppermute | solution.py:59
  25.0 4.5 %collective-permute-start.1 = (bf16[192,512]{1,0:T(8,128)(2,1)S(1)}, bf16[192,512]{1,0:T(8,128)(2,1)S(1)}, u32[]{:S(2)}, u32[]{:S(2)}) collective-permute-start(bf16[192,512]{1,0:T(8,128)(2,1)S(1)} %get-tuple-element.49), channel_id=1, source_target_pairs={{0,2},{1,3},{2,0},{3,1},{4,6},{5,7},{6,4},{7,5},{8,10},{9,11},{10,... | collective-permute-start | bytes 589832 | tf_op jit(solution)/shard_map/ppermute | solution.py:59
  29.5 3.0 %collective-permute-start.2 = (bf16[192,512]{1,0:T(8,128)(2,1)S(1)}, bf16[192,512]{1,0:T(8,128)(2,1)S(1)}, u32[]{:S(2)}, u32[]{:S(2)}) collective-permute-start(bf16[192,512]{1,0:T(8,128)(2,1)S(1)} %get-tuple-element.50), channel_id=1, source_target_pairs={{0,3},{1,0},{2,1},{3,2},{4,7},{5,4},{6,5},{7,6},{8,11},{9,8},{10,9... | collective-permute-start | bytes 589832 | tf_op jit(solution)/shard_map/ppermute | solution.py:59
  32.6 7.3 %psum.28 = f32[2,320]{1,0:T(2,128)S(1)} all-reduce(f32[2,320]{1,0:T(2,128)S(1)} %pad_maximum_fusion), channel_id=1, replica_groups=mesh['z'=16,'c'=2,'y'=4,'x'=4] {'y'}, use_global_device_ids=true, to_apply=%region_2.0 | all-reduce | flops 640 | bytes 5120 | tf_op jit(solution)/shard_map/psum | solution.py:320
  39.9 8.7 %psum.29.sums_ref = f32[2,320]{1,0:T(2,128)S(1)} all-reduce(f32[2,320]{1,0:T(2,128)S(1)} %psum.28), channel_id=1, replica_groups=mesh['z'=16,'c'=2,'y'=4,'x'=4] {'x'}, use_global_device_ids=true, to_apply=%region_3.0 | all-reduce | flops 640 | bytes 5120 | tf_op jit(solution)/shard_map/psum | solution.py:320
  48.6 5.2 %all-to-all-done = bf16[32,32,256]{2,1,0:T(8,128)(2,1)S(1)} async-done(((bf16[32,32,256]{2,1,0:T(8,128)(2,1)}), bf16[32,32,256]{2,1,0:T(8,128)(2,1)S(1)}, u32[]{:S(2)}, u32[]{:S(2)}) %all-to-all-start) | async-done | bytes 524320 | tf_op jit(solution)/shard_map/all_to_all | solution.py:314
  54.0 19.5 %all_to_all.40.a_ref = bf16[4,1024,256]{2,1,0:T(8,128)(2,1)S(1)} all-to-all(bf16[4,1024,256]{2,1,0:T(8,128)(2,1)S(1)} %broadcast_in_dim.15), channel_id=1, replica_groups={{0,4,8,12},{1,5,9,13},{2,6,10,14},{3,7,11,15},{16,17,18,19},{20,21,22,2..., dimensions={0} | all-to-all | bytes 4194304 | tf_op jit(solution)/shard_map/all_to_all | solution.py:68
  73.4 4.0 %pre.1 = bf16[4,192,1024]{2,1,0:T(8,128)(2,1)S(1)} custom-call(s32[64]{0:T(128)S(1)} %dynamic-slice_bitcast_fusion.at_ref, bf16[4,1024,256]{2,1,0:T(8,128)(2,1)S(1)} %all_to_all.40.a_ref, bf16[192,512]{1,0:T(8,128)(2,1)S(1)} %get-tuple-element.52.w0, bf16[192,512]{1,0:T(8,128)(2,1)S(1)} %collective-permute-done.w1, ...), custom_call_target="tpu_custom_call" | custom-call | flops 800000000 | bytes 4400000 | tf_op jit(solution)/shard_map/pre/pallas_call | solution.py:327
  77.5 16.4 %all_to_all.41.p_ref = bf16[4,192,1024]{2,1,0:T(8,128)(2,1)S(1)} all-to-all(bf16[4,192,1024]{2,1,0:T(8,128)(2,1)S(1)} %pre.1), channel_id=1, replica_groups={{0,1,2,3},{4,5,6,7},{8,9,10,11},{12,13,14,15},{16,20,24,28},{17,21,25,2..., dimensions={0} | all-to-all | bytes 3145728 | tf_op jit(solution)/shard_map/all_to_all | solution.py:68
  94.7 15.3 %all_to_all.42.h_ref = bf16[4,192,1024]{2,1,0:T(8,128)(2,1)S(1)} all-to-all(bf16[4,192,1024]{2,1,0:T(8,128)(2,1)S(1)} %gates.1), channel_id=1, replica_groups={{0,1,2,3},{4,5,6,7},{8,9,10,11},{12,13,14,15},{16,20,24,28},{17,21,25,2..., dimensions={0} | all-to-all | bytes 3145728 | tf_op jit(solution)/shard_map/all_to_all | solution.py:68
  112.1 12.5 %all_to_all.43 = bf16[4,1024,128]{2,1,0:T(8,128)(2,1)S(1)} all-to-all(bf16[4,1024,128]{2,1,0:T(8,128)(2,1)S(1)} %partial.1), channel_id=1, replica_groups={{0,4,8,12},{1,5,9,13},{2,6,10,14},{3,7,11,15},{16,17,18,19},{20,21,22,2..., dimensions={0} | all-to-all | bytes 2097152 | tf_op jit(solution)/shard_map/all_to_all | solution.py:68
  125.5 11.7 %all-to-all-start.5 = ((bf16[32,32,128]{2,1,0:T(8,128)(2,1)}), bf16[32,32,128]{2,1,0:T(8,128)(2,1)S(1)}, u32[]{:S(2)}, u32[]{:S(2)}) async-start(bf16[32,32,128]{2,1,0:T(8,128)(2,1)} %bitcast.9), calls=%async_computation.5 | async-start | bytes 524288 | tf_op jit(solution)/shard_map/all_to_all | solution.py:363
  138.7 3.0 %grads.1 = (bf16[192,512]{1,0:T(8,128)(2,1)S(1)}, bf16[192,512]{1,0:T(8,128)(2,1)S(1)}, bf16[192,512]{1,0:T(8,128)(2,1)S(1)}, bf16[192,512]{1,0:T(8,128)(2,1)S(1)}) custom-call(s32[64]{0:T(128)S(1)} %dynamic-slice_bitcast_fusion.at_ref, bf16[4,192,1024]{2,1,0:T(8,128)(2,1)S(1)} %copy-done.1, bf16[4,1024,256]{2,1,0:T(8,128)(2,1)S(1)} %all_to_all.40.a_ref), custom_call_target="tpu_custom_call" | custom-call | flops 800000000 | bytes 4400000 | tf_op jit(solution)/shard_map/grads/pallas_call | solution.py:365
  143.9 3.7 %collective-permute-start.4 = (bf16[192,512]{1,0:T(8,128)(2,1)S(1)}, bf16[192,512]{1,0:T(8,128)(2,1)S(1)}, u32[]{:S(2)}, u32[]{:S(2)}) collective-permute-start(bf16[192,512]{1,0:T(8,128)(2,1)S(1)} %get-tuple-element.58), channel_id=1, source_target_pairs={{0,2},{1,3},{2,0},{3,1},{4,6},{5,7},{6,4},{7,5},{8,10},{9,11},{10,... | collective-permute-start | bytes 589832 | tf_op jit(solution)/shard_map/ppermute | solution.py:59
  147.5 2.5 %collective-permute-start.5 = (bf16[192,512]{1,0:T(8,128)(2,1)S(1)}, bf16[192,512]{1,0:T(8,128)(2,1)S(1)}, u32[]{:S(2)}, u32[]{:S(2)}) collective-permute-start(bf16[192,512]{1,0:T(8,128)(2,1)S(1)} %get-tuple-element.59), channel_id=1, source_target_pairs={{0,3},{1,0},{2,1},{3,2},{4,7},{5,4},{6,5},{7,6},{8,11},{9,8},{10,9... | collective-permute-start | bytes 589832 | tf_op jit(solution)/shard_map/ppermute | solution.py:59
  154.3 5.3 %all-to-all-done.5 = bf16[32,32,128]{2,1,0:T(8,128)(2,1)S(1)} async-done(((bf16[32,32,128]{2,1,0:T(8,128)(2,1)}), bf16[32,32,128]{2,1,0:T(8,128)(2,1)S(1)}, u32[]{:S(2)}, u32[]{:S(2)}) %all-to-all-start.5) | async-done | bytes 262176 | tf_op jit(solution)/shard_map/all_to_all | solution.py:363
  161.0 3.8 %all-to-all-start.6 = ((bf16[16,320,128]{2,1,0:T(8,128)(2,1)}), bf16[16,320,128]{2,1,0:T(8,128)(2,1)S(1)}, u32[]{:S(2)}, u32[]{:S(2)}) async-start(bf16[16,320,128]{2,1,0:T(8,128)(2,1)} %combine.1), calls=%async_computation.6 | async-start | bytes 2621440 | tf_op jit(solution)/shard_map/all_to_all | solution.py:391
  165.0 20.0 %all-to-all-done.6.f_ref = bf16[16,320,128]{2,1,0:T(8,128)(2,1)S(1)} async-done(((bf16[16,320,128]{2,1,0:T(8,128)(2,1)}), bf16[16,320,128]{2,1,0:T(8,128)(2,1)S(1)}, u32[]{:S(2)}, u32[]{:S(2)}) %all-to-all-start.6) | async-done | bytes 1310752 | tf_op jit(solution)/shard_map/all_to_all | solution.py:391
  186.3 8.6 %all-to-all-start.7 = ((bf16[32,32,128]{2,1,0:T(8,128)(2,1)}), bf16[32,32,128]{2,1,0:T(8,128)(2,1)S(1)}, u32[]{:S(2)}, u32[]{:S(2)}) async-start(bf16[32,32,128]{2,1,0:T(8,128)(2,1)} %proj_grad.1), calls=%async_computation.7 | async-start | bytes 524288 | tf_op jit(solution)/shard_map/all_to_all | solution.py:411
  195.5 6.6 %psum.30 = f32[2,320]{1,0:T(2,128)S(1)} all-reduce(f32[2,320]{1,0:T(2,128)S(1)} %get-tuple-element.71), channel_id=1, replica_groups=mesh['z'=16,'c'=2,'y'=4,'x'=4] {'y'}, use_global_device_ids=true, to_apply=%region_6.0 | all-reduce | flops 640 | bytes 5120 | tf_op jit(solution)/shard_map/psum | solution.py:412
  202.1 7.4 %psum.31.t_ref = f32[2,320]{1,0:T(2,128)S(1)} all-reduce(f32[2,320]{1,0:T(2,128)S(1)} %psum.30), channel_id=1, replica_groups=mesh['z'=16,'c'=2,'y'=4,'x'=4] {'x'}, use_global_device_ids=true, to_apply=%region_7.0 | all-reduce | flops 640 | bytes 5120 | tf_op jit(solution)/shard_map/psum | solution.py:412
  209.5 5.0 %collective-permute-start.6 = (f32[64,128]{1,0:T(8,128)S(1)}, f32[64,128]{1,0:T(8,128)S(1)}, u32[]{:S(2)}, u32[]{:S(2)}) collective-permute-start(f32[64,128]{1,0:T(8,128)S(1)} %get-tuple-element.73), channel_id=1, source_target_pairs={{16,0},{32,16},{48,32},{64,48},{80,64},{96,80},{112,96},{128,112},... | collective-permute-start | bytes 98312 | tf_op jit(solution)/shard_map/ppermute | solution.py:423
  (58 shorter events, 22.5 us)
Async XLA Ops:
  0.6 20.4 %copy-start.3 = (bf16[1,64,2048]{2,1,0:T(8,128)(2,1)S(1)}, bf16[1,64,2048]{2,1,0:T(8,128)(2,1)}, u32[]{:S(2)}) copy-start(bf16[1,64,2048]{2,1,0:T(8,128)(2,1)} %param.18) | copy-start | bytes 786436
  0.6 20.4 %copy-start.4 = (bf16[1,64,2048]{2,1,0:T(8,128)(2,1)S(1)}, bf16[1,64,2048]{2,1,0:T(8,128)(2,1)}, u32[]{:S(2)}) copy-start(bf16[1,64,2048]{2,1,0:T(8,128)(2,1)} %param.19) | copy-start | bytes 786436
  0.7 20.4 %copy-start.5 = (bf16[1,64,2048]{2,1,0:T(8,128)(2,1)S(1)}, bf16[1,64,2048]{2,1,0:T(8,128)(2,1)}, u32[]{:S(2)}) copy-start(bf16[1,64,2048]{2,1,0:T(8,128)(2,1)} %param.20) | copy-start | bytes 786436
  0.7 31.9 %copy-start.2 = (bf16[320,64]{0,1:T(8,128)(2,1)S(1)}, bf16[320,64]{0,1:T(8,128)(2,1)}, u32[]{:S(2)}) copy-start(bf16[320,64]{0,1:T(8,128)(2,1)} %param.23) | copy-start | bytes 122884
  3.6 50.3 %all-to-all-start = ((bf16[32,32,256]{2,1,0:T(8,128)(2,1)}), bf16[32,32,256]{2,1,0:T(8,128)(2,1)S(1)}, u32[]{:S(2)}, u32[]{:S(2)}) async-start(bf16[32,32,256]{2,1,0:T(8,128)(2,1)} %bitcast.36), calls=%async_computation | async-start | bytes 1048576 | tf_op jit(solution)/shard_map/all_to_all | solution.py:314
  21.8 26.8 %collective-permute-start = (bf16[192,512]{1,0:T(8,128)(2,1)S(1)}, bf16[192,512]{1,0:T(8,128)(2,1)S(1)}, u32[]{:S(2)}, u32[]{:S(2)}) collective-permute-start(bf16[192,512]{1,0:T(8,128)(2,1)S(1)} %get-tuple-element.48), channel_id=1, source_target_pairs={{0,1},{1,2},{2,3},{3,0},{4,5},{5,6},{6,7},{7,4},{8,9},{9,10},{10,1... | collective-permute-start | bytes 589832 | tf_op jit(solution)/shard_map/ppermute | solution.py:59
  25.0 23.6 %collective-permute-start.1 = (bf16[192,512]{1,0:T(8,128)(2,1)S(1)}, bf16[192,512]{1,0:T(8,128)(2,1)S(1)}, u32[]{:S(2)}, u32[]{:S(2)}) collective-permute-start(bf16[192,512]{1,0:T(8,128)(2,1)S(1)} %get-tuple-element.49), channel_id=1, source_target_pairs={{0,2},{1,3},{2,0},{3,1},{4,6},{5,7},{6,4},{7,5},{8,10},{9,11},{10,... | collective-permute-start | bytes 589832 | tf_op jit(solution)/shard_map/ppermute | solution.py:59
  29.5 19.1 %collective-permute-start.2 = (bf16[192,512]{1,0:T(8,128)(2,1)S(1)}, bf16[192,512]{1,0:T(8,128)(2,1)S(1)}, u32[]{:S(2)}, u32[]{:S(2)}) collective-permute-start(bf16[192,512]{1,0:T(8,128)(2,1)S(1)} %get-tuple-element.50), channel_id=1, source_target_pairs={{0,3},{1,0},{2,1},{3,2},{4,7},{5,4},{6,5},{7,6},{8,11},{9,8},{10,9... | collective-permute-start | bytes 589832 | tf_op jit(solution)/shard_map/ppermute | solution.py:59
  110.0 2.2 copy-start
  125.5 34.0 %all-to-all-start.5 = ((bf16[32,32,128]{2,1,0:T(8,128)(2,1)}), bf16[32,32,128]{2,1,0:T(8,128)(2,1)S(1)}, u32[]{:S(2)}, u32[]{:S(2)}) async-start(bf16[32,32,128]{2,1,0:T(8,128)(2,1)} %bitcast.9), calls=%async_computation.5 | async-start | bytes 524288 | tf_op jit(solution)/shard_map/all_to_all | solution.py:363
  137.3 1.4 copy-start.1
  138.7 11.4 %copy-start.10 = (s32[2,320]{1,0:T(2,128)S(1)}, s32[2,320]{1,0:T(2,128)}, u32[]{:S(2)}) copy-start(s32[2,320]{1,0:T(2,128)} %get-tuple-element.67.t_ref) | copy-start | bytes 7684
  138.7 20.8 %copy-start.7 = (bf16[320,128]{1,0:T(8,128)(2,1)S(1)}, bf16[320,128]{1,0:T(8,128)(2,1)}, u32[]{:S(2)}) copy-start(bf16[320,128]{1,0:T(8,128)(2,1)} %c_ref.3) | copy-start | bytes 245764
  141.6 8.7 %collective-permute-start.3 = (bf16[192,512]{1,0:T(8,128)(2,1)S(1)}, bf16[192,512]{1,0:T(8,128)(2,1)S(1)}, u32[]{:S(2)}, u32[]{:S(2)}) collective-permute-start(bf16[192,512]{1,0:T(8,128)(2,1)S(1)} %get-tuple-element.57), channel_id=1, source_target_pairs={{0,1},{1,2},{2,3},{3,0},{4,5},{5,6},{6,7},{7,4},{8,9},{9,10},{10,1... | collective-permute-start | bytes 589832 | tf_op jit(solution)/shard_map/ppermute | solution.py:59
  143.9 8.2 %collective-permute-start.4 = (bf16[192,512]{1,0:T(8,128)(2,1)S(1)}, bf16[192,512]{1,0:T(8,128)(2,1)S(1)}, u32[]{:S(2)}, u32[]{:S(2)}) collective-permute-start(bf16[192,512]{1,0:T(8,128)(2,1)S(1)} %get-tuple-element.58), channel_id=1, source_target_pairs={{0,2},{1,3},{2,0},{3,1},{4,6},{5,7},{6,4},{7,5},{8,10},{9,11},{10,... | collective-permute-start | bytes 589832 | tf_op jit(solution)/shard_map/ppermute | solution.py:59
  147.5 6.7 %collective-permute-start.5 = (bf16[192,512]{1,0:T(8,128)(2,1)S(1)}, bf16[192,512]{1,0:T(8,128)(2,1)S(1)}, u32[]{:S(2)}, u32[]{:S(2)}) collective-permute-start(bf16[192,512]{1,0:T(8,128)(2,1)S(1)} %get-tuple-element.59), channel_id=1, source_target_pairs={{0,3},{1,0},{2,1},{3,2},{4,7},{5,4},{6,5},{7,6},{8,11},{9,8},{10,9... | collective-permute-start | bytes 589832 | tf_op jit(solution)/shard_map/ppermute | solution.py:59
  161.0 3.9 %copy-start.12 = (f32[64]{0:T(128)S(1)}, f32[64]{0:T(128)}, u32[]{:S(2)}) copy-start(f32[64]{0:T(128)} %param.25) | copy-start | bytes 772
  161.0 24.0 %all-to-all-start.6 = ((bf16[16,320,128]{2,1,0:T(8,128)(2,1)}), bf16[16,320,128]{2,1,0:T(8,128)(2,1)S(1)}, u32[]{:S(2)}, u32[]{:S(2)}) async-start(bf16[16,320,128]{2,1,0:T(8,128)(2,1)} %combine.1), calls=%async_computation.6 | async-start | bytes 2621440 | tf_op jit(solution)/shard_map/all_to_all | solution.py:391
  164.9 30.0 %copy-start.6 = (bf16[64,2048]{1,0:T(8,128)(2,1)S(1)}, bf16[64,2048]{1,0:T(8,128)(2,1)}, u32[]{:S(2)}) copy-start(bf16[64,2048]{1,0:T(8,128)(2,1)} %proj_ref.1) | copy-start | bytes 786436
  186.3 28.3 %copy-start.11 = (f32[31,64]{1,0:T(8,128)S(1)}, f32[31,64]{1,0:T(8,128)}, u32[]{:S(2)}) copy-start(f32[31,64]{1,0:T(8,128)} %param.24) | copy-start | bytes 23812
  186.3 31.2 %copy-start.8 = (bf16[320,64]{0,1:T(8,128)(2,1)S(1)}, bf16[320,64]{0,1:T(8,128)(2,1)}, u32[]{:S(2)}) copy-start(bf16[320,64]{0,1:T(8,128)(2,1)} %param.22) | copy-start | bytes 122884
  186.3 31.2 %copy-start.9 = (bf16[320,64]{0,1:T(8,128)(2,1)S(1)}, bf16[320,64]{0,1:T(8,128)(2,1)}, u32[]{:S(2)}) copy-start(bf16[320,64]{0,1:T(8,128)(2,1)} %param.21) | copy-start | bytes 122884
  186.3 33.1 %all-to-all-start.7 = ((bf16[32,32,128]{2,1,0:T(8,128)(2,1)}), bf16[32,32,128]{2,1,0:T(8,128)(2,1)S(1)}, u32[]{:S(2)}, u32[]{:S(2)}) async-start(bf16[32,32,128]{2,1,0:T(8,128)(2,1)} %proj_grad.1), calls=%async_computation.7 | async-start | bytes 524288 | tf_op jit(solution)/shard_map/all_to_all | solution.py:411
  209.5 8.0 %collective-permute-start.6 = (f32[64,128]{1,0:T(8,128)S(1)}, f32[64,128]{1,0:T(8,128)S(1)}, u32[]{:S(2)}, u32[]{:S(2)}) collective-permute-start(f32[64,128]{1,0:T(8,128)S(1)} %get-tuple-element.73), channel_id=1, source_target_pairs={{16,0},{32,16},{48,32},{64,48},{80,64},{96,80},{112,96},{128,112},... | collective-permute-start | bytes 98312 | tf_op jit(solution)/shard_map/ppermute | solution.py:423

commit v3 on v2

--- a/solution.py
+++ b/solution.py
@@ -13,7 +13,7 @@
 PLANE = ("c", "y", "x")
 SIDE = 4
 SLOT = 32
-ROOM = 24 << 20
+ROOM = 12 << 20
 BF = jnp.bfloat16
 F32 = jnp.float32
 VM = pltpu.VMEM
@@ -41,12 +41,23 @@
     for group in units:
         for me, p in enumerate(group):
             table[p, 0] = me
+            table[p, 1] = of_features[p].index(p)
+            table[p, 2] = p // (SIDE * SIDE)
             for k in range(SIDE):
                 ahead = of_features[group[(me + k) % SIDE]]
                 back = of_features[group[(me - k) % SIDE]]
                 for a in range(SIDE):
                     table[p, 16 + k * SIDE + a] = ahead[a] % (SIDE * SIDE)
                     table[p, 32 + k * SIDE + a] = back[a] % (SIDE * SIDE)
+    of_units = {p: g for g in units for p in g}
+    for p in range(2 * SIDE * SIDE):
+        group = of_features[p]
+        for j in range(SIDE):
+            source = group[(group.index(p) - j) % SIDE]
+            their = of_units[source]
+            for k in range(SIDE):
+                first = their[(their.index(source) - k) % SIDE]
+                table[p, 48 + j * SIDE + k] = first % (SIDE * SIDE)
     return table
 
 
@@ -110,13 +121,47 @@
     p_ref[...] = jnp.where(held, 1.0, 0.0).astype(BF)
 
 
-def split_kernel(at_ref, g_ref, u_ref, d_ref, *outs):
+def split_kernel(at_ref, g_ref, u_ref, d_ref, p_ref, c_ref, *outs):
     for k, out in enumerate(outs):
         for a in range(SIDE):
             at = at_ref[16 + k * SIDE + a]
             cols = pl.ds(pl.multiple_of(at * 128, 128), 128)
-            for q, ref in enumerate((g_ref, u_ref, d_ref)):
+            for q, ref in enumerate((g_ref, u_ref, d_ref, p_ref)):
                 out[q * 64 : q * 64 + 64, a * 128 : a * 128 + 128] = ref[:, cols]
+        out[256:320, :] = c_ref[...]
+
+
+def relay_kernel(at_ref, r0, r1, r2, r3, *outs):
+    for j, out in enumerate(outs):
+        a = lax.rem(at_ref[1] + j, SIDE)
+        cols = pl.ds(pl.multiple_of(a * 128, 128), 128)
+        for k, r_ref in enumerate((r0, r1, r2, r3)):
+            out[k * 64 : k * 64 + 64, 0:128] = r_ref[192:256, cols]
+            out[k * 64 : k * 64 + 64, 128:512] = r_ref[256:320, 128:512]
+
+
+def prep_kernel(q0, q1, q2, q3, act_ref, h_ref, n_ref, stats_ref):
+    qs = (q0, q1, q2, q3)
+    tokens = stats_ref.shape[1]
+    channels = SIDE * q0.shape[0]
+    conv = [q[:, 128 : 128 + tokens].astype(F32) for q in qs]
+    mean = sum(jnp.sum(v, axis=0, keepdims=True) for v in conv) / channels
+    off = [v - mean for v in conv]
+    var = sum(jnp.sum(v * v, axis=0, keepdims=True) for v in off) / channels
+    inv = lax.rsqrt(var + NORM_EPS)
+    stats_ref[0:1, :] = mean
+    stats_ref[1:2, :] = inv
+    lane = lax.broadcasted_iota(jnp.int32, (q0.shape[0], 128), 1)
+    for j, q in enumerate(qs):
+        pieces = jnp.where((lane >= 64) & (lane < 67), q[:, 384:512].astype(F32), 0.0)
+        gain = jnp.sum(pieces, axis=1, keepdims=True)
+        normed = off[j] * inv
+        linear = normed * gain
+        s = jax.nn.sigmoid(linear)
+        slope = s * (1.0 + linear * (1.0 - s)) * gain
+        act_ref[j] = (linear * s).astype(BF)
+        h_ref[j] = slope.astype(BF)
+        n_ref[j] = (slope * normed).astype(BF)
 
 
 def merge_kernel(at_ref, s0, s1, s2, s3, g_ref, u_ref, d_ref):
@@ -180,55 +225,59 @@
         out[128:192, :] = mm(h_ref[b, 128:192, :], c, NN).astype(BF)
 
 
-def combine_kernel(p_ref, r_ref, c_ref, o_ref):
+def tail_kernel(
+    at_ref, p_ref, r_ref, c_ref, q0, q1, q2, q3, act_ref, h_ref, n_ref, o_ref, mine_ref, other_ref
+):
     moe = mm(p_ref[...], r_ref[...], TN)
     total = (c_ref[...].astype(F32) + moe).astype(BF)
+    tokens = total.shape[0]
+    first = jnp.zeros((1, tokens), F32)
+    second = jnp.zeros((1, tokens), F32)
+    own = jnp.full((32, 128), at_ref[2], jnp.int32) == 0
+    low = lax.broadcasted_iota(jnp.int32, (32, 128), 1) < 64
+    for j, q in enumerate((q0, q1, q2, q3)):
+        cot = mm(q[:, 0:128], total, NT)
+        first = first + jnp.sum(cot * h_ref[j].astype(F32), axis=0, keepdims=True)
+        second = second + jnp.sum(cot * n_ref[j].astype(F32), axis=0, keepdims=True)
+        grad = mm(act_ref[j], total, NN)
+        turned = pltpu.roll(grad, 64, 1)
+        for k in range(SIDE):
+            b = at_ref[48 + j * SIDE + k]
+            o_ref[b, 0:64, :] = cot[k * 64 : k * 64 + 64].astype(BF)
+            up, down = slice(k * 64, k * 64 + 32), slice(k * 64 + 32, k * 64 + 64)
+            left = jnp.where(low, grad[up], turned[down])
+            right = jnp.where(low, turned[up], grad[down])
+            mine_ref[b] = jnp.where(own, left, right).astype(BF)
+            other_ref[b] = jnp.where(own, right, left).astype(BF)
+    row = lax.broadcasted_iota(jnp.int32, (16, tokens), 0)
+    sums = jnp.zeros((16, tokens), F32)
+    for i, v in enumerate((first, second)):
+        head = v.astype(BF).astype(F32)
+        sums = jnp.where(row == 2 * i, head, jnp.where(row == 2 * i + 1, v - head, sums))
     for b in range(o_ref.shape[0]):
-        o_ref[b] = total
-
-
-def normed_of(conv, sums, channels):
-    mean = sums[0:1, :] / channels
-    var = sums[1:2, :] / channels - mean * mean
-    inv = lax.rsqrt(var + NORM_EPS)
-    return (conv.astype(F32) - mean) * inv, inv
-
-
-def proj_kernel(f_ref, conv_ref, sums_ref, gain_ref, o_ref):
+        o_ref[b, 64:80, :] = sums.astype(BF)
+
+
+def head_kernel(r_ref, conv_ref, stats_ref, gain_ref, o_ref, h_ref):
+    total = r_ref[0].astype(F32)
+    for b in range(1, r_ref.shape[0]):
+        total = total + r_ref[b].astype(F32)
     channels = 16 * conv_ref.shape[0]
-    normed, _ = normed_of(conv_ref[...], sums_ref[...], channels)
-    linear = normed * gain_ref[...]
-    act = (linear * jax.nn.sigmoid(linear)).astype(BF)
-    low = lax.broadcasted_iota(jnp.int32, (32, 128), 1) < 64
-    for b in range(f_ref.shape[0]):
-        g = mm(act, f_ref[b], NN)
-        turned = pltpu.roll(g, 64, 1)
-        o_ref[2 * b] = jnp.where(low, g[0:32], turned[32:64]).astype(BF)
-        o_ref[2 * b + 1] = jnp.where(low, turned[0:32], g[32:64]).astype(BF)
-
-
-def norm_kernel(f_ref, proj_ref, conv_ref, sums_ref, gain_ref, n_ref, t_ref):
-    channels = 16 * conv_ref.shape[0]
-    total = mm(proj_ref[:, 0:128], f_ref[0], NT)
-    for b in range(1, f_ref.shape[0]):
-        total = total + mm(proj_ref[:, b * 128 : b * 128 + 128], f_ref[b], NT)
-    normed, _ = normed_of(conv_ref[...], sums_ref[...], channels)
+    first = (total[64:65] + total[65:66]) / channels
+    second = (total[66:67] + total[67:68]) / channels
+    inv = stats_ref[1:2, :]
+    normed = (conv_ref[...].astype(F32) - stats_ref[0:1, :]) * inv
     gain = gain_ref[...]
     linear = normed * gain
     s = jax.nn.sigmoid(linear)
-    cot = total * s * (1.0 + linear * (1.0 - s)) * gain
-    n_ref[...] = cot
-    t_ref[0:1, :] = jnp.sum(cot, axis=0, keepdims=True)
-    t_ref[1:2, :] = jnp.sum(cot * normed, axis=0, keepdims=True)
-
-
-def head_kernel(n_ref, t_ref, conv_ref, sums_ref, o_ref, h_ref):
-    channels = 16 * conv_ref.shape[0]
-    normed, inv = normed_of(conv_ref[...], sums_ref[...], channels)
-    t = t_ref[...]
-    cot = inv * (n_ref[...] - t[0:1, :] / channels - normed * (t[1:2, :] / channels))
+    cot = total[0:64] * s * (1.0 + linear * (1.0 - s)) * gain
+    cot = inv * (cot - first - normed * second)
     o_ref[...] = cot
     h_ref[...] = cot[:, 0:128]
+
+
+def add_kernel(a_ref, b_ref, o_ref):
+    o_ref[...] = (a_ref[...].astype(F32) + b_ref[...].astype(F32)).astype(BF)
 
 
 def conv_kernel(cot_ref, next_ref, taps_ref, gate_ref, value_ref, v_ref, g_ref, buf):
@@ -287,8 +336,8 @@
         cost_estimate=cost(400000000, 2000000),
         name="route",
     )(routes.T, route_weight.T, moe_input, out_cotangent)
-    sent, target, table, gate_weight, conv_result = lax.optimization_barrier(
-        (sent, target, jnp.asarray(step_tables()), gate_weight, conv_result)
+    sent, target, table, gate_weight, conv_result, norm_gain = lax.optimization_barrier(
+        (sent, target, jnp.asarray(step_tables()), gate_weight, conv_result, norm_gain)
     )
     at = table[lax.axis_index(PLANE)]
     pick = pl.pallas_call(
@@ -300,26 +349,38 @@
         cost_estimate=cost(1000000, 700000),
         name="pick",
     )(target)
+    conv_t = conv_result.T
+    gain = norm_gain.reshape(-1, 1)
+    high = lax.reduce_precision(gain, 8, 7)
+    middle = lax.reduce_precision(gain - high, 8, 7)
+    pieces = jnp.concatenate([high, middle, gain - high - middle], axis=1).astype(BF)
+    channel_part = jnp.concatenate(
+        [jnp.zeros((64, 128), BF), conv_t, pieces, jnp.zeros((64, 61), BF)], axis=1
+    )
     split = pl.pallas_call(
         split_kernel,
-        out_shape=(whole((192, 512), BF),) * SIDE,
-        in_specs=[smem, vmem, vmem, vmem],
+        out_shape=(whole((320, 512), BF),) * SIDE,
+        in_specs=[smem] + [vmem] * 5,
         out_specs=(vmem,) * SIDE,
         compiler_params=room,
-        cost_estimate=cost(1000000, 1600000),
+        cost_estimate=cost(1000000, 2600000),
         name="split_weights",
-    )(at, gate_weight[0], up_weight[0], down_weight[0])
+    )(at, gate_weight[0], up_weight[0], down_weight[0], proj_weight, channel_part)
     weights = pass_on(split, unit_groups)
+    relay = pl.pallas_call(
+        relay_kernel,
+        out_shape=(whole((256, 512), BF),) * SIDE,
+        in_specs=[smem] + [vmem] * SIDE,
+        out_specs=(vmem,) * SIDE,
+        compiler_params=room,
+        cost_estimate=cost(1000000, 2000000),
+        name="relay",
+    )(at, *weights)
+    relay = pass_on(relay, feature_groups)
 
     got = lax.all_to_all(sent.reshape(sp_count, SLOT, 256), SP, 0, 0, tiled=True)
     got = got.reshape(slots, 256)
-
-    conv_t = conv_result.T
-    conv_f = conv_t.astype(F32)
-    sums = jnp.stack([jnp.sum(conv_f, axis=0), jnp.sum(conv_f * conv_f, axis=0)])
-    sums = lax.psum(lax.psum(sums, "y"), "x")
-    got, sums, weights = lax.optimization_barrier((got, sums, weights))
-    gain = norm_gain.reshape(-1, 1)
+    got, weights, relay = lax.optimization_barrier((got, weights, relay))
     taps_t = conv_taps.T
 
     rows = exchange(jnp.broadcast_to(got[None], (SIDE, slots, 256)), feature_groups)
@@ -336,6 +397,18 @@
         name="pre",
     )(at, rows, *weights)
     pre = exchange(pre, unit_groups)
+    act, slope, slope_normed, stats = pl.pallas_call(
+        prep_kernel,
+        out_shape=(whole((SIDE, 256, tokens), BF),) * 3 + (whole((2, tokens), F32),),
+        in_specs=[vmem] * SIDE,
+        out_specs=(vmem,) * 4,
+        compiler_params=room,
+        cost_estimate=cost(20000000, 3000000),
+        name="prep",
+    )(*relay)
+    pre, act, slope, slope_normed, stats = lax.optimization_barrier(
+        (pre, act, slope, slope_normed, stats)
+    )
     hidden = pl.pallas_call(
         gate_kernel,
         grid=(slots // step,),
@@ -379,46 +452,50 @@
     grads = pass_on(grads, unit_groups)
     returned, grads = lax.optimization_barrier((returned, grads))
 
-    spread = pl.pallas_call(
-        combine_kernel,
-        out_shape=whole((tp_count, tokens, 128), BF),
-        in_specs=[vmem] * 3,
+    act_part, mine, other = pl.pallas_call(
+        tail_kernel,
+        out_shape=(
+            whole((tp_count, 80, tokens), BF),
+            whole((tp_count, 32, 128), BF),
+            whole((tp_count, 32, 128), BF),
+        ),
+        in_specs=[smem] + [vmem] * 10,
+        out_specs=(vmem,) * 3,
+        compiler_params=room,
+        cost_estimate=cost(250000000, 4500000),
+        name="tail",
+    )(at, pick, returned, out_cotangent, *relay, act, slope, slope_normed)
+    act_part = lax.all_to_all(act_part, TP, 0, 0, tiled=True)
+    other = lax.ppermute(other, "c", [(0, 1), (1, 0)])
+    proj_part = pl.pallas_call(
+        add_kernel,
+        out_shape=whole((tp_count, 32, 128), BF),
+        in_specs=[vmem] * 2,
         out_specs=vmem,
         compiler_params=room,
-        cost_estimate=cost(80000000, 2500000),
-        name="combine",
-    )(pick, returned, out_cotangent)
-    full = lax.all_to_all(spread, TP, 0, 0, tiled=True)
-
-    proj_part = pl.pallas_call(
-        proj_kernel,
-        out_shape=whole((sp_count, 32, 128), BF),
-        in_specs=[vmem] * 4,
-        out_specs=vmem,
-        compiler_params=room,
-        cost_estimate=cost(84000000, 1600000),
-        name="proj_grad",
-    )(full, conv_t, sums, gain)
-    norm_cot, cot_sums = pl.pallas_call(
-        norm_kernel,
-        out_shape=(whole((64, tokens), F32), whole((2, tokens), F32)),
-        in_specs=[vmem] * 5,
-        out_specs=(vmem, vmem),
-        compiler_params=room,
-        cost_estimate=cost(84000000, 1600000),
-        name="norm_cot",
-    )(full, proj_weight, conv_t, sums, gain)
-    proj_part = lax.all_to_all(proj_part, SP, 0, 0, tiled=True)
-    cot_sums = lax.psum(lax.psum(cot_sums, "y"), "x")
+        cost_estimate=cost(100000, 400000),
+        name="add_core",
+    )(mine, other)
+    side = SIDE * SIDE
+    swap = [
+        (z * 2 * side + c * side + t, t * 2 * side + c * side + z)
+        for z in range(side)
+        for c in range(2)
+        for t in range(side)
+    ]
+    proj_part = lax.ppermute(proj_part, ("z",) + PLANE, swap)
+    act_part, proj_part = lax.optimization_barrier((act_part, proj_part))
+    proj_part = lax.all_to_all(proj_part, TP, 0, 0, tiled=True)
+
     conv_cot, head = pl.pallas_call(
         head_kernel,
         out_shape=(whole((64, tokens), F32), whole((64, 128), F32)),
         in_specs=[vmem] * 4,
         out_specs=(vmem, vmem),
         compiler_params=room,
-        cost_estimate=cost(1000000, 200000),
+        cost_estimate=cost(3000000, 1200000),
         name="conv_cot",
-    )(norm_cot, cot_sums, conv_t, sums)
+    )(act_part, conv_t, stats, gain)
     behind = [(i + 1, i) for i in range(sp_count - 1)]
     after = lax.ppermute(head, SP, behind)
     value, gate = pl.pallas_call(

time: 221 us -> 235 us (1.063)
  blocking collectives: 93.6 us -> 45.9 us
  starting transfers between devices: 65 us -> 108 us
  local copies, waits for them, and re-layouts: 3.25 us -> 19.9 us
  Pallas kernels: 21 us -> 23.9 us
    psum x4 -> x0, blocking collectives: 30 us -> none  [the longest x2 16 us: body(): sums = lax.psum(lax.psum(sums, 'y'), 'x')]
    all_to_all x2 -> x3, starting transfers between devices: 12.4 us -> 35.2 us  [the longest x1 27.1 us: body(): proj_part = lax.all_to_all(proj_part, TP, 0, 0, tiled=True)]
    all_to_all x4 -> x3, blocking collectives: 63.6 us -> 45.9 us  [exchange(): return lax.all_to_all(v, PLANE, 0, 0, axis_index_groups=groups, tiled=True)]
    unnamed x28 -> x78, local copies, waits for them, and re-layouts: 2.24 us -> 17.4 us
    ppermute x6 -> x9, starting transfers between devices: 19.1 us -> 29.7 us  [pass_on(): lax.ppermute(parts[k], PLANE, steps_ahead(groups, k))]
    ppermute x6 -> x9, waiting for transfers between devices: 3.94 us -> 12.1 us  [pass_on(): lax.ppermute(parts[k], PLANE, steps_ahead(groups, k))]
    all_to_all x1, starting transfers between devices: 11.7 us -> 19.7 us  [body(): returned = lax.all_to_all(back, SP, 0, 0, tiled=True).reshape(slots, 128)]
    all_to_all x1, waiting for transfers between devices: 5.19 us -> 0.01 us  [body(): lax.all_to_all(sent.reshape(sp_count, SLOT, 256), SP, 0, 0, tiled=True)]
  transfers between devices with their start and end apart: 11 -> 17, of which waited for: 6 -> 11; matrix products, arithmetic and copies ran while one was open for 0% -> 1% of each run, Pallas kernels for 4% -> 4%
where the time goes in v3:
time: 235 us; the launch traced here: 234 us
  starting transfers between devices  108 us (46%)
  blocking collectives  45.9 us (20%)
  waiting for transfers between devices  33.9 us (14%)
  Pallas kernels  23.9 us (10%)
  local copies, waits for them, and re-layouts  19.9 us (8%)
    all_to_all x3, blocking collectives, exchange(): return lax.all_to_all(v, PLANE, 0, 0, axis_index_groups=groups, tiled=True)  45.9 us
    ppermute x9, starting transfers between devices, pass_on(): lax.ppermute(parts[k], PLANE, steps_ahead(groups, k))  29.7 us
    all_to_all x1, starting transfers between devices, body(): proj_part = lax.all_to_all(proj_part, TP, 0, 0, tiled=True)  27.1 us
    all_to_all x1, starting transfers between devices, body(): returned = lax.all_to_all(back, SP, 0, 0, tiled=True).reshape(slots, 128)  19.7 us
    unnamed x78, local copies, waits for them, and re-layouts  17.4 us
    all_to_all x1, starting transfers between devices, body(): lax.all_to_all(sent.reshape(sp_count, SLOT, 256), SP, 0, 0, tiled=True)  16.8 us
    ppermute x9, waiting for transfers between devices, pass_on(): lax.ppermute(parts[k], PLANE, steps_ahead(groups, k))  12.1 us
    all_to_all x1, waiting for transfers between devices, body(): act_part = lax.all_to_all(act_part, TP, 0, 0, tiled=True)  10.6 us
  transfers between devices with their start and end apart: 17, of which 11 were waited for; matrix products, arithmetic and copies ran while one was open for 1% of the time, Pallas kernels for 4%

profile of v3, /device:TPU:1, one launch (start us, length us, event | category | flops | bytes accessed | tf_op | source)
XLA Modules:
  0.0 233.9 jit_solution(2824233735522989019)
XLA Ops:
  0.7 2.9 %route.1 = (bf16[1024,256]{1,0:T(8,128)(2,1)}, s32[2,320]{1,0:T(2,128)}) custom-call(s32[2,320]{1,0:T(2,128)} %bitcast.45, f32[2,320]{1,0:T(2,128)} %bitcast.46, bf16[320,128]{1,0:T(8,128)(2,1)} %x_ref.1, bf16[320,128]{1,0:T(8,128)(2,1)} %c_ref.3), custom_call_target="tpu_custom_call" | custom-call | flops 400000000 | bytes 2000000 | tf_op jit(solution)/shard_map/route/pallas_call | solution.py:331
  3.6 16.8 %all-to-all-start = ((bf16[32,32,256]{2,1,0:T(8,128)(2,1)}), bf16[32,32,256]{2,1,0:T(8,128)(2,1)}, u32[]{:S(2)}, u32[]{:S(2)}) async-start(bf16[32,32,256]{2,1,0:T(8,128)(2,1)} %bitcast.38), calls=%async_computation | async-start | bytes 1048576 | tf_op jit(solution)/shard_map/all_to_all | solution.py:381
  22.5 3.2 %collective-permute-start = (bf16[320,512]{1,0:T(8,128)(2,1)S(1)}, bf16[320,512]{1,0:T(8,128)(2,1)S(1)}, u32[]{:S(2)}, u32[]{:S(2)}) collective-permute-start(bf16[320,512]{1,0:T(8,128)(2,1)S(1)} %get-tuple-element.69), channel_id=1, source_target_pairs={{0,1},{1,2},{2,3},{3,0},{4,5},{5,6},{6,7},{7,4},{8,9},{9,10},{10,1... | collective-permute-start | bytes 983048 | tf_op jit(solution)/shard_map/ppermute | solution.py:70
  25.7 4.5 %collective-permute-start.1 = (bf16[320,512]{1,0:T(8,128)(2,1)S(1)}, bf16[320,512]{1,0:T(8,128)(2,1)S(1)}, u32[]{:S(2)}, u32[]{:S(2)}) collective-permute-start(bf16[320,512]{1,0:T(8,128)(2,1)S(1)} %get-tuple-element.70), channel_id=1, source_target_pairs={{0,2},{1,3},{2,0},{3,1},{4,6},{5,7},{6,4},{7,5},{8,10},{9,11},{10,... | collective-permute-start | bytes 983048 | tf_op jit(solution)/shard_map/ppermute | solution.py:70
  30.2 3.0 %collective-permute-start.2 = (bf16[320,512]{1,0:T(8,128)(2,1)S(1)}, bf16[320,512]{1,0:T(8,128)(2,1)S(1)}, u32[]{:S(2)}, u32[]{:S(2)}) collective-permute-start(bf16[320,512]{1,0:T(8,128)(2,1)S(1)} %get-tuple-element.71), channel_id=1, source_target_pairs={{0,3},{1,0},{2,1},{3,2},{4,7},{5,4},{6,5},{7,6},{8,11},{9,8},{10,9... | collective-permute-start | bytes 983048 | tf_op jit(solution)/shard_map/ppermute | solution.py:70
  33.2 3.3 %collective-permute-done.1.r2.w2 = bf16[320,512]{1,0:T(8,128)(2,1)S(1)} collective-permute-done((bf16[320,512]{1,0:T(8,128)(2,1)S(1)}, bf16[320,512]{1,0:T(8,128)(2,1)S(1)}, u32[]{:S(2)}, u32[]{:S(2)}) %collective-permute-start.1) | collective-permute-done | bytes 327712 | tf_op jit(solution)/shard_map/ppermute | solution.py:70
  39.8 3.1 %collective-permute-start.3 = (bf16[256,512]{1,0:T(8,128)(2,1)S(1)}, bf16[256,512]{1,0:T(8,128)(2,1)S(1)}, u32[]{:S(2)}, u32[]{:S(2)}) collective-permute-start(bf16[256,512]{1,0:T(8,128)(2,1)S(1)} %get-tuple-element.73), channel_id=1, source_target_pairs={{0,4},{4,8},{8,12},{12,0},{1,5},{5,9},{9,13},{13,1},{2,6},{6,10},{... | collective-permute-start | bytes 786440 | tf_op jit(solution)/shard_map/ppermute | solution.py:70
  42.9 4.4 %collective-permute-start.4 = (bf16[256,512]{1,0:T(8,128)(2,1)S(1)}, bf16[256,512]{1,0:T(8,128)(2,1)S(1)}, u32[]{:S(2)}, u32[]{:S(2)}) collective-permute-start(bf16[256,512]{1,0:T(8,128)(2,1)S(1)} %get-tuple-element.74), channel_id=1, source_target_pairs={{0,8},{4,12},{8,0},{12,4},{1,9},{5,13},{9,1},{13,5},{2,10},{6,14},... | collective-permute-start | bytes 786440 | tf_op jit(solution)/shard_map/ppermute | solution.py:70
  47.3 3.1 %collective-permute-start.5 = (bf16[256,512]{1,0:T(8,128)(2,1)S(1)}, bf16[256,512]{1,0:T(8,128)(2,1)S(1)}, u32[]{:S(2)}, u32[]{:S(2)}) collective-permute-start(bf16[256,512]{1,0:T(8,128)(2,1)S(1)} %get-tuple-element.75), channel_id=1, source_target_pairs={{0,12},{4,0},{8,4},{12,8},{1,13},{5,1},{9,5},{13,9},{2,14},{6,2},{... | collective-permute-start | bytes 786440 | tf_op jit(solution)/shard_map/ppermute | solution.py:70
  56.6 18.5 %all_to_all.40.a_ref = bf16[4,1024,256]{2,1,0:T(8,128)(2,1)S(1)} all-to-all(bf16[4,1024,256]{2,1,0:T(8,128)(2,1)S(1)} %broadcast_in_dim.23), channel_id=1, replica_groups={{0,4,8,12},{1,5,9,13},{2,6,10,14},{3,7,11,15},{16,17,18,19},{20,21,22,2..., dimensions={0} | all-to-all | bytes 4194304 | tf_op jit(solution)/shard_map/all_to_all | solution.py:79
  75.2 4.0 %pre.1 = bf16[4,192,1024]{2,1,0:T(8,128)(2,1)S(1)} custom-call(s32[64]{0:T(128)S(1)} %dynamic-slice_bitcast_fusion.at_ref, bf16[4,1024,256]{2,1,0:T(8,128)(2,1)S(1)} %all_to_all.40.a_ref, bf16[320,512]{1,0:T(8,128)(2,1)S(1)} %get-tuple-element.77.r0.w0, bf16[320,512]{1,0:T(8,128)(2,1)S(1)} %collective-permute-done.r1.w1, ...), custom_call_target="tpu_custom_call" | custom-call | flops 800000000 | bytes 4400000 | tf_op jit(solution)/shard_map/pre/pallas_call | solution.py:388
  80.3 4.3 %all-to-all-start.2 = ((bf16[4,192,1024]{2,1,0:T(8,128)(2,1)}), bf16[4,192,1024]{2,1,0:T(8,128)(2,1)}, u32[]{:S(2)}, u32[]{:S(2)}) async-start(bf16[4,192,1024]{2,1,0:T(8,128)(2,1)} %copy-done.2), calls=%async_computation.2 | async-start | bytes 3145728 | tf_op jit(solution)/shard_map/all_to_all | solution.py:79
  92.3 5.0 %all-to-all-done.2.p_ref = bf16[4,192,1024]{2,1,0:T(8,128)(2,1)} async-done(((bf16[4,192,1024]{2,1,0:T(8,128)(2,1)}), bf16[4,192,1024]{2,1,0:T(8,128)(2,1)}, u32[]{:S(2)}, u32[]{:S(2)}) %all-to-all-start.2) | async-done | bytes 1572896 | tf_op jit(solution)/shard_map/all_to_all | solution.py:79
  99.7 15.2 %all_to_all.41.h_ref = bf16[4,192,1024]{2,1,0:T(8,128)(2,1)S(1)} all-to-all(bf16[4,192,1024]{2,1,0:T(8,128)(2,1)S(1)} %gates.1), channel_id=1, replica_groups={{0,1,2,3},{4,5,6,7},{8,9,10,11},{12,13,14,15},{16,20,24,28},{17,21,25,2..., dimensions={0} | all-to-all | bytes 3145728 | tf_op jit(solution)/shard_map/all_to_all | solution.py:79
  117.1 12.2 %all_to_all.42 = bf16[4,1024,128]{2,1,0:T(8,128)(2,1)S(1)} all-to-all(bf16[4,1024,128]{2,1,0:T(8,128)(2,1)S(1)} %partial.1), channel_id=1, replica_groups={{0,4,8,12},{1,5,9,13},{2,6,10,14},{3,7,11,15},{16,17,18,19},{20,21,22,2..., dimensions={0} | all-to-all | bytes 2097152 | tf_op jit(solution)/shard_map/all_to_all | solution.py:79
  130.2 19.7 %all-to-all-start.5 = ((bf16[32,32,128]{2,1,0:T(8,128)(2,1)}), bf16[32,32,128]{2,1,0:T(8,128)(2,1)S(1)}, u32[]{:S(2)}, u32[]{:S(2)}) async-start(bf16[32,32,128]{2,1,0:T(8,128)(2,1)} %bitcast.12), calls=%async_computation.5 | async-start | bytes 524288 | tf_op jit(solution)/shard_map/all_to_all | solution.py:436
  151.4 3.0 %grads.1 = (bf16[192,512]{1,0:T(8,128)(2,1)S(1)}, bf16[192,512]{1,0:T(8,128)(2,1)S(1)}, bf16[192,512]{1,0:T(8,128)(2,1)S(1)}, bf16[192,512]{1,0:T(8,128)(2,1)S(1)}) custom-call(s32[64]{0:T(128)S(1)} %dynamic-slice_bitcast_fusion.at_ref, bf16[4,192,1024]{2,1,0:T(8,128)(2,1)S(1)} %copy-done.1, bf16[4,1024,256]{2,1,0:T(8,128)(2,1)S(1)} %all_to_all.40.a_ref), custom_call_target="tpu_custom_call" | custom-call | flops 800000000 | bytes 4400000 | tf_op jit(solution)/shard_map/grads/pallas_call | solution.py:438
  156.6 3.7 %collective-permute-start.7 = (bf16[192,512]{1,0:T(8,128)(2,1)S(1)}, bf16[192,512]{1,0:T(8,128)(2,1)S(1)}, u32[]{:S(2)}, u32[]{:S(2)}) collective-permute-start(bf16[192,512]{1,0:T(8,128)(2,1)S(1)} %get-tuple-element.92), channel_id=1, source_target_pairs={{0,2},{1,3},{2,0},{3,1},{4,6},{5,7},{6,4},{7,5},{8,10},{9,11},{10,... | collective-permute-start | bytes 589832 | tf_op jit(solution)/shard_map/ppermute | solution.py:70
  167.7 4.5 %all-to-all-done.5 = bf16[32,32,128]{2,1,0:T(8,128)(2,1)S(1)} async-done(((bf16[32,32,128]{2,1,0:T(8,128)(2,1)}), bf16[32,32,128]{2,1,0:T(8,128)(2,1)S(1)}, u32[]{:S(2)}, u32[]{:S(2)}) %all-to-all-start.5) | async-done | bytes 262176 | tf_op jit(solution)/shard_map/all_to_all | solution.py:436
  178.9 3.8 %all-to-all-start.6 = ((bf16[16,80,320]{2,1,0:T(8,128)(2,1)}), bf16[16,80,320]{2,1,0:T(8,128)(2,1)S(1)}, u32[]{:S(2)}, u32[]{:S(2)}) async-start(bf16[16,80,320]{2,1,0:T(8,128)(2,1)} %get-tuple-element.106), calls=%async_computation.6 | async-start | bytes 1966080 | tf_op jit(solution)/shard_map/all_to_all | solution.py:468
  182.7 2.7 %collective-permute-start.9 = (bf16[16,32,128]{2,1,0:T(8,128)(2,1)S(1)}, bf16[16,32,128]{2,1,0:T(8,128)(2,1)S(1)}, u32[]{:S(2)}, u32[]{:S(2)}) collective-permute-start(bf16[16,32,128]{2,1,0:T(8,128)(2,1)S(1)} %copy-done.35), channel_id=1, source_target_pairs={{0,16},{16,0},{1,17},{17,1},{2,18},{18,2},{3,19},{19,3},{4,20},{20... | collective-permute-start | bytes 393224 | tf_op jit(solution)/shard_map/ppermute | solution.py:469
  187.7 10.6 %all-to-all-done.6.r_ref = bf16[16,80,320]{2,1,0:T(8,128)(2,1)S(1)} async-done(((bf16[16,80,320]{2,1,0:T(8,128)(2,1)}), bf16[16,80,320]{2,1,0:T(8,128)(2,1)S(1)}, u32[]{:S(2)}, u32[]{:S(2)}) %all-to-all-start.6) | async-done | bytes 819232 | tf_op jit(solution)/shard_map/all_to_all | solution.py:468
  198.3 27.1 %all-to-all-start.7 = ((bf16[16,32,128]{2,1,0:T(8,128)(2,1)}), bf16[16,32,128]{2,1,0:T(8,128)(2,1)S(1)}, u32[]{:S(2)}, u32[]{:S(2)}) async-start(bf16[16,32,128]{2,1,0:T(8,128)(2,1)} %collective-permute-done.10), calls=%async_computation.7 | async-start | bytes 262144 | tf_op jit(solution)/shard_map/all_to_all | solution.py:488
  225.7 2.7 %collective-permute-start.11 = (f32[64,128]{1,0:T(8,128)S(1)}, f32[64,128]{1,0:T(8,128)S(1)}, u32[]{:S(2)}, u32[]{:S(2)}) collective-permute-start(f32[64,128]{1,0:T(8,128)S(1)} %get-tuple-element.113), channel_id=1, source_target_pairs={{16,0},{32,16},{48,32},{64,48},{80,64},{96,80},{112,96},{128,112},... | collective-permute-start | bytes 98312 | tf_op jit(solution)/shard_map/ppermute | solution.py:500
  (119 shorter events, 51.4 us)
Async XLA Ops:
  0.6 21.0 %copy-start.21 = (bf16[1,64,2048]{2,1,0:T(8,128)(2,1)S(1)}, bf16[1,64,2048]{2,1,0:T(8,128)(2,1)}, u32[]{:S(2)}) copy-start(bf16[1,64,2048]{2,1,0:T(8,128)(2,1)} %param.18) | copy-start | bytes 786436
  0.7 21.0 %copy-start.22 = (bf16[1,64,2048]{2,1,0:T(8,128)(2,1)S(1)}, bf16[1,64,2048]{2,1,0:T(8,128)(2,1)}, u32[]{:S(2)}) copy-start(bf16[1,64,2048]{2,1,0:T(8,128)(2,1)} %param.19) | copy-start | bytes 786436
  3.6 51.8 %all-to-all-start = ((bf16[32,32,256]{2,1,0:T(8,128)(2,1)}), bf16[32,32,256]{2,1,0:T(8,128)(2,1)}, u32[]{:S(2)}, u32[]{:S(2)}) async-start(bf16[32,32,256]{2,1,0:T(8,128)(2,1)} %bitcast.38), calls=%async_computation | async-start | bytes 1048576 | tf_op jit(solution)/shard_map/all_to_all | solution.py:381
  22.5 10.7 %collective-permute-start = (bf16[320,512]{1,0:T(8,128)(2,1)S(1)}, bf16[320,512]{1,0:T(8,128)(2,1)S(1)}, u32[]{:S(2)}, u32[]{:S(2)}) collective-permute-start(bf16[320,512]{1,0:T(8,128)(2,1)S(1)} %get-tuple-element.69), channel_id=1, source_target_pairs={{0,1},{1,2},{2,3},{3,0},{4,5},{5,6},{6,7},{7,4},{8,9},{9,10},{10,1... | collective-permute-start | bytes 983048 | tf_op jit(solution)/shard_map/ppermute | solution.py:70
  25.7 10.9 %collective-permute-start.1 = (bf16[320,512]{1,0:T(8,128)(2,1)S(1)}, bf16[320,512]{1,0:T(8,128)(2,1)S(1)}, u32[]{:S(2)}, u32[]{:S(2)}) collective-permute-start(bf16[320,512]{1,0:T(8,128)(2,1)S(1)} %get-tuple-element.70), channel_id=1, source_target_pairs={{0,2},{1,3},{2,0},{3,1},{4,6},{5,7},{6,4},{7,5},{8,10},{9,11},{10,... | collective-permute-start | bytes 983048 | tf_op jit(solution)/shard_map/ppermute | solution.py:70
  30.2 8.2 %collective-permute-start.2 = (bf16[320,512]{1,0:T(8,128)(2,1)S(1)}, bf16[320,512]{1,0:T(8,128)(2,1)S(1)}, u32[]{:S(2)}, u32[]{:S(2)}) collective-permute-start(bf16[320,512]{1,0:T(8,128)(2,1)S(1)} %get-tuple-element.71), channel_id=1, source_target_pairs={{0,3},{1,0},{2,1},{3,2},{4,7},{5,4},{6,5},{7,6},{8,11},{9,8},{10,9... | collective-permute-start | bytes 983048 | tf_op jit(solution)/shard_map/ppermute | solution.py:70
  39.8 10.6 %collective-permute-start.3 = (bf16[256,512]{1,0:T(8,128)(2,1)S(1)}, bf16[256,512]{1,0:T(8,128)(2,1)S(1)}, u32[]{:S(2)}, u32[]{:S(2)}) collective-permute-start(bf16[256,512]{1,0:T(8,128)(2,1)S(1)} %get-tuple-element.73), channel_id=1, source_target_pairs={{0,4},{4,8},{8,12},{12,0},{1,5},{5,9},{9,13},{13,1},{2,6},{6,10},{... | collective-permute-start | bytes 786440 | tf_op jit(solution)/shard_map/ppermute | solution.py:70
  42.9 9.4 %collective-permute-start.4 = (bf16[256,512]{1,0:T(8,128)(2,1)S(1)}, bf16[256,512]{1,0:T(8,128)(2,1)S(1)}, u32[]{:S(2)}, u32[]{:S(2)}) collective-permute-start(bf16[256,512]{1,0:T(8,128)(2,1)S(1)} %get-tuple-element.74), channel_id=1, source_target_pairs={{0,8},{4,12},{8,0},{12,4},{1,9},{5,13},{9,1},{13,5},{2,10},{6,14},... | collective-permute-start | bytes 786440 | tf_op jit(solution)/shard_map/ppermute | solution.py:70
  47.3 7.4 %collective-permute-start.5 = (bf16[256,512]{1,0:T(8,128)(2,1)S(1)}, bf16[256,512]{1,0:T(8,128)(2,1)S(1)}, u32[]{:S(2)}, u32[]{:S(2)}) collective-permute-start(bf16[256,512]{1,0:T(8,128)(2,1)S(1)} %get-tuple-element.75), channel_id=1, source_target_pairs={{0,12},{4,0},{8,4},{12,8},{1,13},{5,1},{9,5},{13,9},{2,14},{6,2},{... | collective-permute-start | bytes 786440 | tf_op jit(solution)/shard_map/ppermute | solution.py:70
  80.3 17.0 %all-to-all-start.2 = ((bf16[4,192,1024]{2,1,0:T(8,128)(2,1)}), bf16[4,192,1024]{2,1,0:T(8,128)(2,1)}, u32[]{:S(2)}, u32[]{:S(2)}) async-start(bf16[4,192,1024]{2,1,0:T(8,128)(2,1)} %copy-done.2), calls=%async_computation.2 | async-start | bytes 3145728 | tf_op jit(solution)/shard_map/all_to_all | solution.py:79
  130.2 42.0 %all-to-all-start.5 = ((bf16[32,32,128]{2,1,0:T(8,128)(2,1)}), bf16[32,32,128]{2,1,0:T(8,128)(2,1)S(1)}, u32[]{:S(2)}, u32[]{:S(2)}) async-start(bf16[32,32,128]{2,1,0:T(8,128)(2,1)} %bitcast.12), calls=%async_computation.5 | async-start | bytes 524288 | tf_op jit(solution)/shard_map/all_to_all | solution.py:436
  154.4 8.7 %collective-permute-start.6 = (bf16[192,512]{1,0:T(8,128)(2,1)S(1)}, bf16[192,512]{1,0:T(8,128)(2,1)S(1)}, u32[]{:S(2)}, u32[]{:S(2)}) collective-permute-start(bf16[192,512]{1,0:T(8,128)(2,1)S(1)} %get-tuple-element.91), channel_id=1, source_target_pairs={{0,1},{1,2},{2,3},{3,0},{4,5},{5,6},{6,7},{7,4},{8,9},{9,10},{10,1... | collective-permute-start | bytes 589832 | tf_op jit(solution)/shard_map/ppermute | solution.py:70
  156.6 8.2 %collective-permute-start.7 = (bf16[192,512]{1,0:T(8,128)(2,1)S(1)}, bf16[192,512]{1,0:T(8,128)(2,1)S(1)}, u32[]{:S(2)}, u32[]{:S(2)}) collective-permute-start(bf16[192,512]{1,0:T(8,128)(2,1)S(1)} %get-tuple-element.92), channel_id=1, source_target_pairs={{0,2},{1,3},{2,0},{3,1},{4,6},{5,7},{6,4},{7,5},{8,10},{9,11},{10,... | collective-permute-start | bytes 589832 | tf_op jit(solution)/shard_map/ppermute | solution.py:70
  160.3 6.7 %collective-permute-start.8 = (bf16[192,512]{1,0:T(8,128)(2,1)S(1)}, bf16[192,512]{1,0:T(8,128)(2,1)S(1)}, u32[]{:S(2)}, u32[]{:S(2)}) collective-permute-start(bf16[192,512]{1,0:T(8,128)(2,1)S(1)} %get-tuple-element.93), channel_id=1, source_target_pairs={{0,3},{1,0},{2,1},{3,2},{4,7},{5,4},{6,5},{7,6},{8,11},{9,8},{10,9... | collective-permute-start | bytes 589832 | tf_op jit(solution)/shard_map/ppermute | solution.py:70
  178.9 49.5 %copy-start.36 = (f32[31,64]{1,0:T(8,128)S(1)}, f32[31,64]{1,0:T(8,128)}, u32[]{:S(2)}) copy-start(f32[31,64]{1,0:T(8,128)} %param.24) | copy-start | bytes 23812
  178.9 49.6 %copy-start.27 = (bf16[192,512]{1,0:T(8,128)(2,1)S(1)}, bf16[192,512]{1,0:T(8,128)(2,1)}, u32[]{:S(2)}) copy-start(bf16[192,512]{1,0:T(8,128)(2,1)} %copy-done.26) | copy-start | bytes 589828
  178.9 49.6 %copy-start.29 = (bf16[192,512]{1,0:T(8,128)(2,1)S(1)}, bf16[192,512]{1,0:T(8,128)(2,1)}, u32[]{:S(2)}) copy-start(bf16[192,512]{1,0:T(8,128)(2,1)} %copy-done.28) | copy-start | bytes 589828
  178.9 19.4 %all-to-all-start.6 = ((bf16[16,80,320]{2,1,0:T(8,128)(2,1)}), bf16[16,80,320]{2,1,0:T(8,128)(2,1)S(1)}, u32[]{:S(2)}, u32[]{:S(2)}) async-start(bf16[16,80,320]{2,1,0:T(8,128)(2,1)} %get-tuple-element.106), calls=%async_computation.6 | async-start | bytes 1966080 | tf_op jit(solution)/shard_map/all_to_all | solution.py:468
  182.7 48.5 %copy-start.31 = (bf16[320,64]{0,1:T(8,128)(2,1)S(1)}, bf16[320,64]{0,1:T(8,128)(2,1)}, u32[]{:S(2)}) copy-start(bf16[320,64]{0,1:T(8,128)(2,1)} %param.22) | copy-start | bytes 122884
  182.7 48.5 %copy-start.32 = (bf16[320,64]{0,1:T(8,128)(2,1)S(1)}, bf16[320,64]{0,1:T(8,128)(2,1)}, u32[]{:S(2)}) copy-start(bf16[320,64]{0,1:T(8,128)(2,1)} %param.21) | copy-start | bytes 122884
  182.7 3.7 %collective-permute-start.9 = (bf16[16,32,128]{2,1,0:T(8,128)(2,1)S(1)}, bf16[16,32,128]{2,1,0:T(8,128)(2,1)S(1)}, u32[]{:S(2)}, u32[]{:S(2)}) collective-permute-start(bf16[16,32,128]{2,1,0:T(8,128)(2,1)S(1)} %copy-done.35), channel_id=1, source_target_pairs={{0,16},{16,0},{1,17},{17,1},{2,18},{18,2},{3,19},{19,3},{4,20},{20... | collective-permute-start | bytes 393224 | tf_op jit(solution)/shard_map/ppermute | solution.py:469
  186.4 1.3 collective-permute-start.10
  198.3 34.8 %all-to-all-start.7 = ((bf16[16,32,128]{2,1,0:T(8,128)(2,1)}), bf16[16,32,128]{2,1,0:T(8,128)(2,1)S(1)}, u32[]{:S(2)}, u32[]{:S(2)}) async-start(bf16[16,32,128]{2,1,0:T(8,128)(2,1)} %collective-permute-done.10), calls=%async_computation.7 | async-start | bytes 262144 | tf_op jit(solution)/shard_map/all_to_all | solution.py:488
  225.7 5.5 %collective-permute-start.11 = (f32[64,128]{1,0:T(8,128)S(1)}, f32[64,128]{1,0:T(8,128)S(1)}, u32[]{:S(2)}, u32[]{:S(2)}) collective-permute-start(f32[64,128]{1,0:T(8,128)S(1)} %get-tuple-element.113), channel_id=1, source_target_pairs={{16,0},{32,16},{48,32},{64,48},{80,64},{96,80},{112,96},{128,112},... | collective-permute-start | bytes 98312 | tf_op jit(solution)/shard_map/ppermute | solution.py:500
  (31 other events, 230.6 us)

commit v4 on v3

--- a/solution.py
+++ b/solution.py
@@ -140,30 +140,6 @@
             out[k * 64 : k * 64 + 64, 128:512] = r_ref[256:320, 128:512]
 
 
-def prep_kernel(q0, q1, q2, q3, act_ref, h_ref, n_ref, stats_ref):
-    qs = (q0, q1, q2, q3)
-    tokens = stats_ref.shape[1]
-    channels = SIDE * q0.shape[0]
-    conv = [q[:, 128 : 128 + tokens].astype(F32) for q in qs]
-    mean = sum(jnp.sum(v, axis=0, keepdims=True) for v in conv) / channels
-    off = [v - mean for v in conv]
-    var = sum(jnp.sum(v * v, axis=0, keepdims=True) for v in off) / channels
-    inv = lax.rsqrt(var + NORM_EPS)
-    stats_ref[0:1, :] = mean
-    stats_ref[1:2, :] = inv
-    lane = lax.broadcasted_iota(jnp.int32, (q0.shape[0], 128), 1)
-    for j, q in enumerate(qs):
-        pieces = jnp.where((lane >= 64) & (lane < 67), q[:, 384:512].astype(F32), 0.0)
-        gain = jnp.sum(pieces, axis=1, keepdims=True)
-        normed = off[j] * inv
-        linear = normed * gain
-        s = jax.nn.sigmoid(linear)
-        slope = s * (1.0 + linear * (1.0 - s)) * gain
-        act_ref[j] = (linear * s).astype(BF)
-        h_ref[j] = slope.astype(BF)
-        n_ref[j] = (slope * normed).astype(BF)
-
-
 def merge_kernel(at_ref, s0, s1, s2, s3, g_ref, u_ref, d_ref):
     for k, s_ref in enumerate((s0, s1, s2, s3)):
         for a in range(SIDE):
@@ -226,20 +202,49 @@
 
 
 def tail_kernel(
-    at_ref, p_ref, r_ref, c_ref, q0, q1, q2, q3, act_ref, h_ref, n_ref, o_ref, mine_ref, other_ref
+    at_ref, p_ref, r_ref, c_ref, q0, q1, q2, q3, o_ref, mine_ref, other_ref, stats_ref, held, sem
 ):
+    copies = [
+        pltpu.make_async_copy(q, held.at[j], sem.at[j]) for j, q in enumerate((q0, q1, q2, q3))
+    ]
+    for copy in copies:
+        copy.start()
     moe = mm(p_ref[...], r_ref[...], TN)
     total = (c_ref[...].astype(F32) + moe).astype(BF)
     tokens = total.shape[0]
+    size = held.shape[1]
+    channels = SIDE * size
+    for copy in copies:
+        copy.wait()
+    mean = jnp.zeros((1, tokens), F32)
+    for j in range(SIDE):
+        conv = held[j, :, 128 : 128 + tokens].astype(F32)
+        mean = mean + jnp.sum(conv, axis=0, keepdims=True)
+    mean = mean / channels
+    var = jnp.zeros((1, tokens), F32)
+    for j in range(SIDE):
+        off = held[j, :, 128 : 128 + tokens].astype(F32) - mean
+        var = var + jnp.sum(off * off, axis=0, keepdims=True)
+    inv = lax.rsqrt(var / channels + NORM_EPS)
+    stats_ref[0:1, :] = mean
+    stats_ref[1:2, :] = inv
     first = jnp.zeros((1, tokens), F32)
     second = jnp.zeros((1, tokens), F32)
     own = jnp.full((32, 128), at_ref[2], jnp.int32) == 0
     low = lax.broadcasted_iota(jnp.int32, (32, 128), 1) < 64
-    for j, q in enumerate((q0, q1, q2, q3)):
-        cot = mm(q[:, 0:128], total, NT)
-        first = first + jnp.sum(cot * h_ref[j].astype(F32), axis=0, keepdims=True)
-        second = second + jnp.sum(cot * n_ref[j].astype(F32), axis=0, keepdims=True)
-        grad = mm(act_ref[j], total, NN)
+    lane = lax.broadcasted_iota(jnp.int32, (size, 128), 1)
+    for j in range(SIDE):
+        pieces = jnp.where((lane >= 64) & (lane < 67), held[j, :, 384:512].astype(F32), 0.0)
+        gain = jnp.sum(pieces, axis=1, keepdims=True)
+        normed = (held[j, :, 128 : 128 + tokens].astype(F32) - mean) * inv
+        linear = normed * gain
+        s = jax.nn.sigmoid(linear)
+        act = (linear * s).astype(BF)
+        cot = mm(held[j, :, 0:128], total, NT)
+        sloped = cot * (s * (1.0 + linear * (1.0 - s)) * gain)
+        first = first + jnp.sum(sloped, axis=0, keepdims=True)
+        second = second + jnp.sum(sloped * normed, axis=0, keepdims=True)
+        grad = mm(act, total, NN)
         turned = pltpu.roll(grad, 64, 1)
         for k in range(SIDE):
             b = at_ref[48 + j * SIDE + k]
@@ -274,6 +279,15 @@
     cot = inv * (cot - first - normed * second)
     o_ref[...] = cot
     h_ref[...] = cot[:, 0:128]
+
+
+def sum_kernel(a_ref, o_ref):
+    total = a_ref[0].astype(F32)
+    for b in range(1, a_ref.shape[0]):
+        total = total + a_ref[b].astype(F32)
+    turned = pltpu.roll(total, 64, 1)
+    block = jnp.concatenate([total, turned], axis=0)
+    o_ref[...] = block.T[0:64, :].astype(BF)
 
 
 def add_kernel(a_ref, b_ref, o_ref):
@@ -367,20 +381,9 @@
         name="split_weights",
     )(at, gate_weight[0], up_weight[0], down_weight[0], proj_weight, channel_part)
     weights = pass_on(split, unit_groups)
-    relay = pl.pallas_call(
-        relay_kernel,
-        out_shape=(whole((256, 512), BF),) * SIDE,
-        in_specs=[smem] + [vmem] * SIDE,
-        out_specs=(vmem,) * SIDE,
-        compiler_params=room,
-        cost_estimate=cost(1000000, 2000000),
-        name="relay",
-    )(at, *weights)
-    relay = pass_on(relay, feature_groups)
-
     got = lax.all_to_all(sent.reshape(sp_count, SLOT, 256), SP, 0, 0, tiled=True)
     got = got.reshape(slots, 256)
-    got, weights, relay = lax.optimization_barrier((got, weights, relay))
+    got, weights = lax.optimization_barrier((got, weights))
     taps_t = conv_taps.T
 
     rows = exchange(jnp.broadcast_to(got[None], (SIDE, slots, 256)), feature_groups)
@@ -397,18 +400,6 @@
         name="pre",
     )(at, rows, *weights)
     pre = exchange(pre, unit_groups)
-    act, slope, slope_normed, stats = pl.pallas_call(
-        prep_kernel,
-        out_shape=(whole((SIDE, 256, tokens), BF),) * 3 + (whole((2, tokens), F32),),
-        in_specs=[vmem] * SIDE,
-        out_specs=(vmem,) * 4,
-        compiler_params=room,
-        cost_estimate=cost(20000000, 3000000),
-        name="prep",
-    )(*relay)
-    pre, act, slope, slope_normed, stats = lax.optimization_barrier(
-        (pre, act, slope, slope_normed, stats)
-    )
     hidden = pl.pallas_call(
         gate_kernel,
         grid=(slots // step,),
@@ -433,6 +424,17 @@
     )(at, hidden, *weights)
     part = exchange(part, feature_groups)
     back = jnp.sum(part.astype(F32), axis=0).astype(BF).reshape(sp_count, SLOT, 128)
+    back, weights = lax.optimization_barrier((back, weights))
+    relay = pl.pallas_call(
+        relay_kernel,
+        out_shape=(whole((256, 512), BF),) * SIDE,
+        in_specs=[smem] + [vmem] * SIDE,
+        out_specs=(vmem,) * SIDE,
+        compiler_params=room,
+        cost_estimate=cost(1000000, 2000000),
+        name="relay",
+    )(at, *weights)
+    relay = pass_on(relay, feature_groups)
     returned = lax.all_to_all(back, SP, 0, 0, tiled=True).reshape(slots, 128)
 
     grads = pl.pallas_call(
@@ -449,22 +451,23 @@
         cost_estimate=cost(800000000, 4400000),
         name="grads",
     )(at, hidden, rows)
-    grads = pass_on(grads, unit_groups)
     returned, grads = lax.optimization_barrier((returned, grads))
 
-    act_part, mine, other = pl.pallas_call(
+    act_part, mine, other, stats = pl.pallas_call(
         tail_kernel,
         out_shape=(
             whole((tp_count, 80, tokens), BF),
             whole((tp_count, 32, 128), BF),
             whole((tp_count, 32, 128), BF),
+            whole((2, tokens), F32),
         ),
-        in_specs=[smem] + [vmem] * 10,
-        out_specs=(vmem,) * 3,
+        in_specs=[smem] + [vmem] * 3 + [pl.BlockSpec(memory_space=pltpu.HBM)] * SIDE,
+        out_specs=(vmem,) * 4,
+        scratch_shapes=[VM((SIDE, 256, 512), BF), pltpu.SemaphoreType.DMA((SIDE,))],
         compiler_params=room,
         cost_estimate=cost(250000000, 4500000),
         name="tail",
-    )(at, pick, returned, out_cotangent, *relay, act, slope, slope_normed)
+    )(at, pick, returned, out_cotangent, *relay)
     act_part = lax.all_to_all(act_part, TP, 0, 0, tiled=True)
     other = lax.ppermute(other, "c", [(0, 1), (1, 0)])
     proj_part = pl.pallas_call(
@@ -476,6 +479,18 @@
         cost_estimate=cost(100000, 400000),
         name="add_core",
     )(mine, other)
+    act_part, proj_part, grads = lax.optimization_barrier((act_part, proj_part, grads))
+    grads = pass_on(grads, unit_groups)
+    proj_part = lax.all_to_all(proj_part, "z", 0, 0, tiled=True)
+    proj_sum = pl.pallas_call(
+        sum_kernel,
+        out_shape=whole((64, 64), BF),
+        in_specs=[vmem],
+        out_specs=vmem,
+        compiler_params=room,
+        cost_estimate=cost(100000, 200000),
+        name="sum_planes",
+    )(proj_part)
     side = SIDE * SIDE
     swap = [
         (z * 2 * side + c * side + t, t * 2 * side + c * side + z)
@@ -483,9 +498,7 @@
         for c in range(2)
         for t in range(side)
     ]
-    proj_part = lax.ppermute(proj_part, ("z",) + PLANE, swap)
-    act_part, proj_part = lax.optimization_barrier((act_part, proj_part))
-    proj_part = lax.all_to_all(proj_part, TP, 0, 0, tiled=True)
+    grad_proj = lax.ppermute(proj_sum, ("z",) + PLANE, swap).astype(F32)
 
     conv_cot, head = pl.pallas_call(
         head_kernel,
@@ -508,9 +521,6 @@
         cost_estimate=cost(4000000, 400000),
         name="conv",
     )(conv_cot, after, taps_t, glu_gate.T, glu_value.T)
-
-    total = jnp.sum(proj_part.astype(F32), axis=0)
-    grad_proj = jnp.concatenate([total[:, 0:64], total[:, 64:128]], axis=0).T
 
     grad_gate, grad_up, grad_down = pl.pallas_call(
         merge_kernel,

time: 235 us -> 222 us (0.945)
  the two profiles are of different devices: /device:TPU:1 before, /device:TPU:16 now
where the time goes in v4:
time: 222 us; the launch traced here: 221 us
  starting transfers between devices  81.5 us (37%)
  blocking collectives  66.4 us (30%)
  waiting for transfers between devices  38 us (17%)
  Pallas kernels  25.2 us (11%)
  local copies, waits for them, and re-layouts  5.98 us (3%)
  other arithmetic  2.78 us (1%)
    all_to_all x4, blocking collectives, exchange(): return lax.all_to_all(v, PLANE, 0, 0, axis_index_groups=groups, tiled=True)  66.4 us
    ppermute x9, starting transfers between devices, pass_on(): lax.ppermute(parts[k], PLANE, steps_ahead(groups, k))  31.9 us
    all_to_all x1, starting transfers between devices, body(): lax.all_to_all(sent.reshape(sp_count, SLOT, 256), SP, 0, 0, tiled=True)  15.6 us
    all_to_all x1, waiting for transfers between devices, body(): lax.all_to_all(sent.reshape(sp_count, SLOT, 256), SP, 0, 0, tiled=True)  14.7 us
    ppermute x1, starting transfers between devices, body(): grad_proj = lax.ppermute(proj_sum, ('z',) + PLANE, swap).astype(F32)  12.1 us
    all_to_all x1, waiting for transfers between devices, body(): act_part = lax.all_to_all(act_part, TP, 0, 0, tiled=True)  9.53 us
    all_to_all x1, starting transfers between devices, body(): proj_part = lax.all_to_all(proj_part, 'z', 0, 0, tiled=True)  7.62 us
    all_to_all x1, starting transfers between devices, body(): act_part = lax.all_to_all(act_part, TP, 0, 0, tiled=True)  6.33 us
  transfers between devices with their start and end apart: 16, of which 8 were waited for; matrix products, arithmetic and copies ran while one was open for 1% of the time, Pallas kernels for 5%

profile of v4, /device:TPU:16, one launch (start us, length us, event | category | flops | bytes accessed | tf_op | source)
XLA Modules:
  0.0 220.9 jit_solution(18228314191730277338)
XLA Ops:
  3.6 15.6 %all-to-all-start = ((bf16[32,32,256]{2,1,0:T(8,128)(2,1)}), bf16[32,32,256]{2,1,0:T(8,128)(2,1)}, u32[]{:S(2)}, u32[]{:S(2)}) async-start(bf16[32,32,256]{2,1,0:T(8,128)(2,1)} %bitcast.36), calls=%async_computation | async-start | bytes 1048576 | tf_op jit(solution)/shard_map/all_to_all | solution.py:384
  21.3 3.4 %collective-permute-start = (bf16[320,512]{1,0:T(8,128)(2,1)S(1)}, bf16[320,512]{1,0:T(8,128)(2,1)S(1)}, u32[]{:S(2)}, u32[]{:S(2)}) collective-permute-start(bf16[320,512]{1,0:T(8,128)(2,1)S(1)} %get-tuple-element.67), channel_id=1, source_target_pairs={{0,1},{1,2},{2,3},{3,0},{4,5},{5,6},{6,7},{7,4},{8,9},{9,10},{10,1... | collective-permute-start | bytes 983048 | tf_op jit(solution)/shard_map/ppermute | solution.py:70
  24.7 4.6 %collective-permute-start.1 = (bf16[320,512]{1,0:T(8,128)(2,1)S(1)}, bf16[320,512]{1,0:T(8,128)(2,1)S(1)}, u32[]{:S(2)}, u32[]{:S(2)}) collective-permute-start(bf16[320,512]{1,0:T(8,128)(2,1)S(1)} %get-tuple-element.68), channel_id=1, source_target_pairs={{0,2},{1,3},{2,0},{3,1},{4,6},{5,7},{6,4},{7,5},{8,10},{9,11},{10,... | collective-permute-start | bytes 983048 | tf_op jit(solution)/shard_map/ppermute | solution.py:70
  29.3 3.3 %collective-permute-start.2 = (bf16[320,512]{1,0:T(8,128)(2,1)S(1)}, bf16[320,512]{1,0:T(8,128)(2,1)S(1)}, u32[]{:S(2)}, u32[]{:S(2)}) collective-permute-start(bf16[320,512]{1,0:T(8,128)(2,1)S(1)} %get-tuple-element.69), channel_id=1, source_target_pairs={{0,3},{1,0},{2,1},{3,2},{4,7},{5,4},{6,5},{7,6},{8,11},{9,8},{10,9... | collective-permute-start | bytes 983048 | tf_op jit(solution)/shard_map/ppermute | solution.py:70
  32.7 3.3 %collective-permute-done.1.w2.r2 = bf16[320,512]{1,0:T(8,128)(2,1)S(1)} collective-permute-done((bf16[320,512]{1,0:T(8,128)(2,1)S(1)}, bf16[320,512]{1,0:T(8,128)(2,1)S(1)}, u32[]{:S(2)}, u32[]{:S(2)}) %collective-permute-start.1) | collective-permute-done | bytes 327712 | tf_op jit(solution)/shard_map/ppermute | solution.py:70
  38.3 14.7 %all-to-all-done = bf16[32,32,256]{2,1,0:T(8,128)(2,1)} async-done(((bf16[32,32,256]{2,1,0:T(8,128)(2,1)}), bf16[32,32,256]{2,1,0:T(8,128)(2,1)}, u32[]{:S(2)}, u32[]{:S(2)}) %all-to-all-start) | async-done | bytes 524320 | tf_op jit(solution)/shard_map/all_to_all | solution.py:384
  54.2 18.4 %all_to_all.40.a_ref = bf16[4,1024,256]{2,1,0:T(8,128)(2,1)S(1)} all-to-all(bf16[4,1024,256]{2,1,0:T(8,128)(2,1)S(1)} %broadcast_in_dim.23), channel_id=1, replica_groups={{0,4,8,12},{1,5,9,13},{2,6,10,14},{3,7,11,15},{16,17,18,19},{20,21,22,2..., dimensions={0} | all-to-all | bytes 4194304 | tf_op jit(solution)/shard_map/all_to_all | solution.py:79
  72.6 4.0 %pre.1 = bf16[4,192,1024]{2,1,0:T(8,128)(2,1)S(1)} custom-call(s32[64]{0:T(128)S(1)} %dynamic-slice_bitcast_fusion.at_ref, bf16[4,1024,256]{2,1,0:T(8,128)(2,1)S(1)} %all_to_all.40.a_ref, bf16[320,512]{1,0:T(8,128)(2,1)S(1)} %get-tuple-element.81.w0.r0, bf16[320,512]{1,0:T(8,128)(2,1)S(1)} %collective-permute-done.w1.r1, ...), custom_call_target="tpu_custom_call" | custom-call | flops 800000000 | bytes 4400000 | tf_op jit(solution)/shard_map/pre/pallas_call | solution.py:391
  76.6 17.8 %all_to_all.41.p_ref = bf16[4,192,1024]{2,1,0:T(8,128)(2,1)S(1)} all-to-all(bf16[4,192,1024]{2,1,0:T(8,128)(2,1)S(1)} %pre.1), channel_id=1, replica_groups={{0,1,2,3},{4,5,6,7},{8,9,10,11},{12,13,14,15},{16,20,24,28},{17,21,25,2..., dimensions={0} | all-to-all | bytes 3145728 | tf_op jit(solution)/shard_map/all_to_all | solution.py:79
  95.2 16.1 %all_to_all.42.h_ref = bf16[4,192,1024]{2,1,0:T(8,128)(2,1)S(1)} all-to-all(bf16[4,192,1024]{2,1,0:T(8,128)(2,1)S(1)} %gates.1), channel_id=1, replica_groups={{0,1,2,3},{4,5,6,7},{8,9,10,11},{12,13,14,15},{16,20,24,28},{17,21,25,2..., dimensions={0} | all-to-all | bytes 3145728 | tf_op jit(solution)/shard_map/all_to_all | solution.py:79
  113.5 14.1 %all_to_all.43 = bf16[4,1024,128]{2,1,0:T(8,128)(2,1)} all-to-all(bf16[4,1024,128]{2,1,0:T(8,128)(2,1)S(1)} %partial.1), channel_id=1, replica_groups={{0,4,8,12},{1,5,9,13},{2,6,10,14},{3,7,11,15},{16,17,18,19},{20,21,22,2..., dimensions={0} | all-to-all | bytes 2097152 | tf_op jit(solution)/shard_map/all_to_all | solution.py:79
  129.7 4.6 %all-to-all-start.5 = ((bf16[32,32,128]{2,1,0:T(8,128)(2,1)}), bf16[32,32,128]{2,1,0:T(8,128)(2,1)}, u32[]{:S(2)}, u32[]{:S(2)}) async-start(bf16[32,32,128]{2,1,0:T(8,128)(2,1)} %bitcast.35), calls=%async_computation.5 | async-start | bytes 524288 | tf_op jit(solution)/shard_map/all_to_all | solution.py:438
  136.5 3.7 %collective-permute-start.3 = (bf16[256,512]{1,0:T(8,128)(2,1)}, bf16[256,512]{1,0:T(8,128)(2,1)S(1)}, u32[]{:S(2)}, u32[]{:S(2)}) collective-permute-start(bf16[256,512]{1,0:T(8,128)(2,1)} %get-tuple-element.86), channel_id=1, source_target_pairs={{0,4},{4,8},{8,12},{12,0},{1,5},{5,9},{9,13},{13,1},{2,6},{6,10},{... | collective-permute-start | bytes 786440 | tf_op jit(solution)/shard_map/ppermute | solution.py:70
  140.2 3.4 %collective-permute-start.4 = (bf16[256,512]{1,0:T(8,128)(2,1)}, bf16[256,512]{1,0:T(8,128)(2,1)}, u32[]{:S(2)}, u32[]{:S(2)}) collective-permute-start(bf16[256,512]{1,0:T(8,128)(2,1)} %get-tuple-element.87), channel_id=1, source_target_pairs={{0,8},{4,12},{8,0},{12,4},{1,9},{5,13},{9,1},{13,5},{2,10},{6,14},... | collective-permute-start | bytes 786440 | tf_op jit(solution)/shard_map/ppermute | solution.py:70
  143.6 4.0 %collective-permute-start.5 = (bf16[256,512]{1,0:T(8,128)(2,1)}, bf16[256,512]{1,0:T(8,128)(2,1)}, u32[]{:S(2)}, u32[]{:S(2)}) collective-permute-start(bf16[256,512]{1,0:T(8,128)(2,1)} %get-tuple-element.88), channel_id=1, source_target_pairs={{0,12},{4,0},{8,4},{12,8},{1,13},{5,1},{9,5},{13,9},{2,14},{6,2},{... | collective-permute-start | bytes 786440 | tf_op jit(solution)/shard_map/ppermute | solution.py:70
  147.9 3.1 %grads.1 = (bf16[192,512]{1,0:T(8,128)(2,1)S(1)}, bf16[192,512]{1,0:T(8,128)(2,1)S(1)}, bf16[192,512]{1,0:T(8,128)(2,1)S(1)}, bf16[192,512]{1,0:T(8,128)(2,1)S(1)}) custom-call(s32[64]{0:T(128)S(1)} %dynamic-slice_bitcast_fusion.at_ref, bf16[4,192,1024]{2,1,0:T(8,128)(2,1)S(1)} %copy-done.1, bf16[4,1024,256]{2,1,0:T(8,128)(2,1)S(1)} %all_to_all.40.a_ref), custom_call_target="tpu_custom_call" | custom-call | flops 800000000 | bytes 4400000 | tf_op jit(solution)/shard_map/grads/pallas_call | solution.py:440
  153.7 3.4 %all-to-all-done.5 = bf16[32,32,128]{2,1,0:T(8,128)(2,1)} async-done(((bf16[32,32,128]{2,1,0:T(8,128)(2,1)}), bf16[32,32,128]{2,1,0:T(8,128)(2,1)}, u32[]{:S(2)}, u32[]{:S(2)}) %all-to-all-start.5) | async-done | bytes 262176 | tf_op jit(solution)/shard_map/all_to_all | solution.py:438
  157.1 4.8 %tail.1 = (bf16[16,80,320]{2,1,0:T(8,128)(2,1)}, bf16[16,32,128]{2,1,0:T(8,128)(2,1)S(1)}, bf16[16,32,128]{2,1,0:T(8,128)(2,1)S(1)}, f32[2,320]{1,0:T(2,128)S(1)}) custom-call(s32[64]{0:T(128)S(1)} %dynamic-slice_bitcast_fusion.at_ref, bf16[1024,320]{1,0:T(8,128)(2,1)S(1)} %pick.1.p_ref, bf16[1024,128]{1,0:T(8,128)(2,1)} %bitcast.13.r_ref, ...), custom_call_target="tpu_custom_call" | custom-call | flops 250000000 | bytes 4500000 | tf_op jit(solution)/shard_map/tail/pallas_call | solution.py:456
  162.0 6.3 %all-to-all-start.6 = ((bf16[16,80,320]{2,1,0:T(8,128)(2,1)}), bf16[16,80,320]{2,1,0:T(8,128)(2,1)S(1)}, u32[]{:S(2)}, u32[]{:S(2)}) async-start(bf16[16,80,320]{2,1,0:T(8,128)(2,1)} %get-tuple-element.89), calls=%async_computation.6 | async-start | bytes 1966080 | tf_op jit(solution)/shard_map/all_to_all | solution.py:471
  172.4 9.5 %all-to-all-done.6.r_ref = bf16[16,80,320]{2,1,0:T(8,128)(2,1)S(1)} async-done(((bf16[16,80,320]{2,1,0:T(8,128)(2,1)}), bf16[16,80,320]{2,1,0:T(8,128)(2,1)S(1)}, u32[]{:S(2)}, u32[]{:S(2)}) %all-to-all-start.6) | async-done | bytes 819232 | tf_op jit(solution)/shard_map/all_to_all | solution.py:471
  182.0 7.6 %all-to-all-start.7 = ((bf16[16,32,128]{2,1,0:T(8,128)(2,1)}), bf16[16,32,128]{2,1,0:T(8,128)(2,1)S(1)}, u32[]{:S(2)}, u32[]{:S(2)}) async-start(bf16[16,32,128]{2,1,0:T(8,128)(2,1)} %add_core.1), calls=%async_computation.7 | async-start | bytes 262144 | tf_op jit(solution)/shard_map/all_to_all | solution.py:484
  191.8 4.1 %collective-permute-start.8 = (bf16[192,512]{1,0:T(8,128)(2,1)S(1)}, bf16[192,512]{1,0:T(8,128)(2,1)S(1)}, u32[]{:S(2)}, u32[]{:S(2)}) collective-permute-start(bf16[192,512]{1,0:T(8,128)(2,1)S(1)} %copy-done.18), channel_id=1, source_target_pairs={{0,2},{1,3},{2,0},{3,1},{4,6},{5,7},{6,4},{7,5},{8,10},{9,11},{10,... | collective-permute-start | bytes 589832 | tf_op jit(solution)/shard_map/ppermute | solution.py:70
  196.0 3.2 %collective-permute-start.9 = (bf16[192,512]{1,0:T(8,128)(2,1)S(1)}, bf16[192,512]{1,0:T(8,128)(2,1)S(1)}, u32[]{:S(2)}, u32[]{:S(2)}) collective-permute-start(bf16[192,512]{1,0:T(8,128)(2,1)S(1)} %copy-done.16), channel_id=1, source_target_pairs={{0,3},{1,0},{2,1},{3,2},{4,7},{5,4},{6,5},{7,6},{8,11},{9,8},{10,9... | collective-permute-start | bytes 589832 | tf_op jit(solution)/shard_map/ppermute | solution.py:70
  203.6 12.1 %collective-permute-start.10 = (bf16[64,64]{1,0:T(8,128)(2,1)S(1)}, bf16[64,64]{1,0:T(8,128)(2,1)S(1)}, u32[]{:S(2)}, u32[]{:S(2)}) collective-permute-start(bf16[64,64]{1,0:T(8,128)(2,1)S(1)} %sum_planes.1), channel_id=1, source_target_pairs={{0,0},{1,32},{2,64},{3,96},{4,128},{5,160},{6,192},{7,224},{8,256}... | collective-permute-start | bytes 24584 | tf_op jit(solution)/shard_map/ppermute | solution.py:501
  (85 shorter events, 34.6 us)
Async XLA Ops:
  3.6 49.4 %all-to-all-start = ((bf16[32,32,256]{2,1,0:T(8,128)(2,1)}), bf16[32,32,256]{2,1,0:T(8,128)(2,1)}, u32[]{:S(2)}, u32[]{:S(2)}) async-start(bf16[32,32,256]{2,1,0:T(8,128)(2,1)} %bitcast.36), calls=%async_computation | async-start | bytes 1048576 | tf_op jit(solution)/shard_map/all_to_all | solution.py:384
  21.3 11.4 %collective-permute-start = (bf16[320,512]{1,0:T(8,128)(2,1)S(1)}, bf16[320,512]{1,0:T(8,128)(2,1)S(1)}, u32[]{:S(2)}, u32[]{:S(2)}) collective-permute-start(bf16[320,512]{1,0:T(8,128)(2,1)S(1)} %get-tuple-element.67), channel_id=1, source_target_pairs={{0,1},{1,2},{2,3},{3,0},{4,5},{5,6},{6,7},{7,4},{8,9},{9,10},{10,1... | collective-permute-start | bytes 983048 | tf_op jit(solution)/shard_map/ppermute | solution.py:70
  24.7 11.3 %collective-permute-start.1 = (bf16[320,512]{1,0:T(8,128)(2,1)S(1)}, bf16[320,512]{1,0:T(8,128)(2,1)S(1)}, u32[]{:S(2)}, u32[]{:S(2)}) collective-permute-start(bf16[320,512]{1,0:T(8,128)(2,1)S(1)} %get-tuple-element.68), channel_id=1, source_target_pairs={{0,2},{1,3},{2,0},{3,1},{4,6},{5,7},{6,4},{7,5},{8,10},{9,11},{10,... | collective-permute-start | bytes 983048 | tf_op jit(solution)/shard_map/ppermute | solution.py:70
  29.3 9.0 %collective-permute-start.2 = (bf16[320,512]{1,0:T(8,128)(2,1)S(1)}, bf16[320,512]{1,0:T(8,128)(2,1)S(1)}, u32[]{:S(2)}, u32[]{:S(2)}) collective-permute-start(bf16[320,512]{1,0:T(8,128)(2,1)S(1)} %get-tuple-element.69), channel_id=1, source_target_pairs={{0,3},{1,0},{2,1},{3,2},{4,7},{5,4},{6,5},{7,6},{8,11},{9,8},{10,9... | collective-permute-start | bytes 983048 | tf_op jit(solution)/shard_map/ppermute | solution.py:70
  127.6 20.0 %copy-start.14 = (s32[2,320]{1,0:T(2,128)S(1)}, s32[2,320]{1,0:T(2,128)}, u32[]{:S(2)}) copy-start(s32[2,320]{1,0:T(2,128)} %get-tuple-element.61.t_ref) | copy-start | bytes 7684
  129.7 27.4 %all-to-all-start.5 = ((bf16[32,32,128]{2,1,0:T(8,128)(2,1)}), bf16[32,32,128]{2,1,0:T(8,128)(2,1)}, u32[]{:S(2)}, u32[]{:S(2)}) async-start(bf16[32,32,128]{2,1,0:T(8,128)(2,1)} %bitcast.35), calls=%async_computation.5 | async-start | bytes 524288 | tf_op jit(solution)/shard_map/all_to_all | solution.py:438
  136.5 20.6 %collective-permute-start.3 = (bf16[256,512]{1,0:T(8,128)(2,1)}, bf16[256,512]{1,0:T(8,128)(2,1)S(1)}, u32[]{:S(2)}, u32[]{:S(2)}) collective-permute-start(bf16[256,512]{1,0:T(8,128)(2,1)} %get-tuple-element.86), channel_id=1, source_target_pairs={{0,4},{4,8},{8,12},{12,0},{1,5},{5,9},{9,13},{13,1},{2,6},{6,10},{... | collective-permute-start | bytes 786440 | tf_op jit(solution)/shard_map/ppermute | solution.py:70
  140.2 16.9 %collective-permute-start.4 = (bf16[256,512]{1,0:T(8,128)(2,1)}, bf16[256,512]{1,0:T(8,128)(2,1)}, u32[]{:S(2)}, u32[]{:S(2)}) collective-permute-start(bf16[256,512]{1,0:T(8,128)(2,1)} %get-tuple-element.87), channel_id=1, source_target_pairs={{0,8},{4,12},{8,0},{12,4},{1,9},{5,13},{9,1},{13,5},{2,10},{6,14},... | collective-permute-start | bytes 786440 | tf_op jit(solution)/shard_map/ppermute | solution.py:70
  143.6 13.5 %collective-permute-start.5 = (bf16[256,512]{1,0:T(8,128)(2,1)}, bf16[256,512]{1,0:T(8,128)(2,1)}, u32[]{:S(2)}, u32[]{:S(2)}) collective-permute-start(bf16[256,512]{1,0:T(8,128)(2,1)} %get-tuple-element.88), channel_id=1, source_target_pairs={{0,12},{4,0},{8,4},{12,8},{1,13},{5,1},{9,5},{13,9},{2,14},{6,2},{... | collective-permute-start | bytes 786440 | tf_op jit(solution)/shard_map/ppermute | solution.py:70
  162.0 27.6 %copy-start.20 = (bf16[192,512]{1,0:T(8,128)(2,1)S(1)}, bf16[192,512]{1,0:T(8,128)(2,1)}, u32[]{:S(2)}) copy-start(bf16[192,512]{1,0:T(8,128)(2,1)} %copy-done.19) | copy-start | bytes 589828
  162.0 29.8 %copy-start.18 = (bf16[192,512]{1,0:T(8,128)(2,1)S(1)}, bf16[192,512]{1,0:T(8,128)(2,1)}, u32[]{:S(2)}) copy-start(bf16[192,512]{1,0:T(8,128)(2,1)} %copy-done.17) | copy-start | bytes 589828
  162.0 34.0 %copy-start.16 = (bf16[192,512]{1,0:T(8,128)(2,1)S(1)}, bf16[192,512]{1,0:T(8,128)(2,1)}, u32[]{:S(2)}) copy-start(bf16[192,512]{1,0:T(8,128)(2,1)} %copy-done.15) | copy-start | bytes 589828
  162.0 53.7 %copy-start.21 = (f32[31,64]{1,0:T(8,128)S(1)}, f32[31,64]{1,0:T(8,128)}, u32[]{:S(2)}) copy-start(f32[31,64]{1,0:T(8,128)} %param.24) | copy-start | bytes 23812
  162.0 53.8 %copy-start.12 = (bf16[320,64]{0,1:T(8,128)(2,1)S(1)}, bf16[320,64]{0,1:T(8,128)(2,1)}, u32[]{:S(2)}) copy-start(bf16[320,64]{0,1:T(8,128)(2,1)} %param.22) | copy-start | bytes 122884
  162.0 53.8 %copy-start.13 = (bf16[320,64]{0,1:T(8,128)(2,1)S(1)}, bf16[320,64]{0,1:T(8,128)(2,1)}, u32[]{:S(2)}) copy-start(bf16[320,64]{0,1:T(8,128)(2,1)} %param.21) | copy-start | bytes 122884
  162.0 19.9 %all-to-all-start.6 = ((bf16[16,80,320]{2,1,0:T(8,128)(2,1)}), bf16[16,80,320]{2,1,0:T(8,128)(2,1)S(1)}, u32[]{:S(2)}, u32[]{:S(2)}) async-start(bf16[16,80,320]{2,1,0:T(8,128)(2,1)} %get-tuple-element.89), calls=%async_computation.6 | async-start | bytes 1966080 | tf_op jit(solution)/shard_map/all_to_all | solution.py:471
  168.4 49.3 %copy-start.10 = (bf16[192,512]{1,0:T(8,128)(2,1)S(1)}, bf16[192,512]{1,0:T(8,128)(2,1)}, u32[]{:S(2)}) copy-start(bf16[192,512]{1,0:T(8,128)(2,1)} %copy-done.9) | copy-start | bytes 589828
  168.4 3.4 %collective-permute-start.6 = (bf16[16,32,128]{2,1,0:T(8,128)(2,1)S(1)}, bf16[16,32,128]{2,1,0:T(8,128)(2,1)S(1)}, u32[]{:S(2)}, u32[]{:S(2)}) collective-permute-start(bf16[16,32,128]{2,1,0:T(8,128)(2,1)S(1)} %get-tuple-element.91), channel_id=1, source_target_pairs={{0,16},{16,0},{1,17},{17,1},{2,18},{18,2},{3,19},{19,3},{4,20},{20... | collective-permute-start | bytes 393224 | tf_op jit(solution)/shard_map/ppermute | solution.py:472
  182.0 21.4 %all-to-all-start.7 = ((bf16[16,32,128]{2,1,0:T(8,128)(2,1)}), bf16[16,32,128]{2,1,0:T(8,128)(2,1)S(1)}, u32[]{:S(2)}, u32[]{:S(2)}) async-start(bf16[16,32,128]{2,1,0:T(8,128)(2,1)} %add_core.1), calls=%async_computation.7 | async-start | bytes 262144 | tf_op jit(solution)/shard_map/all_to_all | solution.py:484
  189.6 28.1 %collective-permute-start.7 = (bf16[192,512]{1,0:T(8,128)(2,1)S(1)}, bf16[192,512]{1,0:T(8,128)(2,1)S(1)}, u32[]{:S(2)}, u32[]{:S(2)}) collective-permute-start(bf16[192,512]{1,0:T(8,128)(2,1)S(1)} %copy-done.20), channel_id=1, source_target_pairs={{0,1},{1,2},{2,3},{3,0},{4,5},{5,6},{6,7},{7,4},{8,9},{9,10},{10,1... | collective-permute-start | bytes 589832 | tf_op jit(solution)/shard_map/ppermute | solution.py:70
  191.8 25.9 %collective-permute-start.8 = (bf16[192,512]{1,0:T(8,128)(2,1)S(1)}, bf16[192,512]{1,0:T(8,128)(2,1)S(1)}, u32[]{:S(2)}, u32[]{:S(2)}) collective-permute-start(bf16[192,512]{1,0:T(8,128)(2,1)S(1)} %copy-done.18), channel_id=1, source_target_pairs={{0,2},{1,3},{2,0},{3,1},{4,6},{5,7},{6,4},{7,5},{8,10},{9,11},{10,... | collective-permute-start | bytes 589832 | tf_op jit(solution)/shard_map/ppermute | solution.py:70
  196.0 21.7 %collective-permute-start.9 = (bf16[192,512]{1,0:T(8,128)(2,1)S(1)}, bf16[192,512]{1,0:T(8,128)(2,1)S(1)}, u32[]{:S(2)}, u32[]{:S(2)}) collective-permute-start(bf16[192,512]{1,0:T(8,128)(2,1)S(1)} %copy-done.16), channel_id=1, source_target_pairs={{0,3},{1,0},{2,1},{3,2},{4,7},{5,4},{6,5},{7,6},{8,11},{9,8},{10,9... | collective-permute-start | bytes 589832 | tf_op jit(solution)/shard_map/ppermute | solution.py:70
  199.4 16.4 %collective-permute-start.11 = (f32[64,128]{1,0:T(8,128)S(1)}, f32[64,128]{1,0:T(8,128)S(1)}, u32[]{:S(2)}, u32[]{:S(2)}) collective-permute-start(f32[64,128]{1,0:T(8,128)S(1)} %get-tuple-element.107), channel_id=1, source_target_pairs={{16,0},{32,16},{48,32},{64,48},{80,64},{96,80},{112,96},{128,112},... | collective-permute-start | bytes 98312 | tf_op jit(solution)/shard_map/ppermute | solution.py:513
  203.6 16.7 %collective-permute-start.10 = (bf16[64,64]{1,0:T(8,128)(2,1)S(1)}, bf16[64,64]{1,0:T(8,128)(2,1)S(1)}, u32[]{:S(2)}, u32[]{:S(2)}) collective-permute-start(bf16[64,64]{1,0:T(8,128)(2,1)S(1)} %sum_planes.1), channel_id=1, source_target_pairs={{0,0},{1,32},{2,64},{3,96},{4,128},{5,160},{6,192},{7,224},{8,256}... | collective-permute-start | bytes 24584 | tf_op jit(solution)/shard_map/ppermute | solution.py:501
  (15 other events, 154.3 us)

commit v5 on v4

--- a/solution.py
+++ b/solution.py
@@ -160,12 +160,15 @@
 
 
 def pre_kernel(at_ref, a_ref, w0, w1, w2, w3, o_ref):
+    ws = (w0, w1, w2, w3)
     x = jnp.concatenate([a_ref[i, :, 0:128] for i in range(SIDE)], axis=1)
     c = jnp.concatenate([a_ref[i, :, 128:256] for i in range(SIDE)], axis=1)
-    for k, w_ref in enumerate((w0, w1, w2, w3)):
+    pairs = mm(jnp.concatenate([w[0:128, :] for w in ws], axis=0), x, NT)
+    downs = mm(jnp.concatenate([w[128:192, :] for w in ws], axis=0), c, NT)
+    for k in range(SIDE):
         b = behind_of(at_ref, k)
-        o_ref[b, 0:128, :] = mm(w_ref[0:128, :], x, NT).astype(BF)
-        o_ref[b, 128:192, :] = mm(w_ref[128:192, :], c, NT).astype(BF)
+        o_ref[b, 0:128, :] = pairs[k * 128 : k * 128 + 128].astype(BF)
+        o_ref[b, 128:192, :] = downs[k * 64 : k * 64 + 64].astype(BF)
 
 
 def gate_kernel(p_ref, o_ref):
@@ -201,72 +204,98 @@
         out[128:192, :] = mm(h_ref[b, 128:192, :], c, NN).astype(BF)
 
 
-def tail_kernel(
-    at_ref, p_ref, r_ref, c_ref, q0, q1, q2, q3, o_ref, mine_ref, other_ref, stats_ref, held, sem
+def total_kernel(
+    at_ref, p_ref, r_ref, c_ref, q0, q1, q2, q3, mine_ref, other_ref, total_ref, stats_ref
 ):
-    copies = [
-        pltpu.make_async_copy(q, held.at[j], sem.at[j]) for j, q in enumerate((q0, q1, q2, q3))
-    ]
-    for copy in copies:
-        copy.start()
+    qs = (q0, q1, q2, q3)
     moe = mm(p_ref[...], r_ref[...], TN)
     total = (c_ref[...].astype(F32) + moe).astype(BF)
     tokens = total.shape[0]
-    size = held.shape[1]
+    total_ref[0:tokens, :] = total
+    total_ref[tokens:, :] = jnp.zeros((total_ref.shape[0] - tokens, 128), BF)
+    size = q0.shape[0]
     channels = SIDE * size
-    for copy in copies:
-        copy.wait()
     mean = jnp.zeros((1, tokens), F32)
-    for j in range(SIDE):
-        conv = held[j, :, 128 : 128 + tokens].astype(F32)
+    for q in qs:
+        conv = q[:, 128 : 128 + tokens].astype(F32)
         mean = mean + jnp.sum(conv, axis=0, keepdims=True)
     mean = mean / channels
     var = jnp.zeros((1, tokens), F32)
-    for j in range(SIDE):
-        off = held[j, :, 128 : 128 + tokens].astype(F32) - mean
+    for q in qs:
+        off = q[:, 128 : 128 + tokens].astype(F32) - mean
         var = var + jnp.sum(off * off, axis=0, keepdims=True)
     inv = lax.rsqrt(var / channels + NORM_EPS)
     stats_ref[0:1, :] = mean
     stats_ref[1:2, :] = inv
-    first = jnp.zeros((1, tokens), F32)
-    second = jnp.zeros((1, tokens), F32)
-    own = jnp.full((32, 128), at_ref[2], jnp.int32) == 0
-    low = lax.broadcasted_iota(jnp.int32, (32, 128), 1) < 64
-    lane = lax.broadcasted_iota(jnp.int32, (size, 128), 1)
-    for j in range(SIDE):
-        pieces = jnp.where((lane >= 64) & (lane < 67), held[j, :, 384:512].astype(F32), 0.0)
-        gain = jnp.sum(pieces, axis=1, keepdims=True)
-        normed = (held[j, :, 128 : 128 + tokens].astype(F32) - mean) * inv
-        linear = normed * gain
-        s = jax.nn.sigmoid(linear)
-        act = (linear * s).astype(BF)
-        cot = mm(held[j, :, 0:128], total, NT)
-        sloped = cot * (s * (1.0 + linear * (1.0 - s)) * gain)
-        first = first + jnp.sum(sloped, axis=0, keepdims=True)
-        second = second + jnp.sum(sloped * normed, axis=0, keepdims=True)
+    own = jnp.full((64, 128), at_ref[2], jnp.int32) == 0
+    for j, q in enumerate(qs):
+        normed = (q[:, 128 : 128 + tokens].astype(F32) - mean) * inv
+        linear = normed * gain_of(q)
+        act = (linear * jax.nn.sigmoid(linear)).astype(BF)
         grad = mm(act, total, NN)
         turned = pltpu.roll(grad, 64, 1)
         for k in range(SIDE):
             b = at_ref[48 + j * SIDE + k]
-            o_ref[b, 0:64, :] = cot[k * 64 : k * 64 + 64].astype(BF)
-            up, down = slice(k * 64, k * 64 + 32), slice(k * 64 + 32, k * 64 + 64)
-            left = jnp.where(low, grad[up], turned[down])
-            right = jnp.where(low, turned[up], grad[down])
-            mine_ref[b] = jnp.where(own, left, right).astype(BF)
-            other_ref[b] = jnp.where(own, right, left).astype(BF)
+            rows = slice(k * 64, k * 64 + 64)
+            mine_ref[b] = jnp.where(own, turned[rows], grad[rows]).astype(BF)
+            other_ref[b] = jnp.where(own, grad[rows], turned[rows]).astype(BF)
+
+
+def gain_of(q):
+    lane = lax.broadcasted_iota(jnp.int32, (q.shape[0], 128), 1)
+    pieces = jnp.where((lane >= 64) & (lane < 67), q[:, 384:512].astype(F32), 0.0)
+    return jnp.sum(pieces, axis=1, keepdims=True)
+
+
+def cot_kernel(at_ref, total_ref, stats_ref, q0, q1, q2, q3, o_ref):
+    wide = total_ref.shape[0]
+    tokens = stats_ref.shape[1]
+    total = total_ref[...]
+    mean, inv = stats_ref[0:1, :], stats_ref[1:2, :]
+    first = jnp.zeros((1, tokens), F32)
+    second = jnp.zeros((1, tokens), F32)
+    for j, q in enumerate((q0, q1, q2, q3)):
+        normed = (q[:, 128 : 128 + tokens].astype(F32) - mean) * inv
+        gain = gain_of(q)
+        linear = normed * gain
+        s = jax.nn.sigmoid(linear)
+        cot = mm(q[:, 0:128], total, NT)
+        sloped = cot[:, 0:tokens] * (s * (1.0 + linear * (1.0 - s)) * gain)
+        first = first + jnp.sum(sloped, axis=0, keepdims=True)
+        second = second + jnp.sum(sloped * normed, axis=0, keepdims=True)
+        for k in range(SIDE):
+            o_ref[at_ref[48 + j * SIDE + k], 0:64, :] = cot[k * 64 : k * 64 + 64].astype(BF)
     row = lax.broadcasted_iota(jnp.int32, (16, tokens), 0)
     sums = jnp.zeros((16, tokens), F32)
     for i, v in enumerate((first, second)):
         head = v.astype(BF).astype(F32)
         sums = jnp.where(row == 2 * i, head, jnp.where(row == 2 * i + 1, v - head, sums))
     for b in range(o_ref.shape[0]):
-        o_ref[b, 64:80, :] = sums.astype(BF)
+        o_ref[b, 64:80, 0:tokens] = sums.astype(BF)
+        o_ref[b, 64:80, tokens:wide] = jnp.zeros((16, wide - tokens), BF)
+
+
+def join_kernel(a_ref, mine_ref, other_ref, o_ref):
+    low = lax.broadcasted_iota(jnp.int32, (64, 128), 1) < 64
+    for b in range(o_ref.shape[0]):
+        piece = mine_ref[b].astype(F32) + other_ref[b].astype(F32)
+        o_ref[b, 0:64, :] = jnp.where(low, a_ref[b, 0:64, :].astype(F32), piece).astype(BF)
+        o_ref[b, 64:80, :] = a_ref[b, 64:80, :]
+
+
+def part_kernel(r_ref, o_ref):
+    low = lax.broadcasted_iota(jnp.int32, (32, 128), 1) < 64
+    for b in range(o_ref.shape[0]):
+        upper = pltpu.roll(r_ref[b, 0:32, 256:384].astype(F32), 64, 1)
+        lower = r_ref[b, 32:64, 256:384].astype(F32)
+        o_ref[b] = jnp.where(low, upper, lower).astype(BF)
 
 
 def head_kernel(r_ref, conv_ref, stats_ref, gain_ref, o_ref, h_ref):
-    total = r_ref[0].astype(F32)
+    tokens = conv_ref.shape[1]
+    total = r_ref[0, :, 0:tokens].astype(F32)
     for b in range(1, r_ref.shape[0]):
-        total = total + r_ref[b].astype(F32)
+        total = total + r_ref[b, :, 0:tokens].astype(F32)
     channels = 16 * conv_ref.shape[0]
     first = (total[64:65] + total[65:66]) / channels
     second = (total[66:67] + total[67:68]) / channels
@@ -287,11 +316,14 @@
         total = total + a_ref[b].astype(F32)
     turned = pltpu.roll(total, 64, 1)
     block = jnp.concatenate([total, turned], axis=0)
-    o_ref[...] = block.T[0:64, :].astype(BF)
-
-
-def add_kernel(a_ref, b_ref, o_ref):
-    o_ref[...] = (a_ref[...].astype(F32) + b_ref[...].astype(F32)).astype(BF)
+    o_ref[...] = block.T[0:64, :]
+
+
+def sum_side_kernel(p_ref, o_ref):
+    total = p_ref[0].astype(F32)
+    for a in range(1, SIDE):
+        total = total + p_ref[a].astype(F32)
+    o_ref[...] = total.astype(BF)
 
 
 def conv_kernel(cot_ref, next_ref, taps_ref, gate_ref, value_ref, v_ref, g_ref, buf):
@@ -423,7 +455,15 @@
         name="partial",
     )(at, hidden, *weights)
     part = exchange(part, feature_groups)
-    back = jnp.sum(part.astype(F32), axis=0).astype(BF).reshape(sp_count, SLOT, 128)
+    back = pl.pallas_call(
+        sum_side_kernel,
+        out_shape=whole((slots, 128), BF),
+        in_specs=[vmem],
+        out_specs=vmem,
+        compiler_params=room,
+        cost_estimate=cost(1000000, 1300000),
+        name="sum_side",
+    )(part).reshape(sp_count, SLOT, 128)
     back, weights = lax.optimization_barrier((back, weights))
     relay = pl.pallas_call(
         relay_kernel,
@@ -453,52 +493,68 @@
     )(at, hidden, rows)
     returned, grads = lax.optimization_barrier((returned, grads))
 
-    act_part, mine, other, stats = pl.pallas_call(
-        tail_kernel,
+    wide = 384
+    mine, other, total_cot, stats = pl.pallas_call(
+        total_kernel,
         out_shape=(
-            whole((tp_count, 80, tokens), BF),
-            whole((tp_count, 32, 128), BF),
-            whole((tp_count, 32, 128), BF),
+            whole((tp_count, 64, 128), BF),
+            whole((tp_count, 64, 128), BF),
+            whole((wide, 128), BF),
             whole((2, tokens), F32),
         ),
-        in_specs=[smem] + [vmem] * 3 + [pl.BlockSpec(memory_space=pltpu.HBM)] * SIDE,
+        in_specs=[smem] + [vmem] * 7,
         out_specs=(vmem,) * 4,
-        scratch_shapes=[VM((SIDE, 256, 512), BF), pltpu.SemaphoreType.DMA((SIDE,))],
-        compiler_params=room,
-        cost_estimate=cost(250000000, 4500000),
-        name="tail",
+        compiler_params=room,
+        cost_estimate=cost(170000000, 2500000),
+        name="total_cot",
     )(at, pick, returned, out_cotangent, *relay)
+    other = lax.ppermute(other, "c", [(0, 1), (1, 0)])
+    act_part = pl.pallas_call(
+        cot_kernel,
+        out_shape=whole((tp_count, 80, wide), BF),
+        in_specs=[smem] + [vmem] * 6,
+        out_specs=vmem,
+        compiler_params=room,
+        cost_estimate=cost(100000000, 2500000),
+        name="act_cot",
+    )(at, total_cot, stats, *relay)
+    act_part = pl.pallas_call(
+        join_kernel,
+        grid=(1,),
+        out_shape=whole((tp_count, 80, wide), BF),
+        in_specs=[
+            pl.BlockSpec((tp_count, 80, 128), lambda i: (0, 0, 2)),
+            pl.BlockSpec((tp_count, 64, 128), lambda i: (0, 0, 0)),
+            pl.BlockSpec((tp_count, 64, 128), lambda i: (0, 0, 0)),
+        ],
+        out_specs=pl.BlockSpec((tp_count, 80, 128), lambda i: (0, 0, 2)),
+        input_output_aliases={0: 0},
+        compiler_params=room,
+        cost_estimate=cost(100000, 1200000),
+        name="join_cores",
+    )(act_part, mine, other)
     act_part = lax.all_to_all(act_part, TP, 0, 0, tiled=True)
-    other = lax.ppermute(other, "c", [(0, 1), (1, 0)])
     proj_part = pl.pallas_call(
-        add_kernel,
+        part_kernel,
         out_shape=whole((tp_count, 32, 128), BF),
-        in_specs=[vmem] * 2,
+        in_specs=[vmem],
         out_specs=vmem,
         compiler_params=room,
         cost_estimate=cost(100000, 400000),
-        name="add_core",
-    )(mine, other)
+        name="proj_part",
+    )(act_part)
     act_part, proj_part, grads = lax.optimization_barrier((act_part, proj_part, grads))
     grads = pass_on(grads, unit_groups)
     proj_part = lax.all_to_all(proj_part, "z", 0, 0, tiled=True)
-    proj_sum = pl.pallas_call(
+    grad_proj = pl.pallas_call(
         sum_kernel,
-        out_shape=whole((64, 64), BF),
+        out_shape=whole((64, 64), F32),
         in_specs=[vmem],
         out_specs=vmem,
         compiler_params=room,
         cost_estimate=cost(100000, 200000),
         name="sum_planes",
     )(proj_part)
-    side = SIDE * SIDE
-    swap = [
-        (z * 2 * side + c * side + t, t * 2 * side + c * side + z)
-        for z in range(side)
-        for c in range(2)
-        for t in range(side)
-    ]
-    grad_proj = lax.ppermute(proj_sum, ("z",) + PLANE, swap).astype(F32)
 
     conv_cot, head = pl.pallas_call(
         head_kernel,

time: 222 us -> 213 us (0.959)
  the two profiles are of different devices: /device:TPU:16 before, /device:TPU:1 now
where the time goes in v5:
time: 213 us; the launch traced here: 212 us
  blocking collectives  82.4 us (39%)
  starting transfers between devices  69 us (32%)
  waiting for transfers between devices  28.7 us (13%)
  Pallas kernels  24.3 us (11%)
  local copies, waits for them, and re-layouts  6.69 us (3%)
    all_to_all x4, blocking collectives, exchange(): return lax.all_to_all(v, PLANE, 0, 0, axis_index_groups=groups, tiled=True)  63.6 us
    ppermute x9, starting transfers between devices, pass_on(): lax.ppermute(parts[k], PLANE, steps_ahead(groups, k))  27.5 us
    all_to_all x1, blocking collectives, body(): act_part = lax.all_to_all(act_part, TP, 0, 0, tiled=True)  18.8 us
    all_to_all x1, starting transfers between devices, body(): lax.all_to_all(sent.reshape(sp_count, SLOT, 256), SP, 0, 0, tiled=True)  16.8 us
    all_to_all x1, waiting for transfers between devices, body(): lax.all_to_all(sent.reshape(sp_count, SLOT, 256), SP, 0, 0, tiled=True)  15.5 us
    all_to_all x1, starting transfers between devices, body(): returned = lax.all_to_all(back, SP, 0, 0, tiled=True).reshape(slots, 128)  9.09 us
    all_to_all x1, starting transfers between devices, body(): proj_part = lax.all_to_all(proj_part, 'z', 0, 0, tiled=True)  7.81 us
    ppermute x9, waiting for transfers between devices, pass_on(): lax.ppermute(parts[k], PLANE, steps_ahead(groups, k))  5.24 us
  transfers between devices with their start and end apart: 14, of which 5 were waited for; matrix products, arithmetic and copies ran while one was open for 1% of the time, Pallas kernels for 5%

profile of v5, /device:TPU:1, one launch (start us, length us, event | category | flops | bytes accessed | tf_op | source)
XLA Modules:
  0.0 212.3 jit_solution(7158775709731072022)
XLA Ops:
  0.7 2.9 %route.1 = (bf16[1024,256]{1,0:T(8,128)(2,1)}, s32[2,320]{1,0:T(2,128)}) custom-call(s32[2,320]{1,0:T(2,128)} %bitcast.43, f32[2,320]{1,0:T(2,128)} %bitcast.44, bf16[320,128]{1,0:T(8,128)(2,1)} %x_ref.1, bf16[320,128]{1,0:T(8,128)(2,1)} %c_ref.3), custom_call_target="tpu_custom_call" | custom-call | flops 400000000 | bytes 2000000 | tf_op jit(solution)/shard_map/route/pallas_call | solution.py:377
  3.6 16.8 %all-to-all-start = ((bf16[32,32,256]{2,1,0:T(8,128)(2,1)}), bf16[32,32,256]{2,1,0:T(8,128)(2,1)}, u32[]{:S(2)}, u32[]{:S(2)}) async-start(bf16[32,32,256]{2,1,0:T(8,128)(2,1)} %bitcast.36), calls=%async_computation | async-start | bytes 1048576 | tf_op jit(solution)/shard_map/all_to_all | solution.py:416
  22.5 3.2 %collective-permute-start = (bf16[320,512]{1,0:T(8,128)(2,1)S(1)}, bf16[320,512]{1,0:T(8,128)(2,1)S(1)}, u32[]{:S(2)}, u32[]{:S(2)}) collective-permute-start(bf16[320,512]{1,0:T(8,128)(2,1)S(1)} %get-tuple-element.67), channel_id=1, source_target_pairs={{0,1},{1,2},{2,3},{3,0},{4,5},{5,6},{6,7},{7,4},{8,9},{9,10},{10,1... | collective-permute-start | bytes 983048 | tf_op jit(solution)/shard_map/ppermute | solution.py:70
  25.7 4.5 %collective-permute-start.1 = (bf16[320,512]{1,0:T(8,128)(2,1)S(1)}, bf16[320,512]{1,0:T(8,128)(2,1)S(1)}, u32[]{:S(2)}, u32[]{:S(2)}) collective-permute-start(bf16[320,512]{1,0:T(8,128)(2,1)S(1)} %get-tuple-element.68), channel_id=1, source_target_pairs={{0,2},{1,3},{2,0},{3,1},{4,6},{5,7},{6,4},{7,5},{8,10},{9,11},{10,... | collective-permute-start | bytes 983048 | tf_op jit(solution)/shard_map/ppermute | solution.py:70
  30.2 3.0 %collective-permute-start.2 = (bf16[320,512]{1,0:T(8,128)(2,1)S(1)}, bf16[320,512]{1,0:T(8,128)(2,1)S(1)}, u32[]{:S(2)}, u32[]{:S(2)}) collective-permute-start(bf16[320,512]{1,0:T(8,128)(2,1)S(1)} %get-tuple-element.69), channel_id=1, source_target_pairs={{0,3},{1,0},{2,1},{3,2},{4,7},{5,4},{6,5},{7,6},{8,11},{9,8},{10,9... | collective-permute-start | bytes 983048 | tf_op jit(solution)/shard_map/ppermute | solution.py:70
  33.2 3.3 %collective-permute-done.1.w2.r2 = bf16[320,512]{1,0:T(8,128)(2,1)S(1)} collective-permute-done((bf16[320,512]{1,0:T(8,128)(2,1)S(1)}, bf16[320,512]{1,0:T(8,128)(2,1)S(1)}, u32[]{:S(2)}, u32[]{:S(2)}) %collective-permute-start.1) | collective-permute-done | bytes 327712 | tf_op jit(solution)/shard_map/ppermute | solution.py:70
  38.5 15.5 %all-to-all-done = bf16[32,32,256]{2,1,0:T(8,128)(2,1)} async-done(((bf16[32,32,256]{2,1,0:T(8,128)(2,1)}), bf16[32,32,256]{2,1,0:T(8,128)(2,1)}, u32[]{:S(2)}, u32[]{:S(2)}) %all-to-all-start) | async-done | bytes 524320 | tf_op jit(solution)/shard_map/all_to_all | solution.py:416
  55.2 19.5 %all_to_all.40.a_ref = bf16[4,1024,256]{2,1,0:T(8,128)(2,1)S(1)} all-to-all(bf16[4,1024,256]{2,1,0:T(8,128)(2,1)S(1)} %broadcast_in_dim.23), channel_id=1, replica_groups={{0,4,8,12},{1,5,9,13},{2,6,10,14},{3,7,11,15},{16,17,18,19},{20,21,22,2..., dimensions={0} | all-to-all | bytes 4194304 | tf_op jit(solution)/shard_map/all_to_all | solution.py:79
  74.6 2.5 %pre.1 = bf16[4,192,1024]{2,1,0:T(8,128)(2,1)S(1)} custom-call(s32[64]{0:T(128)S(1)} %dynamic-slice_bitcast_fusion.at_ref, bf16[4,1024,256]{2,1,0:T(8,128)(2,1)S(1)} %all_to_all.40.a_ref, bf16[320,512]{1,0:T(8,128)(2,1)S(1)} %get-tuple-element.81.w0.r0, bf16[320,512]{1,0:T(8,128)(2,1)S(1)} %collective-permute-done.w1.r1, ...), custom_call_target="tpu_custom_call" | custom-call | flops 800000000 | bytes 4400000 | tf_op jit(solution)/shard_map/pre/pallas_call | solution.py:423
  77.2 16.4 %all_to_all.41.p_ref = bf16[4,192,1024]{2,1,0:T(8,128)(2,1)S(1)} all-to-all(bf16[4,192,1024]{2,1,0:T(8,128)(2,1)S(1)} %pre.1), channel_id=1, replica_groups={{0,1,2,3},{4,5,6,7},{8,9,10,11},{12,13,14,15},{16,20,24,28},{17,21,25,2..., dimensions={0} | all-to-all | bytes 3145728 | tf_op jit(solution)/shard_map/all_to_all | solution.py:79
  94.4 15.3 %all_to_all.42.h_ref = bf16[4,192,1024]{2,1,0:T(8,128)(2,1)S(1)} all-to-all(bf16[4,192,1024]{2,1,0:T(8,128)(2,1)S(1)} %gates.1), channel_id=1, replica_groups={{0,1,2,3},{4,5,6,7},{8,9,10,11},{12,13,14,15},{16,20,24,28},{17,21,25,2..., dimensions={0} | all-to-all | bytes 3145728 | tf_op jit(solution)/shard_map/all_to_all | solution.py:79
  111.9 12.5 %all_to_all.43.p_ref = bf16[4,1024,128]{2,1,0:T(8,128)(2,1)S(1)} all-to-all(bf16[4,1024,128]{2,1,0:T(8,128)(2,1)S(1)} %partial.1), channel_id=1, replica_groups={{0,4,8,12},{1,5,9,13},{2,6,10,14},{3,7,11,15},{16,17,18,19},{20,21,22,2..., dimensions={0} | all-to-all | bytes 2097152 | tf_op jit(solution)/shard_map/all_to_all | solution.py:79
  125.2 9.1 %all-to-all-start.5 = ((bf16[32,32,128]{2,1,0:T(8,128)(2,1)}), bf16[32,32,128]{2,1,0:T(8,128)(2,1)}, u32[]{:S(2)}, u32[]{:S(2)}) async-start(bf16[32,32,128]{2,1,0:T(8,128)(2,1)} %bitcast.27), calls=%async_computation.5 | async-start | bytes 524288 | tf_op jit(solution)/shard_map/all_to_all | solution.py:478
  138.7 3.7 %collective-permute-start.4 = (bf16[256,512]{1,0:T(8,128)(2,1)}, bf16[256,512]{1,0:T(8,128)(2,1)}, u32[]{:S(2)}, u32[]{:S(2)}) collective-permute-start(bf16[256,512]{1,0:T(8,128)(2,1)} %get-tuple-element.87), channel_id=1, source_target_pairs={{0,8},{4,12},{8,0},{12,4},{1,9},{5,13},{9,1},{13,5},{2,10},{6,14},... | collective-permute-start | bytes 786440 | tf_op jit(solution)/shard_map/ppermute | solution.py:70
  142.4 2.5 %collective-permute-start.5 = (bf16[256,512]{1,0:T(8,128)(2,1)}, bf16[256,512]{1,0:T(8,128)(2,1)}, u32[]{:S(2)}, u32[]{:S(2)}) collective-permute-start(bf16[256,512]{1,0:T(8,128)(2,1)} %get-tuple-element.88), channel_id=1, source_target_pairs={{0,12},{4,0},{8,4},{12,8},{1,13},{5,1},{9,5},{13,9},{2,14},{6,2},{... | collective-permute-start | bytes 786440 | tf_op jit(solution)/shard_map/ppermute | solution.py:70
  145.2 3.1 %grads.1 = (bf16[192,512]{1,0:T(8,128)(2,1)S(1)}, bf16[192,512]{1,0:T(8,128)(2,1)S(1)}, bf16[192,512]{1,0:T(8,128)(2,1)S(1)}, bf16[192,512]{1,0:T(8,128)(2,1)S(1)}) custom-call(s32[64]{0:T(128)S(1)} %dynamic-slice_bitcast_fusion.at_ref, bf16[4,192,1024]{2,1,0:T(8,128)(2,1)S(1)} %copy-done.1, bf16[4,1024,256]{2,1,0:T(8,128)(2,1)S(1)} %all_to_all.40.a_ref), custom_call_target="tpu_custom_call" | custom-call | flops 800000000 | bytes 4400000 | tf_op jit(solution)/shard_map/grads/pallas_call | solution.py:480
  151.0 5.0 %all-to-all-done.5 = bf16[32,32,128]{2,1,0:T(8,128)(2,1)} async-done(((bf16[32,32,128]{2,1,0:T(8,128)(2,1)}), bf16[32,32,128]{2,1,0:T(8,128)(2,1)}, u32[]{:S(2)}, u32[]{:S(2)}) %all-to-all-start.5) | async-done | bytes 262176 | tf_op jit(solution)/shard_map/all_to_all | solution.py:478
  158.5 3.4 %collective-permute-start.6 = (bf16[16,64,128]{2,1,0:T(8,128)(2,1)S(1)}, bf16[16,64,128]{2,1,0:T(8,128)(2,1)S(1)}, u32[]{:S(2)}, u32[]{:S(2)}) collective-permute-start(bf16[16,64,128]{2,1,0:T(8,128)(2,1)S(1)} %get-tuple-element.92), channel_id=1, source_target_pairs={{0,16},{16,0},{1,17},{17,1},{2,18},{18,2},{3,19},{19,3},{4,20},{20... | collective-permute-start | bytes 786440 | tf_op jit(solution)/shard_map/ppermute | solution.py:511
  164.1 18.8 %all_to_all.44.r_ref = bf16[16,80,384]{2,1,0:T(8,128)(2,1)S(1)} all-to-all(bf16[16,80,384]{2,1,0:T(8,128)(2,1)S(1)} %join_cores.1), channel_id=1, replica_groups=mesh['z'=16,'c'=2,'y'=4,'x'=4] {'y','x'}, dimensions={0} | all-to-all | bytes 1966080 | tf_op jit(solution)/shard_map/all_to_all | solution.py:536
  183.7 7.8 %all-to-all-start.7 = ((bf16[16,32,128]{2,1,0:T(8,128)(2,1)}), bf16[16,32,128]{2,1,0:T(8,128)(2,1)S(1)}, u32[]{:S(2)}, u32[]{:S(2)}) async-start(bf16[16,32,128]{2,1,0:T(8,128)(2,1)} %proj_part.1), calls=%async_computation.7 | async-start | bytes 262144 | tf_op jit(solution)/shard_map/all_to_all | solution.py:548
  193.5 3.7 %collective-permute-start.8 = (bf16[192,512]{1,0:T(8,128)(2,1)S(1)}, bf16[192,512]{1,0:T(8,128)(2,1)S(1)}, u32[]{:S(2)}, u32[]{:S(2)}) collective-permute-start(bf16[192,512]{1,0:T(8,128)(2,1)S(1)} %copy-done.19), channel_id=1, source_target_pairs={{0,2},{1,3},{2,0},{3,1},{4,6},{5,7},{6,4},{7,5},{8,10},{9,11},{10,... | collective-permute-start | bytes 589832 | tf_op jit(solution)/shard_map/ppermute | solution.py:70
  197.1 2.8 %collective-permute-start.9 = (bf16[192,512]{1,0:T(8,128)(2,1)S(1)}, bf16[192,512]{1,0:T(8,128)(2,1)S(1)}, u32[]{:S(2)}, u32[]{:S(2)}) collective-permute-start(bf16[192,512]{1,0:T(8,128)(2,1)S(1)} %copy-done.17), channel_id=1, source_target_pairs={{0,3},{1,0},{2,1},{3,2},{4,7},{5,4},{6,5},{7,6},{8,11},{9,8},{10,9... | collective-permute-start | bytes 589832 | tf_op jit(solution)/shard_map/ppermute | solution.py:70
  200.3 4.3 %collective-permute-start.10 = (f32[64,128]{1,0:T(8,128)S(1)}, f32[64,128]{1,0:T(8,128)S(1)}, u32[]{:S(2)}, u32[]{:S(2)}) collective-permute-start(f32[64,128]{1,0:T(8,128)S(1)} %get-tuple-element.107), channel_id=1, source_target_pairs={{16,0},{32,16},{48,32},{64,48},{80,64},{96,80},{112,96},{128,112},... | collective-permute-start | bytes 98312 | tf_op jit(solution)/shard_map/ppermute | solution.py:569
  204.7 3.0 %collective-permute-done.10.next_ref = f32[64,128]{1,0:T(8,128)S(1)} collective-permute-done((f32[64,128]{1,0:T(8,128)S(1)}, f32[64,128]{1,0:T(8,128)S(1)}, u32[]{:S(2)}, u32[]{:S(2)}) %collective-permute-start.10) | collective-permute-done | bytes 32800 | tf_op jit(solution)/shard_map/ppermute | solution.py:569
  (85 shorter events, 28.5 us)
Async XLA Ops:
  0.6 21.0 %copy-start.5 = (bf16[1,64,2048]{2,1,0:T(8,128)(2,1)S(1)}, bf16[1,64,2048]{2,1,0:T(8,128)(2,1)}, u32[]{:S(2)}) copy-start(bf16[1,64,2048]{2,1,0:T(8,128)(2,1)} %param.18) | copy-start | bytes 786436
  0.7 21.0 %copy-start.6 = (bf16[1,64,2048]{2,1,0:T(8,128)(2,1)S(1)}, bf16[1,64,2048]{2,1,0:T(8,128)(2,1)}, u32[]{:S(2)}) copy-start(bf16[1,64,2048]{2,1,0:T(8,128)(2,1)} %param.19) | copy-start | bytes 786436
  0.7 21.0 %copy-start.7 = (bf16[1,64,2048]{2,1,0:T(8,128)(2,1)S(1)}, bf16[1,64,2048]{2,1,0:T(8,128)(2,1)}, u32[]{:S(2)}) copy-start(bf16[1,64,2048]{2,1,0:T(8,128)(2,1)} %param.20) | copy-start | bytes 786436
  3.6 50.4 %all-to-all-start = ((bf16[32,32,256]{2,1,0:T(8,128)(2,1)}), bf16[32,32,256]{2,1,0:T(8,128)(2,1)}, u32[]{:S(2)}, u32[]{:S(2)}) async-start(bf16[32,32,256]{2,1,0:T(8,128)(2,1)} %bitcast.36), calls=%async_computation | async-start | bytes 1048576 | tf_op jit(solution)/shard_map/all_to_all | solution.py:416
  22.5 10.7 %collective-permute-start = (bf16[320,512]{1,0:T(8,128)(2,1)S(1)}, bf16[320,512]{1,0:T(8,128)(2,1)S(1)}, u32[]{:S(2)}, u32[]{:S(2)}) collective-permute-start(bf16[320,512]{1,0:T(8,128)(2,1)S(1)} %get-tuple-element.67), channel_id=1, source_target_pairs={{0,1},{1,2},{2,3},{3,0},{4,5},{5,6},{6,7},{7,4},{8,9},{9,10},{10,1... | collective-permute-start | bytes 983048 | tf_op jit(solution)/shard_map/ppermute | solution.py:70
  25.7 10.9 %collective-permute-start.1 = (bf16[320,512]{1,0:T(8,128)(2,1)S(1)}, bf16[320,512]{1,0:T(8,128)(2,1)S(1)}, u32[]{:S(2)}, u32[]{:S(2)}) collective-permute-start(bf16[320,512]{1,0:T(8,128)(2,1)S(1)} %get-tuple-element.68), channel_id=1, source_target_pairs={{0,2},{1,3},{2,0},{3,1},{4,6},{5,7},{6,4},{7,5},{8,10},{9,11},{10,... | collective-permute-start | bytes 983048 | tf_op jit(solution)/shard_map/ppermute | solution.py:70
  30.2 8.2 %collective-permute-start.2 = (bf16[320,512]{1,0:T(8,128)(2,1)S(1)}, bf16[320,512]{1,0:T(8,128)(2,1)S(1)}, u32[]{:S(2)}, u32[]{:S(2)}) collective-permute-start(bf16[320,512]{1,0:T(8,128)(2,1)S(1)} %get-tuple-element.69), channel_id=1, source_target_pairs={{0,3},{1,0},{2,1},{3,2},{4,7},{5,4},{6,5},{7,6},{8,11},{9,8},{10,9... | collective-permute-start | bytes 983048 | tf_op jit(solution)/shard_map/ppermute | solution.py:70
  125.2 30.8 %all-to-all-start.5 = ((bf16[32,32,128]{2,1,0:T(8,128)(2,1)}), bf16[32,32,128]{2,1,0:T(8,128)(2,1)}, u32[]{:S(2)}, u32[]{:S(2)}) async-start(bf16[32,32,128]{2,1,0:T(8,128)(2,1)} %bitcast.27), calls=%async_computation.5 | async-start | bytes 524288 | tf_op jit(solution)/shard_map/all_to_all | solution.py:478
  136.5 19.5 %collective-permute-start.3 = (bf16[256,512]{1,0:T(8,128)(2,1)}, bf16[256,512]{1,0:T(8,128)(2,1)S(1)}, u32[]{:S(2)}, u32[]{:S(2)}) collective-permute-start(bf16[256,512]{1,0:T(8,128)(2,1)} %get-tuple-element.86), channel_id=1, source_target_pairs={{0,4},{4,8},{8,12},{12,0},{1,5},{5,9},{9,13},{13,1},{2,6},{6,10},{... | collective-permute-start | bytes 786440 | tf_op jit(solution)/shard_map/ppermute | solution.py:70
  138.7 17.3 %collective-permute-start.4 = (bf16[256,512]{1,0:T(8,128)(2,1)}, bf16[256,512]{1,0:T(8,128)(2,1)}, u32[]{:S(2)}, u32[]{:S(2)}) collective-permute-start(bf16[256,512]{1,0:T(8,128)(2,1)} %get-tuple-element.87), channel_id=1, source_target_pairs={{0,8},{4,12},{8,0},{12,4},{1,9},{5,13},{9,1},{13,5},{2,10},{6,14},... | collective-permute-start | bytes 786440 | tf_op jit(solution)/shard_map/ppermute | solution.py:70
  142.4 13.6 %collective-permute-start.5 = (bf16[256,512]{1,0:T(8,128)(2,1)}, bf16[256,512]{1,0:T(8,128)(2,1)}, u32[]{:S(2)}, u32[]{:S(2)}) collective-permute-start(bf16[256,512]{1,0:T(8,128)(2,1)} %get-tuple-element.88), channel_id=1, source_target_pairs={{0,12},{4,0},{8,4},{12,8},{1,13},{5,1},{9,5},{13,9},{2,14},{6,2},{... | collective-permute-start | bytes 786440 | tf_op jit(solution)/shard_map/ppermute | solution.py:70
  158.5 5.4 %collective-permute-start.6 = (bf16[16,64,128]{2,1,0:T(8,128)(2,1)S(1)}, bf16[16,64,128]{2,1,0:T(8,128)(2,1)S(1)}, u32[]{:S(2)}, u32[]{:S(2)}) collective-permute-start(bf16[16,64,128]{2,1,0:T(8,128)(2,1)S(1)} %get-tuple-element.92), channel_id=1, source_target_pairs={{0,16},{16,0},{1,17},{17,1},{2,18},{18,2},{3,19},{19,3},{4,20},{20... | collective-permute-start | bytes 786440 | tf_op jit(solution)/shard_map/ppermute | solution.py:511
  164.1 27.4 %copy-start.21 = (bf16[192,512]{1,0:T(8,128)(2,1)S(1)}, bf16[192,512]{1,0:T(8,128)(2,1)}, u32[]{:S(2)}) copy-start(bf16[192,512]{1,0:T(8,128)(2,1)} %copy-done.20) | copy-start | bytes 589828
  164.1 29.3 %copy-start.19 = (bf16[192,512]{1,0:T(8,128)(2,1)S(1)}, bf16[192,512]{1,0:T(8,128)(2,1)}, u32[]{:S(2)}) copy-start(bf16[192,512]{1,0:T(8,128)(2,1)} %copy-done.18) | copy-start | bytes 589828
  164.1 33.0 %copy-start.17 = (bf16[192,512]{1,0:T(8,128)(2,1)S(1)}, bf16[192,512]{1,0:T(8,128)(2,1)}, u32[]{:S(2)}) copy-start(bf16[192,512]{1,0:T(8,128)(2,1)} %copy-done.16) | copy-start | bytes 589828
  182.9 21.7 %copy-start.22 = (f32[31,64]{1,0:T(8,128)S(1)}, f32[31,64]{1,0:T(8,128)}, u32[]{:S(2)}) copy-start(f32[31,64]{1,0:T(8,128)} %param.24) | copy-start | bytes 23812
  182.9 24.8 %copy-start.13 = (bf16[320,64]{0,1:T(8,128)(2,1)S(1)}, bf16[320,64]{0,1:T(8,128)(2,1)}, u32[]{:S(2)}) copy-start(bf16[320,64]{0,1:T(8,128)(2,1)} %param.22) | copy-start | bytes 122884
  182.9 24.8 %copy-start.14 = (bf16[320,64]{0,1:T(8,128)(2,1)S(1)}, bf16[320,64]{0,1:T(8,128)(2,1)}, u32[]{:S(2)}) copy-start(bf16[320,64]{0,1:T(8,128)(2,1)} %param.21) | copy-start | bytes 122884
  182.9 26.7 %copy-start.11 = (bf16[192,512]{1,0:T(8,128)(2,1)S(1)}, bf16[192,512]{1,0:T(8,128)(2,1)}, u32[]{:S(2)}) copy-start(bf16[192,512]{1,0:T(8,128)(2,1)} %copy-done.10) | copy-start | bytes 589828
  183.7 27.8 %all-to-all-start.7 = ((bf16[16,32,128]{2,1,0:T(8,128)(2,1)}), bf16[16,32,128]{2,1,0:T(8,128)(2,1)S(1)}, u32[]{:S(2)}, u32[]{:S(2)}) async-start(bf16[16,32,128]{2,1,0:T(8,128)(2,1)} %proj_part.1), calls=%async_computation.7 | async-start | bytes 262144 | tf_op jit(solution)/shard_map/all_to_all | solution.py:548
  191.5 18.1 %collective-permute-start.7 = (bf16[192,512]{1,0:T(8,128)(2,1)S(1)}, bf16[192,512]{1,0:T(8,128)(2,1)S(1)}, u32[]{:S(2)}, u32[]{:S(2)}) collective-permute-start(bf16[192,512]{1,0:T(8,128)(2,1)S(1)} %copy-done.21), channel_id=1, source_target_pairs={{0,1},{1,2},{2,3},{3,0},{4,5},{5,6},{6,7},{7,4},{8,9},{9,10},{10,1... | collective-permute-start | bytes 589832 | tf_op jit(solution)/shard_map/ppermute | solution.py:70
  193.5 16.2 %collective-permute-start.8 = (bf16[192,512]{1,0:T(8,128)(2,1)S(1)}, bf16[192,512]{1,0:T(8,128)(2,1)S(1)}, u32[]{:S(2)}, u32[]{:S(2)}) collective-permute-start(bf16[192,512]{1,0:T(8,128)(2,1)S(1)} %copy-done.19), channel_id=1, source_target_pairs={{0,2},{1,3},{2,0},{3,1},{4,6},{5,7},{6,4},{7,5},{8,10},{9,11},{10,... | collective-permute-start | bytes 589832 | tf_op jit(solution)/shard_map/ppermute | solution.py:70
  197.1 12.5 %collective-permute-start.9 = (bf16[192,512]{1,0:T(8,128)(2,1)S(1)}, bf16[192,512]{1,0:T(8,128)(2,1)S(1)}, u32[]{:S(2)}, u32[]{:S(2)}) collective-permute-start(bf16[192,512]{1,0:T(8,128)(2,1)S(1)} %copy-done.17), channel_id=1, source_target_pairs={{0,3},{1,0},{2,1},{3,2},{4,7},{5,4},{6,5},{7,6},{8,11},{9,8},{10,9... | collective-permute-start | bytes 589832 | tf_op jit(solution)/shard_map/ppermute | solution.py:70
  200.3 7.5 %collective-permute-start.10 = (f32[64,128]{1,0:T(8,128)S(1)}, f32[64,128]{1,0:T(8,128)S(1)}, u32[]{:S(2)}, u32[]{:S(2)}) collective-permute-start(f32[64,128]{1,0:T(8,128)S(1)} %get-tuple-element.107), channel_id=1, source_target_pairs={{16,0},{32,16},{48,32},{64,48},{80,64},{96,80},{112,96},{128,112},... | collective-permute-start | bytes 98312 | tf_op jit(solution)/shard_map/ppermute | solution.py:569
  (14 other events, 120.3 us)

commit v6 on v5

--- a/solution.py
+++ b/solution.py
@@ -265,14 +265,14 @@
         second = second + jnp.sum(sloped * normed, axis=0, keepdims=True)
         for k in range(SIDE):
             o_ref[at_ref[48 + j * SIDE + k], 0:64, :] = cot[k * 64 : k * 64 + 64].astype(BF)
-    row = lax.broadcasted_iota(jnp.int32, (16, tokens), 0)
-    sums = jnp.zeros((16, tokens), F32)
+    row = lax.broadcasted_iota(jnp.int32, (8, tokens), 0)
+    sums = jnp.zeros((8, tokens), F32)
     for i, v in enumerate((first, second)):
         head = v.astype(BF).astype(F32)
         sums = jnp.where(row == 2 * i, head, jnp.where(row == 2 * i + 1, v - head, sums))
     for b in range(o_ref.shape[0]):
-        o_ref[b, 64:80, 0:tokens] = sums.astype(BF)
-        o_ref[b, 64:80, tokens:wide] = jnp.zeros((16, wide - tokens), BF)
+        o_ref[b, 64:72, 0:tokens] = sums.astype(BF)
+        o_ref[b, 64:72, tokens:wide] = jnp.zeros((8, wide - tokens), BF)
 
 
 def join_kernel(a_ref, mine_ref, other_ref, o_ref):
@@ -280,7 +280,7 @@
     for b in range(o_ref.shape[0]):
         piece = mine_ref[b].astype(F32) + other_ref[b].astype(F32)
         o_ref[b, 0:64, :] = jnp.where(low, a_ref[b, 0:64, :].astype(F32), piece).astype(BF)
-        o_ref[b, 64:80, :] = a_ref[b, 64:80, :]
+        o_ref[b, 64:72, :] = a_ref[b, 64:72, :]
 
 
 def part_kernel(r_ref, o_ref):
@@ -477,22 +477,6 @@
     relay = pass_on(relay, feature_groups)
     returned = lax.all_to_all(back, SP, 0, 0, tiled=True).reshape(slots, 128)
 
-    grads = pl.pallas_call(
-        grads_kernel,
-        grid=(SIDE,),
-        out_shape=(whole((192, 512), BF),) * SIDE,
-        in_specs=[
-            smem,
-            pl.BlockSpec((SIDE, 192, slots), lambda i: (0, 0, 0)),
-            pl.BlockSpec((1, slots, 256), lambda i: (i, 0, 0)),
-        ],
-        out_specs=(pl.BlockSpec((192, 128), lambda i: (0, i)),) * SIDE,
-        compiler_params=room,
-        cost_estimate=cost(800000000, 4400000),
-        name="grads",
-    )(at, hidden, rows)
-    returned, grads = lax.optimization_barrier((returned, grads))
-
     wide = 384
     mine, other, total_cot, stats = pl.pallas_call(
         total_kernel,
@@ -511,7 +495,7 @@
     other = lax.ppermute(other, "c", [(0, 1), (1, 0)])
     act_part = pl.pallas_call(
         cot_kernel,
-        out_shape=whole((tp_count, 80, wide), BF),
+        out_shape=whole((tp_count, 72, wide), BF),
         in_specs=[smem] + [vmem] * 6,
         out_specs=vmem,
         compiler_params=room,
@@ -521,18 +505,34 @@
     act_part = pl.pallas_call(
         join_kernel,
         grid=(1,),
-        out_shape=whole((tp_count, 80, wide), BF),
+        out_shape=whole((tp_count, 72, wide), BF),
         in_specs=[
-            pl.BlockSpec((tp_count, 80, 128), lambda i: (0, 0, 2)),
+            pl.BlockSpec((tp_count, 72, 128), lambda i: (0, 0, 2)),
             pl.BlockSpec((tp_count, 64, 128), lambda i: (0, 0, 0)),
             pl.BlockSpec((tp_count, 64, 128), lambda i: (0, 0, 0)),
         ],
-        out_specs=pl.BlockSpec((tp_count, 80, 128), lambda i: (0, 0, 2)),
+        out_specs=pl.BlockSpec((tp_count, 72, 128), lambda i: (0, 0, 2)),
         input_output_aliases={0: 0},
         compiler_params=room,
         cost_estimate=cost(100000, 1200000),
         name="join_cores",
     )(act_part, mine, other)
+    act_part, hidden, rows = lax.optimization_barrier((act_part, hidden, rows))
+    grads = pl.pallas_call(
+        grads_kernel,
+        grid=(SIDE,),
+        out_shape=(whole((192, 512), BF),) * SIDE,
+        in_specs=[
+            smem,
+            pl.BlockSpec((SIDE, 192, slots), lambda i: (0, 0, 0)),
+            pl.BlockSpec((1, slots, 256), lambda i: (i, 0, 0)),
+        ],
+        out_specs=(pl.BlockSpec((192, 128), lambda i: (0, i)),) * SIDE,
+        compiler_params=room,
+        cost_estimate=cost(800000000, 4400000),
+        name="grads",
+    )(at, hidden, rows)
+    grads = pass_on(grads, unit_groups)
     act_part = lax.all_to_all(act_part, TP, 0, 0, tiled=True)
     proj_part = pl.pallas_call(
         part_kernel,
@@ -543,8 +543,7 @@
         cost_estimate=cost(100000, 400000),
         name="proj_part",
     )(act_part)
-    act_part, proj_part, grads = lax.optimization_barrier((act_part, proj_part, grads))
-    grads = pass_on(grads, unit_groups)
+    act_part, proj_part = lax.optimization_barrier((act_part, proj_part))
     proj_part = lax.all_to_all(proj_part, "z", 0, 0, tiled=True)
     grad_proj = pl.pallas_call(
         sum_kernel,

time: 213 us -> 218 us (1.023)
  waiting for transfers between devices: 28.7 us -> 32 us
  local copies, waits for them, and re-layouts: 6.69 us -> 9.62 us
    ppermute x9, waiting for transfers between devices: 5.24 us -> 9.89 us  [pass_on(): lax.ppermute(parts[k], PLANE, steps_ahead(groups, k))]
    unnamed x49 -> x45, local copies, waits for them, and re-layouts: 4.27 us -> 7.2 us
  transfers between devices with their start and end apart: 14 -> 14, of which waited for: 5 -> 7; matrix products, arithmetic and copies ran while one was open for 1% -> 1% of each run, Pallas kernels for 5% -> 5%
where the time goes in v6:
time: 218 us; the launch traced here: 216 us
  blocking collectives  81.2 us (37%)
  starting transfers between devices  69.1 us (32%)
  waiting for transfers between devices  32 us (15%)
  Pallas kernels  23.3 us (11%)
  local copies, waits for them, and re-layouts  9.62 us (4%)
    all_to_all x4, blocking collectives, exchange(): return lax.all_to_all(v, PLANE, 0, 0, axis_index_groups=groups, tiled=True)  63.6 us
    ppermute x9, starting transfers between devices, pass_on(): lax.ppermute(parts[k], PLANE, steps_ahead(groups, k))  27.8 us
    all_to_all x1, blocking collectives, body(): act_part = lax.all_to_all(act_part, TP, 0, 0, tiled=True)  17.6 us
    all_to_all x1, starting transfers between devices, body(): lax.all_to_all(sent.reshape(sp_count, SLOT, 256), SP, 0, 0, tiled=True)  16.8 us
    all_to_all x1, waiting for transfers between devices, body(): lax.all_to_all(sent.reshape(sp_count, SLOT, 256), SP, 0, 0, tiled=True)  15.5 us
    ppermute x9, waiting for transfers between devices, pass_on(): lax.ppermute(parts[k], PLANE, steps_ahead(groups, k))  9.89 us
    all_to_all x1, starting transfers between devices, body(): returned = lax.all_to_all(back, SP, 0, 0, tiled=True).reshape(slots, 128)  9.22 us
    all_to_all x1, starting transfers between devices, body(): proj_part = lax.all_to_all(proj_part, 'z', 0, 0, tiled=True)  7.51 us
  transfers between devices with their start and end apart: 14, of which 7 were waited for; matrix products, arithmetic and copies ran while one was open for 1% of the time, Pallas kernels for 5%

profile of v6, /device:TPU:1, one launch (start us, length us, event | category | flops | bytes accessed | tf_op | source)
XLA Modules:
  0.0 216.3 jit_solution(6739936635424618208)
XLA Ops:
  0.7 2.9 %route.1 = (bf16[1024,256]{1,0:T(8,128)(2,1)}, s32[2,320]{1,0:T(2,128)}) custom-call(s32[2,320]{1,0:T(2,128)} %bitcast.43, f32[2,320]{1,0:T(2,128)} %bitcast.44, bf16[320,128]{1,0:T(8,128)(2,1)} %x_ref.1, bf16[320,128]{1,0:T(8,128)(2,1)} %c_ref.3), custom_call_target="tpu_custom_call" | custom-call | flops 400000000 | bytes 2000000 | tf_op jit(solution)/shard_map/route/pallas_call | solution.py:377
  3.6 16.8 %all-to-all-start = ((bf16[32,32,256]{2,1,0:T(8,128)(2,1)}), bf16[32,32,256]{2,1,0:T(8,128)(2,1)}, u32[]{:S(2)}, u32[]{:S(2)}) async-start(bf16[32,32,256]{2,1,0:T(8,128)(2,1)} %bitcast.36), calls=%async_computation | async-start | bytes 1048576 | tf_op jit(solution)/shard_map/all_to_all | solution.py:416
  22.5 3.2 %collective-permute-start = (bf16[320,512]{1,0:T(8,128)(2,1)S(1)}, bf16[320,512]{1,0:T(8,128)(2,1)S(1)}, u32[]{:S(2)}, u32[]{:S(2)}) collective-permute-start(bf16[320,512]{1,0:T(8,128)(2,1)S(1)} %get-tuple-element.61), channel_id=1, source_target_pairs={{0,1},{1,2},{2,3},{3,0},{4,5},{5,6},{6,7},{7,4},{8,9},{9,10},{10,1... | collective-permute-start | bytes 983048 | tf_op jit(solution)/shard_map/ppermute | solution.py:70
  25.7 4.5 %collective-permute-start.1 = (bf16[320,512]{1,0:T(8,128)(2,1)S(1)}, bf16[320,512]{1,0:T(8,128)(2,1)S(1)}, u32[]{:S(2)}, u32[]{:S(2)}) collective-permute-start(bf16[320,512]{1,0:T(8,128)(2,1)S(1)} %get-tuple-element.62), channel_id=1, source_target_pairs={{0,2},{1,3},{2,0},{3,1},{4,6},{5,7},{6,4},{7,5},{8,10},{9,11},{10,... | collective-permute-start | bytes 983048 | tf_op jit(solution)/shard_map/ppermute | solution.py:70
  30.2 3.0 %collective-permute-start.2 = (bf16[320,512]{1,0:T(8,128)(2,1)S(1)}, bf16[320,512]{1,0:T(8,128)(2,1)S(1)}, u32[]{:S(2)}, u32[]{:S(2)}) collective-permute-start(bf16[320,512]{1,0:T(8,128)(2,1)S(1)} %get-tuple-element.63), channel_id=1, source_target_pairs={{0,3},{1,0},{2,1},{3,2},{4,7},{5,4},{6,5},{7,6},{8,11},{9,8},{10,9... | collective-permute-start | bytes 983048 | tf_op jit(solution)/shard_map/ppermute | solution.py:70
  33.2 3.3 %collective-permute-done.1.w2.r2 = bf16[320,512]{1,0:T(8,128)(2,1)S(1)} collective-permute-done((bf16[320,512]{1,0:T(8,128)(2,1)S(1)}, bf16[320,512]{1,0:T(8,128)(2,1)S(1)}, u32[]{:S(2)}, u32[]{:S(2)}) %collective-permute-start.1) | collective-permute-done | bytes 327712 | tf_op jit(solution)/shard_map/ppermute | solution.py:70
  38.5 15.5 %all-to-all-done = bf16[32,32,256]{2,1,0:T(8,128)(2,1)} async-done(((bf16[32,32,256]{2,1,0:T(8,128)(2,1)}), bf16[32,32,256]{2,1,0:T(8,128)(2,1)}, u32[]{:S(2)}, u32[]{:S(2)}) %all-to-all-start) | async-done | bytes 524320 | tf_op jit(solution)/shard_map/all_to_all | solution.py:416
  55.2 19.5 %all_to_all.40.a_ref = bf16[4,1024,256]{2,1,0:T(8,128)(2,1)S(1)} all-to-all(bf16[4,1024,256]{2,1,0:T(8,128)(2,1)S(1)} %broadcast_in_dim.23), channel_id=1, replica_groups={{0,4,8,12},{1,5,9,13},{2,6,10,14},{3,7,11,15},{16,17,18,19},{20,21,22,2..., dimensions={0} | all-to-all | bytes 4194304 | tf_op jit(solution)/shard_map/all_to_all | solution.py:79
  74.6 2.5 %pre.1 = bf16[4,192,1024]{2,1,0:T(8,128)(2,1)S(1)} custom-call(s32[64]{0:T(128)S(1)} %dynamic-slice_bitcast_fusion.at_ref, bf16[4,1024,256]{2,1,0:T(8,128)(2,1)S(1)} %all_to_all.40.a_ref, bf16[320,512]{1,0:T(8,128)(2,1)S(1)} %get-tuple-element.70.w0.r0, bf16[320,512]{1,0:T(8,128)(2,1)S(1)} %collective-permute-done.w1.r1, ...), custom_call_target="tpu_custom_call" | custom-call | flops 800000000 | bytes 4400000 | tf_op jit(solution)/shard_map/pre/pallas_call | solution.py:423
  77.2 16.4 %all_to_all.41.p_ref = bf16[4,192,1024]{2,1,0:T(8,128)(2,1)S(1)} all-to-all(bf16[4,192,1024]{2,1,0:T(8,128)(2,1)S(1)} %pre.1), channel_id=1, replica_groups={{0,1,2,3},{4,5,6,7},{8,9,10,11},{12,13,14,15},{16,20,24,28},{17,21,25,2..., dimensions={0} | all-to-all | bytes 3145728 | tf_op jit(solution)/shard_map/all_to_all | solution.py:79
  94.4 15.3 %all_to_all.42.h_ref = bf16[4,192,1024]{2,1,0:T(8,128)(2,1)S(1)} all-to-all(bf16[4,192,1024]{2,1,0:T(8,128)(2,1)S(1)} %gates.1), channel_id=1, replica_groups={{0,1,2,3},{4,5,6,7},{8,9,10,11},{12,13,14,15},{16,20,24,28},{17,21,25,2..., dimensions={0} | all-to-all | bytes 3145728 | tf_op jit(solution)/shard_map/all_to_all | solution.py:79
  111.8 12.5 %all_to_all.43.p_ref = bf16[4,1024,128]{2,1,0:T(8,128)(2,1)S(1)} all-to-all(bf16[4,1024,128]{2,1,0:T(8,128)(2,1)S(1)} %partial.1), channel_id=1, replica_groups={{0,4,8,12},{1,5,9,13},{2,6,10,14},{3,7,11,15},{16,17,18,19},{20,21,22,2..., dimensions={0} | all-to-all | bytes 2097152 | tf_op jit(solution)/shard_map/all_to_all | solution.py:79
  125.1 9.2 %all-to-all-start.5 = ((bf16[32,32,128]{2,1,0:T(8,128)(2,1)}), bf16[32,32,128]{2,1,0:T(8,128)(2,1)}, u32[]{:S(2)}, u32[]{:S(2)}) async-start(bf16[32,32,128]{2,1,0:T(8,128)(2,1)} %bitcast.27), calls=%async_computation.5 | async-start | bytes 524288 | tf_op jit(solution)/shard_map/all_to_all | solution.py:478
  138.1 3.7 %collective-permute-start.4 = (bf16[256,512]{1,0:T(8,128)(2,1)S(1)}, bf16[256,512]{1,0:T(8,128)(2,1)S(1)}, u32[]{:S(2)}, u32[]{:S(2)}) collective-permute-start(bf16[256,512]{1,0:T(8,128)(2,1)S(1)} %get-tuple-element.76), channel_id=1, source_target_pairs={{0,8},{4,12},{8,0},{12,4},{1,9},{5,13},{9,1},{13,5},{2,10},{6,14},... | collective-permute-start | bytes 786440 | tf_op jit(solution)/shard_map/ppermute | solution.py:70
  141.8 2.5 %collective-permute-start.5 = (bf16[256,512]{1,0:T(8,128)(2,1)S(1)}, bf16[256,512]{1,0:T(8,128)(2,1)S(1)}, u32[]{:S(2)}, u32[]{:S(2)}) collective-permute-start(bf16[256,512]{1,0:T(8,128)(2,1)S(1)} %get-tuple-element.77), channel_id=1, source_target_pairs={{0,12},{4,0},{8,4},{12,8},{1,13},{5,1},{9,5},{13,9},{2,14},{6,2},{... | collective-permute-start | bytes 786440 | tf_op jit(solution)/shard_map/ppermute | solution.py:70
  144.5 2.9 %collective-permute-done.3.q1 = bf16[256,512]{1,0:T(8,128)(2,1)S(1)} collective-permute-done((bf16[256,512]{1,0:T(8,128)(2,1)S(1)}, bf16[256,512]{1,0:T(8,128)(2,1)S(1)}, u32[]{:S(2)}, u32[]{:S(2)}) %collective-permute-start.3) | collective-permute-done | bytes 262176 | tf_op jit(solution)/shard_map/ppermute | solution.py:70
  150.6 5.5 %all-to-all-done.5 = bf16[32,32,128]{2,1,0:T(8,128)(2,1)} async-done(((bf16[32,32,128]{2,1,0:T(8,128)(2,1)}), bf16[32,32,128]{2,1,0:T(8,128)(2,1)}, u32[]{:S(2)}, u32[]{:S(2)}) %all-to-all-start.5) | async-done | bytes 262176 | tf_op jit(solution)/shard_map/all_to_all | solution.py:478
  161.3 3.4 %collective-permute-start.6 = (bf16[16,64,128]{2,1,0:T(8,128)(2,1)S(1)}, bf16[16,64,128]{2,1,0:T(8,128)(2,1)S(1)}, u32[]{:S(2)}, u32[]{:S(2)}) collective-permute-start(bf16[16,64,128]{2,1,0:T(8,128)(2,1)S(1)} %get-tuple-element.81), channel_id=1, source_target_pairs={{0,16},{16,0},{1,17},{17,1},{2,18},{18,2},{3,19},{19,3},{4,20},{20... | collective-permute-start | bytes 786440 | tf_op jit(solution)/shard_map/ppermute | solution.py:495
  166.4 17.6 %all_to_all.44.r_ref = bf16[16,72,384]{2,1,0:T(8,128)(2,1)S(1)} all-to-all(bf16[16,72,384]{2,1,0:T(8,128)(2,1)S(1)} %join_cores.1), channel_id=1, replica_groups=mesh['z'=16,'c'=2,'y'=4,'x'=4] {'y','x'}, dimensions={0} | all-to-all | bytes 1769472 | tf_op jit(solution)/shard_map/all_to_all | solution.py:536
  184.7 7.5 %all-to-all-start.7 = ((bf16[16,32,128]{2,1,0:T(8,128)(2,1)}), bf16[16,32,128]{2,1,0:T(8,128)(2,1)S(1)}, u32[]{:S(2)}, u32[]{:S(2)}) async-start(bf16[16,32,128]{2,1,0:T(8,128)(2,1)} %proj_part.1), calls=%async_computation.7 | async-start | bytes 262144 | tf_op jit(solution)/shard_map/all_to_all | solution.py:547
  193.7 3.6 %grads.1 = (bf16[192,512]{1,0:T(8,128)(2,1)S(1)}, bf16[192,512]{1,0:T(8,128)(2,1)}, bf16[192,512]{1,0:T(8,128)(2,1)}, bf16[192,512]{1,0:T(8,128)(2,1)}) custom-call(s32[64]{0:T(128)S(1)} %dynamic-slice_bitcast_fusion.at_ref, bf16[4,192,1024]{2,1,0:T(8,128)(2,1)S(1)} %copy-done.1, bf16[4,1024,256]{2,1,0:T(8,128)(2,1)S(1)} %all_to_all.40.a_ref), custom_call_target="tpu_custom_call" | custom-call | flops 800000000 | bytes 4400000 | tf_op jit(solution)/shard_map/grads/pallas_call | solution.py:521
  199.3 3.9 %collective-permute-start.8 = (bf16[192,512]{1,0:T(8,128)(2,1)}, bf16[192,512]{1,0:T(8,128)(2,1)S(1)}, u32[]{:S(2)}, u32[]{:S(2)}) collective-permute-start(bf16[192,512]{1,0:T(8,128)(2,1)} %get-tuple-element.86), channel_id=1, source_target_pairs={{0,2},{1,3},{2,0},{3,1},{4,6},{5,7},{6,4},{7,5},{8,10},{9,11},{10,... | collective-permute-start | bytes 589832 | tf_op jit(solution)/shard_map/ppermute | solution.py:70
  203.2 2.6 %collective-permute-start.9 = (bf16[192,512]{1,0:T(8,128)(2,1)}, bf16[192,512]{1,0:T(8,128)(2,1)S(1)}, u32[]{:S(2)}, u32[]{:S(2)}) collective-permute-start(bf16[192,512]{1,0:T(8,128)(2,1)} %get-tuple-element.87), channel_id=1, source_target_pairs={{0,3},{1,0},{2,1},{3,2},{4,7},{5,4},{6,5},{7,6},{8,11},{9,8},{10,9... | collective-permute-start | bytes 589832 | tf_op jit(solution)/shard_map/ppermute | solution.py:70
  206.1 4.4 %collective-permute-start.10 = (f32[64,128]{1,0:T(8,128)S(1)}, f32[64,128]{1,0:T(8,128)S(1)}, u32[]{:S(2)}, u32[]{:S(2)}) collective-permute-start(f32[64,128]{1,0:T(8,128)S(1)} %get-tuple-element.95), channel_id=1, source_target_pairs={{16,0},{32,16},{48,32},{64,48},{80,64},{96,80},{112,96},{128,112},... | collective-permute-start | bytes 98312 | tf_op jit(solution)/shard_map/ppermute | solution.py:568
  (81 shorter events, 33.1 us)
Async XLA Ops:
  0.6 21.0 %copy-start.11 = (bf16[1,64,2048]{2,1,0:T(8,128)(2,1)S(1)}, bf16[1,64,2048]{2,1,0:T(8,128)(2,1)}, u32[]{:S(2)}) copy-start(bf16[1,64,2048]{2,1,0:T(8,128)(2,1)} %param.18) | copy-start | bytes 786436
  0.6 20.2 %copy-start.15 = (bf16[320,64]{0,1:T(8,128)(2,1)S(1)}, bf16[320,64]{0,1:T(8,128)(2,1)}, u32[]{:S(2)}) copy-start(bf16[320,64]{0,1:T(8,128)(2,1)} %param.23) | copy-start | bytes 122884
  0.7 19.8 %copy-start.21 = (f32[64]{0:T(128)S(1)}, f32[64]{0:T(128)}, u32[]{:S(2)}) copy-start(f32[64]{0:T(128)} %param.25) | copy-start | bytes 772
  0.7 21.0 %copy-start.12 = (bf16[1,64,2048]{2,1,0:T(8,128)(2,1)S(1)}, bf16[1,64,2048]{2,1,0:T(8,128)(2,1)}, u32[]{:S(2)}) copy-start(bf16[1,64,2048]{2,1,0:T(8,128)(2,1)} %param.19) | copy-start | bytes 786436
  0.7 21.0 %copy-start.13 = (bf16[1,64,2048]{2,1,0:T(8,128)(2,1)S(1)}, bf16[1,64,2048]{2,1,0:T(8,128)(2,1)}, u32[]{:S(2)}) copy-start(bf16[1,64,2048]{2,1,0:T(8,128)(2,1)} %param.20) | copy-start | bytes 786436
  0.7 20.9 %copy-start.14 = (bf16[64,2048]{1,0:T(8,128)(2,1)S(1)}, bf16[64,2048]{1,0:T(8,128)(2,1)}, u32[]{:S(2)}) copy-start(bf16[64,2048]{1,0:T(8,128)(2,1)} %p_ref.1) | copy-start | bytes 786436
  3.6 50.4 %all-to-all-start = ((bf16[32,32,256]{2,1,0:T(8,128)(2,1)}), bf16[32,32,256]{2,1,0:T(8,128)(2,1)}, u32[]{:S(2)}, u32[]{:S(2)}) async-start(bf16[32,32,256]{2,1,0:T(8,128)(2,1)} %bitcast.36), calls=%async_computation | async-start | bytes 1048576 | tf_op jit(solution)/shard_map/all_to_all | solution.py:416
  22.5 10.7 %collective-permute-start = (bf16[320,512]{1,0:T(8,128)(2,1)S(1)}, bf16[320,512]{1,0:T(8,128)(2,1)S(1)}, u32[]{:S(2)}, u32[]{:S(2)}) collective-permute-start(bf16[320,512]{1,0:T(8,128)(2,1)S(1)} %get-tuple-element.61), channel_id=1, source_target_pairs={{0,1},{1,2},{2,3},{3,0},{4,5},{5,6},{6,7},{7,4},{8,9},{9,10},{10,1... | collective-permute-start | bytes 983048 | tf_op jit(solution)/shard_map/ppermute | solution.py:70
  25.7 10.9 %collective-permute-start.1 = (bf16[320,512]{1,0:T(8,128)(2,1)S(1)}, bf16[320,512]{1,0:T(8,128)(2,1)S(1)}, u32[]{:S(2)}, u32[]{:S(2)}) collective-permute-start(bf16[320,512]{1,0:T(8,128)(2,1)S(1)} %get-tuple-element.62), channel_id=1, source_target_pairs={{0,2},{1,3},{2,0},{3,1},{4,6},{5,7},{6,4},{7,5},{8,10},{9,11},{10,... | collective-permute-start | bytes 983048 | tf_op jit(solution)/shard_map/ppermute | solution.py:70
  30.2 8.2 %collective-permute-start.2 = (bf16[320,512]{1,0:T(8,128)(2,1)S(1)}, bf16[320,512]{1,0:T(8,128)(2,1)S(1)}, u32[]{:S(2)}, u32[]{:S(2)}) collective-permute-start(bf16[320,512]{1,0:T(8,128)(2,1)S(1)} %get-tuple-element.63), channel_id=1, source_target_pairs={{0,3},{1,0},{2,1},{3,2},{4,7},{5,4},{6,5},{7,6},{8,11},{9,8},{10,9... | collective-permute-start | bytes 983048 | tf_op jit(solution)/shard_map/ppermute | solution.py:70
  124.3 20.0 %copy-start.19 = (s32[2,320]{1,0:T(2,128)S(1)}, s32[2,320]{1,0:T(2,128)}, u32[]{:S(2)}) copy-start(s32[2,320]{1,0:T(2,128)} %get-tuple-element.55.t_ref) | copy-start | bytes 7684
  125.1 30.9 %copy-start.16 = (bf16[320,128]{1,0:T(8,128)(2,1)S(1)}, bf16[320,128]{1,0:T(8,128)(2,1)}, u32[]{:S(2)}) copy-start(bf16[320,128]{1,0:T(8,128)(2,1)} %c_ref.3) | copy-start | bytes 245764
  125.1 30.9 %all-to-all-start.5 = ((bf16[32,32,128]{2,1,0:T(8,128)(2,1)}), bf16[32,32,128]{2,1,0:T(8,128)(2,1)}, u32[]{:S(2)}, u32[]{:S(2)}) async-start(bf16[32,32,128]{2,1,0:T(8,128)(2,1)} %bitcast.27), calls=%async_computation.5 | async-start | bytes 524288 | tf_op jit(solution)/shard_map/all_to_all | solution.py:478
  135.7 29.0 %copy-start.4 = (bf16[256,512]{1,0:T(8,128)(2,1)S(1)}, bf16[256,512]{1,0:T(8,128)(2,1)}, u32[]{:S(2)}) copy-start(bf16[256,512]{1,0:T(8,128)(2,1)} %copy-done.2) | copy-start | bytes 786436
  135.7 11.7 %collective-permute-start.3 = (bf16[256,512]{1,0:T(8,128)(2,1)S(1)}, bf16[256,512]{1,0:T(8,128)(2,1)S(1)}, u32[]{:S(2)}, u32[]{:S(2)}) collective-permute-start(bf16[256,512]{1,0:T(8,128)(2,1)S(1)} %get-tuple-element.75), channel_id=1, source_target_pairs={{0,4},{4,8},{8,12},{12,0},{1,5},{5,9},{9,13},{13,1},{2,6},{6,10},{... | collective-permute-start | bytes 786440 | tf_op jit(solution)/shard_map/ppermute | solution.py:70
  138.1 9.3 %collective-permute-start.4 = (bf16[256,512]{1,0:T(8,128)(2,1)S(1)}, bf16[256,512]{1,0:T(8,128)(2,1)S(1)}, u32[]{:S(2)}, u32[]{:S(2)}) collective-permute-start(bf16[256,512]{1,0:T(8,128)(2,1)S(1)} %get-tuple-element.76), channel_id=1, source_target_pairs={{0,8},{4,12},{8,0},{12,4},{1,9},{5,13},{9,1},{13,5},{2,10},{6,14},... | collective-permute-start | bytes 786440 | tf_op jit(solution)/shard_map/ppermute | solution.py:70
  141.8 8.1 %collective-permute-start.5 = (bf16[256,512]{1,0:T(8,128)(2,1)S(1)}, bf16[256,512]{1,0:T(8,128)(2,1)S(1)}, u32[]{:S(2)}, u32[]{:S(2)}) collective-permute-start(bf16[256,512]{1,0:T(8,128)(2,1)S(1)} %get-tuple-element.77), channel_id=1, source_target_pairs={{0,12},{4,0},{8,4},{12,8},{1,13},{5,1},{9,5},{13,9},{2,14},{6,2},{... | collective-permute-start | bytes 786440 | tf_op jit(solution)/shard_map/ppermute | solution.py:70
  161.3 5.0 %collective-permute-start.6 = (bf16[16,64,128]{2,1,0:T(8,128)(2,1)S(1)}, bf16[16,64,128]{2,1,0:T(8,128)(2,1)S(1)}, u32[]{:S(2)}, u32[]{:S(2)}) collective-permute-start(bf16[16,64,128]{2,1,0:T(8,128)(2,1)S(1)} %get-tuple-element.81), channel_id=1, source_target_pairs={{0,16},{16,0},{1,17},{17,1},{2,18},{18,2},{3,19},{19,3},{4,20},{20... | collective-permute-start | bytes 786440 | tf_op jit(solution)/shard_map/ppermute | solution.py:495
  184.7 30.8 %all-to-all-start.7 = ((bf16[16,32,128]{2,1,0:T(8,128)(2,1)}), bf16[16,32,128]{2,1,0:T(8,128)(2,1)S(1)}, u32[]{:S(2)}, u32[]{:S(2)}) async-start(bf16[16,32,128]{2,1,0:T(8,128)(2,1)} %proj_part.1), calls=%async_computation.7 | async-start | bytes 262144 | tf_op jit(solution)/shard_map/all_to_all | solution.py:547
  193.7 16.8 %copy-start.20 = (f32[31,64]{1,0:T(8,128)S(1)}, f32[31,64]{1,0:T(8,128)}, u32[]{:S(2)}) copy-start(f32[31,64]{1,0:T(8,128)} %param.24) | copy-start | bytes 23812
  197.3 13.3 %collective-permute-start.7 = (bf16[192,512]{1,0:T(8,128)(2,1)}, bf16[192,512]{1,0:T(8,128)(2,1)S(1)}, u32[]{:S(2)}, u32[]{:S(2)}) collective-permute-start(bf16[192,512]{1,0:T(8,128)(2,1)} %get-tuple-element.85), channel_id=1, source_target_pairs={{0,1},{1,2},{2,3},{3,0},{4,5},{5,6},{6,7},{7,4},{8,9},{9,10},{10,1... | collective-permute-start | bytes 589832 | tf_op jit(solution)/shard_map/ppermute | solution.py:70
  199.3 11.3 %collective-permute-start.8 = (bf16[192,512]{1,0:T(8,128)(2,1)}, bf16[192,512]{1,0:T(8,128)(2,1)S(1)}, u32[]{:S(2)}, u32[]{:S(2)}) collective-permute-start(bf16[192,512]{1,0:T(8,128)(2,1)} %get-tuple-element.86), channel_id=1, source_target_pairs={{0,2},{1,3},{2,0},{3,1},{4,6},{5,7},{6,4},{7,5},{8,10},{9,11},{10,... | collective-permute-start | bytes 589832 | tf_op jit(solution)/shard_map/ppermute | solution.py:70
  203.2 7.4 %collective-permute-start.9 = (bf16[192,512]{1,0:T(8,128)(2,1)}, bf16[192,512]{1,0:T(8,128)(2,1)S(1)}, u32[]{:S(2)}, u32[]{:S(2)}) collective-permute-start(bf16[192,512]{1,0:T(8,128)(2,1)} %get-tuple-element.87), channel_id=1, source_target_pairs={{0,3},{1,0},{2,1},{3,2},{4,7},{5,4},{6,5},{7,6},{8,11},{9,8},{10,9... | collective-permute-start | bytes 589832 | tf_op jit(solution)/shard_map/ppermute | solution.py:70
  206.1 7.5 %collective-permute-start.10 = (f32[64,128]{1,0:T(8,128)S(1)}, f32[64,128]{1,0:T(8,128)S(1)}, u32[]{:S(2)}, u32[]{:S(2)}) collective-permute-start(f32[64,128]{1,0:T(8,128)S(1)} %get-tuple-element.95), channel_id=1, source_target_pairs={{16,0},{32,16},{48,32},{64,48},{80,64},{96,80},{112,96},{128,112},... | collective-permute-start | bytes 98312 | tf_op jit(solution)/shard_map/ppermute | solution.py:568
  (12 other events, 47.7 us)
